TPU v7x, 128 devices: a whole 4x4x4 slice. The times are simulated.
128 devices in a mesh: sp: 16 (over z, y), dp: 8 (over x, core).
Axes of the slice: x: 4, y: 4, z: 4, core: 2. Of those that a mesh axis runs over, the one named last changes fastest.
Arguments:
- hidden_in: bfloat16 [2048, 16, 2048], P('sp', 'dp'), may hold values from -6 to 6
- query_act: bfloat16 [2048, 16, 1024], P('sp', 'dp'), may hold values from -4 to 4
- key_act: bfloat16 [2048, 16, 1024], P('sp', 'dp'), may hold values from -4 to 4
- gate_act: bfloat16 [2048, 16, 1024], P('sp', 'dp'), may hold values from -4 to 4
- decay_bias: float32 [1024], replicated, as said below
- value_weight: bfloat16 [2048, 2048], P('dp'), may hold values from -0.125 to 0.125
- out_grad: bfloat16 [2048, 16, 2048], P('sp', 'dp'), may hold values from -0.29882812 to 0.29882812
Outputs:
- hidden_grad: bfloat16 [2048, 16, 2048], P('sp', 'dp')
- query_grad: bfloat16 [2048, 16, 1024], P('sp', 'dp')
- key_grad: bfloat16 [2048, 16, 1024], P('sp', 'dp')
- gate_grad: bfloat16 [2048, 16, 1024], P('sp', 'dp')
- weight_grad: float32 [2048, 2048], P('dp', 'sp')
Inputs may be any that keep to these rules, and one draw needn't show every extreme that they name: `decay_bias`: every offset is at least -1 and at most 1 plus the natural logarithm of 128.
All inputs are finite; a program needn't handle non-finite values.
Results may differ from a plain program's by a relative error of at most 0.018.
Values may be sent and summed in bfloat16 or wider, within the bound.
No kernel may reach another device: no remote copies, remote signals or barrier semaphores. Data moves between devices by JAX's collectives and lax.ppermute only.
A program may use at most 128 MiB of HBM per device.

v0:
```python
import functools

import jax
import jax.numpy as jnp
from jax import lax
from jax.experimental import pallas as pl
from jax.experimental.pallas import tpu as pltpu
from jax.sharding import PartitionSpec as P

HEADS = 8
DK = 128
DV = 256
BLK = 128
EXTRA = 16
SOFTNESS = 16.0
SCALE = DK**-0.5
F32 = jnp.float32
BF16 = jnp.bfloat16

NN = (((1,), (0,)), ((), ()))
NT = (((1,), (1,)), ((), ()))
TN = (((0,), (0,)), ((), ()))


def dot(a, b, dims):
    return lax.dot_general(a, b, dims, preferred_element_type=F32)


def split2(x):
    hi = x.astype(BF16)
    lo = (x - hi.astype(F32)).astype(BF16)
    return hi, lo


def iota_pair(shape):
    return (
        lax.broadcasted_iota(jnp.int32, shape, 0),
        lax.broadcasted_iota(jnp.int32, shape, 1),
    )


def cost(flops, moved):
    return pl.CostEstimate(flops=flops, bytes_accessed=moved, transcendentals=0)


def params():
    return pltpu.CompilerParams(dimension_semantics=("arbitrary",))


def decay_kernel(pair, q_ref, g_ref, bias_ref, do_ref, delta_ref, cum_ref):
    row, col = iota_pair((BLK, BLK))
    lower = (row >= col).astype(BF16)
    for s in range(2):
        for j in range(pair):
            keys = slice(j * DK, (j + 1) * DK)
            x = g_ref[s, :, keys].astype(F32) + bias_ref[:, keys]
            log_decay = (jnp.minimum(x, 0.0) - jnp.log1p(jnp.exp(-jnp.abs(x)))) / SOFTNESS
            hi, lo = split2(log_decay)
            cum = dot(lower, hi, NN) + dot(lower, lo, NN)
            cum_ref[s, :, keys] = cum
            q_dec = (q_ref[s, :, keys].astype(F32) * SCALE * jnp.exp(cum)).astype(BF16)
            delta = dot(do_ref[s, :, j * DV : (j + 1) * DV], q_dec, TN)
            delta_ref[s, j, :DV, :] = delta.astype(BF16)
            last = cum[BLK - 1 : BLK, :]
            one, two = split2(last)
            three = (last - one.astype(F32) - two.astype(F32)).astype(BF16)
            rows = lax.broadcasted_iota(jnp.int32, (EXTRA, DK), 0)
            tail = jnp.where(
                rows == 0,
                one.astype(F32),
                jnp.where(rows == 1, two.astype(F32), three.astype(F32)),
            )
            delta_ref[s, j, DV:, :] = tail.astype(BF16)


def intra_kernel(pair, q_ref, k_ref, cum_ref, do_ref, dv_ref):
    row, col = iota_pair((BLK, BLK))
    for s in range(2):
        for j in range(pair):
            keys = slice(j * DK, (j + 1) * DK)
            vals = slice(j * DV, (j + 1) * DV)
            cum = cum_ref[s, :, keys]
            q_dec = (q_ref[s, :, keys].astype(F32) * SCALE * jnp.exp(cum)).astype(BF16)
            k_inv = (k_ref[s, :, keys].astype(F32) * jnp.exp(-cum)).astype(BF16)
            scores = dot(q_dec, k_inv, NT)
            scores = jnp.where(row >= col, scores, 0.0).astype(BF16)
            dv_ref[s, :, vals] = dot(scores, do_ref[s, :, vals], TN)


def scan_kernel(blocks, reverse, rx_ref, last_ref, out_ref):
    state = jnp.zeros((DV, DK), F32)
    order = range(blocks - 1, -1, -1) if reverse else range(blocks)
    for b in order:
        out_ref[b] = state.astype(BF16)
        tail = last_ref[b].astype(F32)
        decay = jnp.exp(tail[0:1] + tail[1:2] + tail[2:3])
        state = state * decay + rx_ref[b, :DV, :].astype(F32)


def value_grad_kernel(pair, k_ref, cum_ref, dstate_ref, dv_in_ref, dv_ref):
    for s in range(2):
        for j in range(pair):
            keys = slice(j * DK, (j + 1) * DK)
            vals = slice(j * DV, (j + 1) * DV)
            cum = cum_ref[s, :, keys]
            last = cum[BLK - 1 : BLK, :]
            k_dec = (k_ref[s, :, keys].astype(F32) * jnp.exp(last - cum)).astype(BF16)
            inter = dot(k_dec, dstate_ref[s, j], NT)
            dv_ref[s, :, vals] = (dv_in_ref[s, :, vals] + inter).astype(BF16)


def project_kernel(h_ref, w_ref, k_ref, cum_ref, v_ref, delta_ref):
    v_all = dot(h_ref[...], w_ref[...], NN).astype(BF16)
    for s in range(2):
        v = v_all[s * BLK : (s + 1) * BLK]
        v_ref[s] = v
        cum = cum_ref[s]
        last = cum[BLK - 1 : BLK, :]
        k_dec = (k_ref[s].astype(F32) * jnp.exp(last - cum)).astype(BF16)
        delta_ref[s, 0] = dot(v, k_dec, TN).astype(BF16)


def final_kernel(
    pair,
    q_ref,
    k_ref,
    g_ref,
    bias_ref,
    cum_ref,
    do_ref,
    v_ref,
    state_ref,
    dstate_ref,
    dq_ref,
    dk_ref,
    dg_ref,
):
    row, col = iota_pair((BLK, BLK))
    row2, col2 = iota_pair((BLK, 2 * BLK))
    sums = ((col2 >= row2) & (col2 < BLK) | (col2 - BLK < row2) & (col2 >= BLK)).astype(BF16)
    for s in range(2):
        for j in range(pair):
            keys = slice(j * DK, (j + 1) * DK)
            vals = slice(j * DV, (j + 1) * DV)
            cum = cum_ref[s, :, keys]
            last = cum[BLK - 1 : BLK, :]
            q_scale = SCALE * jnp.exp(cum)
            inv_scale = jnp.exp(-cum)
            dec_scale = jnp.exp(last - cum)
            k = k_ref[s, :, keys].astype(F32)
            q_dec = (q_ref[s, :, keys].astype(F32) * q_scale).astype(BF16)
            k_inv = (k * inv_scale).astype(BF16)
            k_dec = (k * dec_scale).astype(BF16)
            do = do_ref[s, :, vals]
            v = v_ref[s, :, vals]
            state = state_ref[s, j]
            dstate = dstate_ref[s, j]
            dscores = jnp.where(row >= col, dot(do, v, NT), 0.0).astype(BF16)
            dq_intra = dot(dscores, k_inv, NN)
            dk_inv = dot(dscores, q_dec, TN)
            dq_inter = dot(do, state, NN)
            dk_dec = dot(v, dstate, NN)
            dq_ref[s, :, keys] = (q_scale * (dq_intra + dq_inter)).astype(BF16)
            dk_ref[s, :, keys] = (inv_scale * dk_inv + dec_scale * dk_dec).astype(BF16)
            q_dec = q_dec.astype(F32)
            after = q_dec * (dq_intra + dq_inter) - k_inv.astype(F32) * dk_inv
            before = k_dec.astype(F32) * dk_dec
            hi, lo = split2(jnp.concatenate([after, before], axis=0))
            through = jnp.sum(state.astype(F32) * dstate.astype(F32), axis=0, keepdims=True)
            dlog = dot(sums, hi, NN) + dot(sums, lo, NN) + jnp.exp(last) * through
            x = g_ref[s, :, keys].astype(F32) + bias_ref[:, keys]
            slope = (1.0 / SOFTNESS) / (1.0 + jnp.exp(x))
            dg_ref[s, :, keys] = (dlog * slope).astype(BF16)


def local(hidden_in, query_act, key_act, gate_act, decay_bias, value_weight, out_grad):
    positions, sequences, width = hidden_in.shape
    blocks = lax.axis_size("sp")
    weight = lax.all_gather(value_weight, "dp", axis=0, tiled=True)
    items = sequences * HEADS
    pair = 2
    steps = HEADS // pair

    q = jnp.transpose(query_act, (1, 0, 2))
    k = jnp.transpose(key_act, (1, 0, 2))
    g = jnp.transpose(gate_act, (1, 0, 2))
    do = jnp.transpose(out_grad, (1, 0, 2))
    flat = jnp.transpose(hidden_in, (1, 0, 2)).reshape(sequences * positions, width)
    bias = decay_bias.reshape(1, HEADS * DK)

    key_spec = pl.BlockSpec((2, BLK, pair * DK), lambda i: (0, 0, i))
    val_spec = pl.BlockSpec((2, BLK, pair * DV), lambda i: (0, 0, i))
    bias_spec = pl.BlockSpec((1, pair * DK), lambda i: (0, i))
    state_spec = pl.BlockSpec((2, pair, DV, DK), lambda i: (0, i, 0, 0))
    key_shape = (sequences, positions, HEADS * DK)
    val_shape = (sequences, positions, HEADS * DV)
    state_shape = (sequences, HEADS, DV, DK)
    mm = 2 * BLK * DK * DV * items

    delta, cum = pl.pallas_call(
        functools.partial(decay_kernel, pair),
        grid=(steps,),
        in_specs=[key_spec, key_spec, bias_spec, val_spec],
        out_specs=[
            pl.BlockSpec((2, pair, DV + EXTRA, DK), lambda i: (0, i, 0, 0)),
            key_spec,
        ],
        out_shape=[
            jax.ShapeDtypeStruct((sequences, HEADS, DV + EXTRA, DK), BF16),
            jax.ShapeDtypeStruct(key_shape, F32),
        ],
        compiler_params=params(),
        cost_estimate=cost(3 * mm, 5 << 20),
        name="decay",
    )(q, g, bias, do)

    rx = lax.all_to_all(
        delta.reshape(items, DV + EXTRA, DK), "sp", split_axis=0, concat_axis=0, tiled=True
    )
    dv_intra = pl.pallas_call(
        functools.partial(intra_kernel, pair),
        grid=(steps,),
        in_specs=[key_spec, key_spec, key_spec, val_spec],
        out_specs=val_spec,
        out_shape=jax.ShapeDtypeStruct(val_shape, F32),
        compiler_params=params(),
        cost_estimate=cost(3 * mm, 5 << 20),
        name="intra",
    )(q, k, cum, do)

    tails = lax.slice_in_dim(rx, DV, DV + EXTRA, axis=1)

    def scan(arrived, reverse):
        return pl.pallas_call(
            functools.partial(scan_kernel, blocks, reverse),
            out_shape=jax.ShapeDtypeStruct((blocks, DV, DK), BF16),
            cost_estimate=cost(mm, 3 << 20),
            name="scan",
        )(arrived, tails)

    dstate = lax.all_to_all(scan(rx, True), "sp", split_axis=0, concat_axis=0, tiled=True)
    dstate = dstate.reshape(state_shape)

    dv = pl.pallas_call(
        functools.partial(value_grad_kernel, pair),
        grid=(steps,),
        in_specs=[key_spec, key_spec, state_spec, val_spec],
        out_specs=val_spec,
        out_shape=jax.ShapeDtypeStruct(val_shape, BF16),
        compiler_params=params(),
        cost_estimate=cost(mm, 5 << 20),
        name="value_grad",
    )(k, cum, dstate, dv_intra)
    flat_dv = dv.reshape(sequences * positions, HEADS * DV)

    partial = dot(flat, flat_dv, TN).astype(BF16)
    partial = lax.psum_scatter(partial, "dp", scatter_dimension=0, tiled=True)

    v, vdelta = pl.pallas_call(
        project_kernel,
        grid=(HEADS,),
        in_specs=[
            pl.BlockSpec((sequences * positions, width), lambda i: (0, 0)),
            pl.BlockSpec((width, DV), lambda i: (0, i)),
            pl.BlockSpec((2, BLK, DK), lambda i: (0, 0, i)),
            pl.BlockSpec((2, BLK, DK), lambda i: (0, 0, i)),
        ],
        out_specs=[
            pl.BlockSpec((2, BLK, DV), lambda i: (0, 0, i)),
            pl.BlockSpec((2, 1, DV, DK), lambda i: (0, i, 0, 0)),
        ],
        out_shape=[
            jax.ShapeDtypeStruct(val_shape, BF16),
            jax.ShapeDtypeStruct(state_shape, BF16),
        ],
        compiler_params=params(),
        cost_estimate=cost(2 * 256 * width * HEADS * DV + mm, 12 << 20),
        name="project",
    )(flat, weight, k, cum)

    vrx = lax.all_to_all(
        vdelta.reshape(items, DV, DK), "sp", split_axis=0, concat_axis=0, tiled=True
    )
    state = lax.all_to_all(scan(vrx, False), "sp", split_axis=0, concat_axis=0, tiled=True)
    state = state.reshape(state_shape)

    hidden_grad = dot(flat_dv, weight, NT).astype(BF16)

    dq, dk, dg = pl.pallas_call(
        functools.partial(final_kernel, pair),
        grid=(steps,),
        in_specs=[
            key_spec,
            key_spec,
            key_spec,
            bias_spec,
            key_spec,
            val_spec,
            val_spec,
            state_spec,
            state_spec,
        ],
        out_specs=[key_spec, key_spec, key_spec],
        out_shape=[jax.ShapeDtypeStruct(key_shape, BF16)] * 3,
        compiler_params=params(),
        cost_estimate=cost(6 * mm, 10 << 20),
        name="final",
    )(q, k, g, bias, cum, do, v, state, dstate)

    tiles = partial.reshape(partial.shape[0], blocks, -1).transpose(1, 0, 2)
    tiles = lax.all_to_all(tiles, "sp", split_axis=0, concat_axis=0, tiled=True)
    weight_grad = jnp.sum(tiles.astype(F32), axis=0)

    def back(value):
        return jnp.transpose(value.reshape(sequences, positions, -1), (1, 0, 2))

    return (back(hidden_grad), back(dq), back(dk), back(dg), weight_grad)


def solution(mesh):
    return jax.shard_map(
        local,
        mesh=mesh,
        in_specs=(
            P("sp", "dp", None),
            P("sp", "dp", None),
            P("sp", "dp", None),
            P("sp", "dp", None),
            P(),
            P("dp", None),
            P("sp", "dp", None),
        ),
        out_specs=(
            P("sp", "dp", None),
            P("sp", "dp", None),
            P("sp", "dp", None),
            P("sp", "dp", None),
            P("dp", "sp"),
        ),
        check_vma=False,
    )
```

profile of v0, /device:TPU:8, one launch (start us, length us, event | category | flops | bytes accessed | tf_op | source)
XLA Modules:
  0.0 169.8 jit_solution(13571628343304339369)
XLA Ops:
  7.2 0.0 copy-start.4
  7.2 0.0 all-gather.2.cloned.1.call-start
  7.2 0.7 all-gather.2.cloned.1.call-update
  7.9 2.6 %copy.44 = bf16[128,2,2048]{2,0,1:T(8,128)(2,1)} copy(bf16[128,2,2048]{2,1,0:T(2,128)(2,1)} %param.13) | data formatting | bytes 2097152 | tf_op args[6]
  10.5 2.4 %copy_bitcast_fusion.2 = (bf16[2,128,1024]{2,1,0:T(8,128)(2,1)}, bf16[2,128,1024]{2,1,0:T(8,128)(2,1)}) fusion(bf16[128,2,1024]{2,1,0:T(2,128)(2,1)} %param.10, bf16[128,2,1024]{2,1,0:T(2,128)(2,1)} %param.8), kind=kLoop, calls=%fused_computation.6 | loop fusion | bytes 2097152 | tf_op jit(solution)/shard_map/transpose | solution.py:186
  12.9 4.9 %decay.1 = (bf16[2,8,272,128]{3,2,1,0:T(8,128)(2,1)}, f32[2,128,1024]{2,1,0:T(8,128)}) custom-call(bf16[2,128,1024]{2,1,0:T(8,128)(2,1)} %get-tuple-element.30.q_ref, bf16[2,128,1024]{2,1,0:T(8,128)(2,1)} %get-tuple-element.29.g_ref, f32[1,1024]{1,0:T(1,128)} %bitcast.59, bf16[2,128,2048]{2,1,0:T(8,128)(2,1)} %bitcast.37), custom_call_target="tpu_custom_call" | custom-call | flops 402653184 | bytes 5242880 | tf_op jit(solution)/shard_map/decay/pallas_call | solution.py:200
  17.8 24.9 %all_to_all.25.rx_ref = bf16[16,272,128]{2,1,0:T(8,128)(2,1)S(1)} all-to-all(bf16[16,272,128]{2,1,0:T(8,128)(2,1)} %bitcast.51), channel_id=1, replica_groups=mesh['sp'=16,'dp'=8] {'sp'}, dimensions={0} | all-to-all | bytes 2228224 | tf_op jit(solution)/shard_map/all_to_all | solution.py:217
  42.7 0.0 copy-start.2
  42.7 0.0 copy-start.3
  42.8 0.6 slice.4.last_ref
  43.4 0.5 copy-done.2
  43.8 2.6 %scan.2 = bf16[16,256,128]{2,1,0:T(8,128)(2,1)} custom-call(bf16[16,272,128]{2,1,0:T(8,128)(2,1)} %copy-done.2, bf16[16,16,128]{2,1,0:T(8,128)(2,1)} %slice.4.last_ref), custom_call_target="tpu_custom_call" | custom-call | flops 134217728 | bytes 3145728 | tf_op jit(solution)/shard_map/scan/pallas_call | solution.py:234
  46.4 4.9 %all-to-all-start.1 = ((bf16[16,256,128]{2,1,0:T(8,128)(2,1)}), bf16[16,256,128]{2,1,0:T(8,128)(2,1)S(1)}, u32[]{:S(2)}, u32[]{:S(2)}) async-start(bf16[16,256,128]{2,1,0:T(8,128)(2,1)} %scan.2), calls=%async_computation.1 | async-start | bytes 2097152 | tf_op jit(solution)/shard_map/all_to_all | solution.py:241
  51.3 0.0 reduce-scatter.2.cloned.1.call-start
  51.3 0.0 copy-done.4
  51.3 0.9 copy.45
  52.3 6.4 %intra.1.dv_in_ref = f32[2,128,2048]{2,1,0:T(8,128)} custom-call(bf16[2,128,1024]{2,1,0:T(8,128)(2,1)} %get-tuple-element.30.q_ref, bf16[2,128,1024]{2,1,0:T(8,128)(2,1)} %bitcast.40, f32[2,128,1024]{2,1,0:T(8,128)} %get-tuple-element.12.cum_ref, bf16[2,128,2048]{2,1,0:T(8,128)(2,1)} %bitcast.38), custom_call_target="tpu_custom_call" | custom-call | flops 402653184 | bytes 5242880 | tf_op jit(solution)/shard_map/intra/pallas_call | solution.py:220
  58.6 7.8 %all-to-all-done.1 = bf16[16,256,128]{2,1,0:T(8,128)(2,1)S(1)} async-done(((bf16[16,256,128]{2,1,0:T(8,128)(2,1)}), bf16[16,256,128]{2,1,0:T(8,128)(2,1)S(1)}, u32[]{:S(2)}, u32[]{:S(2)}) %all-to-all-start.1) | async-done | bytes 1048608 | tf_op jit(solution)/shard_map/all_to_all | solution.py:241
  66.4 0.0 copy-start
  66.4 1.0 copy-done
  67.4 4.5 %value_grad.1 = bf16[2,128,2048]{2,1,0:T(8,128)(2,1)} custom-call(bf16[2,128,1024]{2,1,0:T(8,128)(2,1)} %bitcast.41, f32[2,128,1024]{2,1,0:T(8,128)} %get-tuple-element.12.cum_ref, bf16[2,8,256,128]{3,2,1,0:T(8,128)(2,1)} %bitcast.44, f32[2,128,2048]{2,1,0:T(8,128)} %intra.1.dv_in_ref), custom_call_target="tpu_custom_call" | custom-call | flops 134217728 | bytes 5242880 | tf_op jit(solution)/shard_map/value_grad/pallas_call | solution.py:244
  71.9 0.0 copy-done.3
  71.9 6.9 %fusion = bf16[2048,2048]{0,1:T(8,128)(2,1)} fusion(bf16[2,128,2048]{2,1,0:T(8,128)(2,1)} %value_grad.1, bf16[2,128,2048]{2,0,1:T(2,128)(2,1)S(1)} %bitcast.48), kind=kOutput, calls=%fused_computation.1 | convolution fusion | flops 2151677952 | bytes 10485760 | tf_op jit(solution)/shard_map/dot_general | solution.py:26
  78.8 0.0 reduce-scatter.2.cloned.1.call-update
  78.8 1.4 copy.28
  80.2 0.0 all-gather.2.cloned.1.call-done.w_ref
  80.2 0.0 copy-start.1
  80.2 10.4 %project.1 = (bf16[2,128,2048]{2,1,0:T(8,128)(2,1)}, bf16[2,8,256,128]{3,2,1,0:T(8,128)(2,1)}) custom-call(bf16[256,2048]{1,0:T(8,128)(2,1)} %bitcast.50, bf16[2048,2048]{1,0:T(8,128)(2,1)} %all-gather.2.cloned.1.call-done.w_ref, bf16[2,128,1024]{2,1,0:T(8,128)(2,1)} %bitcast.42, f32[2,128,1024]{2,1,0:T(8,128)} %get-tuple-element.12.cum_ref), custom_call_target="tpu_custom_call" | custom-call | flops 2281701376 | bytes 12582912 | tf_op jit(solution)/shard_map/project/pallas_call | solution.py:259
  90.6 19.9 %all_to_all.26.rx_ref = bf16[16,256,128]{2,1,0:T(8,128)(2,1)} all-to-all(bf16[16,256,128]{2,1,0:T(8,128)(2,1)} %bitcast.54), channel_id=1, replica_groups=mesh['sp'=16,'dp'=8] {'sp'}, dimensions={0} | all-to-all | bytes 2097152 | tf_op jit(solution)/shard_map/all_to_all | solution.py:281
  110.5 2.5 %scan.3 = bf16[16,256,128]{2,1,0:T(8,128)(2,1)} custom-call(bf16[16,256,128]{2,1,0:T(8,128)(2,1)} %all_to_all.26.rx_ref, bf16[16,16,128]{2,1,0:T(8,128)(2,1)} %slice.4.last_ref), custom_call_target="tpu_custom_call" | custom-call | flops 134217728 | bytes 3145728 | tf_op jit(solution)/shard_map/scan/pallas_call | solution.py:234
  113.0 19.0 %all_to_all.27 = bf16[16,256,128]{2,1,0:T(8,128)(2,1)} all-to-all(bf16[16,256,128]{2,1,0:T(8,128)(2,1)} %scan.3), channel_id=1, replica_groups=mesh['sp'=16,'dp'=8] {'sp'}, dimensions={0} | all-to-all | bytes 2097152 | tf_op jit(solution)/shard_map/all_to_all | solution.py:284
  132.0 0.0 reduce-scatter.2.cloned.1.call-done
  132.0 5.2 %all-to-all-start.4 = ((bf16[16,256,128]{1,2,0:T(8,128)(2,1)}), bf16[16,256,128]{1,2,0:T(8,128)(2,1)S(1)}, u32[]{:S(2)}, u32[]{:S(2)}) async-start(bf16[16,256,128]{1,2,0:T(8,128)(2,1)} %bitcast.52), calls=%async_computation.5 | async-start | bytes 2097152 | tf_op jit(solution)/shard_map/all_to_all | solution.py:311
  137.2 0.0 copy-done.1
  137.2 5.7 %convolution_convert_fusion = bf16[256,2048]{1,0:T(8,128)(2,1)S(1)} fusion(bf16[256,2048]{1,0:T(8,128)(2,1)S(1)} %bitcast.46, bf16[2048,2048]{1,0:T(8,128)(2,1)} %all-gather.2.cloned.1.call-done.w_ref), kind=kOutput, calls=%fused_computation.2 | convolution fusion | flops 2148007936 | bytes 10485760 | tf_op jit(solution)/shard_map/dot_general | solution.py:26
  143.0 2.0 %copy.43 = bf16[2,128,2048]{2,0,1:T(2,128)(2,1)} copy(bf16[2,128,2048]{2,1,0:T(8,128)(2,1)S(1)} %bitcast.55) | data formatting | bytes 2097152 | tf_op jit(solution)/shard_map/reshape | solution.py:315
  145.0 9.9 %final.1 = (bf16[2,128,1024]{2,1,0:T(8,128)(2,1)}, bf16[2,128,1024]{2,1,0:T(8,128)(2,1)}, bf16[2,128,1024]{2,1,0:T(8,128)(2,1)}) custom-call(bf16[2,128,1024]{2,1,0:T(8,128)(2,1)} %get-tuple-element.30.q_ref, bf16[2,128,1024]{2,1,0:T(8,128)(2,1)} %bitcast.43, bf16[2,128,1024]{2,1,0:T(8,128)(2,1)} %get-tuple-element.29.g_ref, f32[1,1024]{1,0:T(1,128)} %bitcast.60, ...), custom_call_target="tpu_custom_call" | custom-call | flops 805306368 | bytes 10485760 | tf_op jit(solution)/shard_map/final/pallas_call | solution.py:289
  154.9 2.4 %copy.31 = bf16[128,2,1024]{2,1,0:T(2,128)(2,1)} copy(bf16[128,2,1024]{2,0,1:T(8,128)(2,1)} %bitcast.58) | data formatting | bytes 1048576
  157.3 2.4 %copy.32 = bf16[128,2,1024]{2,1,0:T(2,128)(2,1)} copy(bf16[128,2,1024]{2,0,1:T(8,128)(2,1)} %bitcast.57) | data formatting | bytes 1048576
  159.6 2.4 %copy.33 = bf16[128,2,1024]{2,1,0:T(2,128)(2,1)} copy(bf16[128,2,1024]{2,0,1:T(8,128)(2,1)} %bitcast.56) | data formatting | bytes 1048576
  162.0 0.0 all-to-all-done.4
  162.0 0.1 convert_reduce_fusion
  162.2 0.8 copy.34
Async XLA Ops:
  7.2 44.2 %copy-start.4 = (bf16[128,2,1024]{2,1,0:T(2,128)(2,1)S(1)}, bf16[128,2,1024]{2,1,0:T(2,128)(2,1)}, u32[]{:S(2)}) copy-start(bf16[128,2,1024]{2,1,0:T(2,128)(2,1)} %param.9) | copy-start | bytes 1572868
  7.2 73.0 %all-gather.2.cloned.1.call-start = ((), (), s32[]{:S(2)}) async-start(), calls=%async_computation.6 | async-start | bytes 9437184 | tf_op jit(solution)/shard_map/all_gather | solution.py:179
  42.7 1.1 copy-start.2
  42.7 29.1 %copy-start.3 = (bf16[128,2,2048]{2,1,0:T(2,128)(2,1)S(1)}, bf16[128,2,2048]{2,1,0:T(2,128)(2,1)}, u32[]{:S(2)}) copy-start(bf16[128,2,2048]{2,1,0:T(2,128)(2,1)} %param.7) | copy-start | bytes 3145732
  46.4 20.0 %all-to-all-start.1 = ((bf16[16,256,128]{2,1,0:T(8,128)(2,1)}), bf16[16,256,128]{2,1,0:T(8,128)(2,1)S(1)}, u32[]{:S(2)}, u32[]{:S(2)}) async-start(bf16[16,256,128]{2,1,0:T(8,128)(2,1)} %scan.2), calls=%async_computation.1 | async-start | bytes 2097152 | tf_op jit(solution)/shard_map/all_to_all | solution.py:241
  51.3 80.7 %reduce-scatter.2.cloned.1.call-start = ((), (), s32[]{:S(2)}) async-start(), calls=%async_computation.7 | async-start | bytes 9437184 | tf_op jit(solution)/shard_map/reduce_scatter | solution.py:257
  66.4 1.0 copy-start
  80.2 57.0 %copy-start.1 = (bf16[2,128,2048]{2,1,0:T(8,128)(2,1)S(1)}, bf16[2,128,2048]{2,1,0:T(8,128)(2,1)}, u32[]{:S(2)}) copy-start(bf16[2,128,2048]{2,1,0:T(8,128)(2,1)} %value_grad.1) | copy-start | bytes 3145732
  132.0 30.0 %all-to-all-start.4 = ((bf16[16,256,128]{1,2,0:T(8,128)(2,1)}), bf16[16,256,128]{1,2,0:T(8,128)(2,1)S(1)}, u32[]{:S(2)}, u32[]{:S(2)}) async-start(bf16[16,256,128]{1,2,0:T(8,128)(2,1)} %bitcast.52), calls=%async_computation.5 | async-start | bytes 2097152 | tf_op jit(solution)/shard_map/all_to_all | solution.py:311
Sparse Core Ops, SparseCore 0:
  9.7 51.8 all-gather.1
  79.0 50.7 reduce-scatter.1
where the time goes:
time: 171 us; the launch traced here: 170 us
  blocking collectives  63.8 us (37%)
  Pallas kernels  41.1 us (24%)
  local copies, waits for them, and re-layouts  19.3 us (11%)
  between operations  14.1 us (8%)
  matrix products  12.7 us (7%)
  starting transfers between devices  10.1 us (6%)
  waiting for transfers between devices  8.47 us (5%)
    all_to_all x1, blocking collectives, local(): lax.all_to_all(delta.reshape(items, DV + EXTRA, DK), 'sp', split_axis=0,...  24.9 us
    all_to_all x1, blocking collectives, local(): lax.all_to_all(vdelta.reshape(items, DV, DK), 'sp', split_axis=0, concat_...  19.9 us
    all_to_all x1, blocking collectives, local(): lax.all_to_all(scan(vrx, False), 'sp', split_axis=0, concat_axis=0, tiled...  19 us
    unnamed x16, local copies, waits for them, and re-layouts  12.8 us
    dot_general x2, matrix products, dot(): return lax.dot_general(a, b, dims, preferred_element_type=F32)  12.7 us
    pallas_call x1, Pallas kernels, local(): pl.pallas_call(project_kernel, grid=(HEADS,), in_specs=[pl.BlockSpec((seq...  10.4 us
    pallas_call x1, Pallas kernels, local(): pl.pallas_call(functools.partial(final_kernel, pair), grid=(steps,), in_s...  9.87 us
    all_to_all x1, waiting for transfers between devices, local(): lax.all_to_all(scan(rx, True), 'sp', split_axis=0, concat_axis=0, tiled=T...  7.77 us
  transfers between devices with their start and end apart: 4, of which 1 were waited for; matrix products, arithmetic and copies ran while one was open for 18% of the time, Pallas kernels for 24%

commit v1 on v0

--- a/solution.py
+++ b/solution.py
@@ -73,51 +73,61 @@
             delta_ref[s, j, DV:, :] = tail.astype(BF16)
 
 
-def intra_kernel(pair, q_ref, k_ref, cum_ref, do_ref, dv_ref):
+def intra_kernel(pair, q_ref, k_ref, cum_ref, scores_ref, k_dec_ref):
     row, col = iota_pair((BLK, BLK))
     for s in range(2):
         for j in range(pair):
             keys = slice(j * DK, (j + 1) * DK)
-            vals = slice(j * DV, (j + 1) * DV)
             cum = cum_ref[s, :, keys]
+            last = cum[BLK - 1 : BLK, :]
+            k = k_ref[s, :, keys].astype(F32)
             q_dec = (q_ref[s, :, keys].astype(F32) * SCALE * jnp.exp(cum)).astype(BF16)
-            k_inv = (k_ref[s, :, keys].astype(F32) * jnp.exp(-cum)).astype(BF16)
+            k_inv = (k * jnp.exp(-cum)).astype(BF16)
             scores = dot(q_dec, k_inv, NT)
-            scores = jnp.where(row >= col, scores, 0.0).astype(BF16)
-            dv_ref[s, :, vals] = dot(scores, do_ref[s, :, vals], TN)
+            scores_ref[s, j] = jnp.where(row >= col, scores, 0.0).astype(BF16)
+            k_dec_ref[s, :, keys] = (k * jnp.exp(last - cum)).astype(BF16)
 
 
 def scan_kernel(blocks, reverse, rx_ref, last_ref, out_ref):
-    state = jnp.zeros((DV, DK), F32)
+    state = jnp.zeros(out_ref.shape[1:], F32)
     order = range(blocks - 1, -1, -1) if reverse else range(blocks)
     for b in order:
         out_ref[b] = state.astype(BF16)
         tail = last_ref[b].astype(F32)
         decay = jnp.exp(tail[0:1] + tail[1:2] + tail[2:3])
-        state = state * decay + rx_ref[b, :DV, :].astype(F32)
-
-
-def value_grad_kernel(pair, k_ref, cum_ref, dstate_ref, dv_in_ref, dv_ref):
-    for s in range(2):
-        for j in range(pair):
-            keys = slice(j * DK, (j + 1) * DK)
+        state = state * decay + rx_ref[b].astype(F32)
+
+
+def value_grad_kernel(
+    pair, scores_ref, do_ref, k_dec_ref, dstate_ref, turned_ref, dv_ref, part_ref
+):
+    rows = []
+    for s in range(2):
+        heads = []
+        for j in range(pair):
             vals = slice(j * DV, (j + 1) * DV)
-            cum = cum_ref[s, :, keys]
-            last = cum[BLK - 1 : BLK, :]
-            k_dec = (k_ref[s, :, keys].astype(F32) * jnp.exp(last - cum)).astype(BF16)
-            inter = dot(k_dec, dstate_ref[s, j], NT)
-            dv_ref[s, :, vals] = (dv_in_ref[s, :, vals] + inter).astype(BF16)
-
-
-def project_kernel(h_ref, w_ref, k_ref, cum_ref, v_ref, delta_ref):
+            k_dec = k_dec_ref[s, :, j * DK : (j + 1) * DK]
+            intra = dot(scores_ref[s, j], do_ref[s, :, vals], TN)
+            dv = (intra + dot(k_dec, dstate_ref[s, j], NT)).astype(BF16)
+            dv_ref[s, :, vals] = dv
+            heads.append(dv)
+        rows.append(jnp.concatenate(heads, axis=1))
+    dv_all = jnp.concatenate(rows, axis=0)
+    group, tiles, height, span = part_ref.shape
+    for m in range(group):
+        part = dot(turned_ref[m * height : (m + 1) * height, :], dv_all, NN).astype(BF16)
+        for t in range(tiles):
+            part_ref[m, t] = part[:, t * span : (t + 1) * span]
+
+
+def project_kernel(pair, h_ref, w_ref, k_dec_ref, v_ref, delta_ref):
     v_all = dot(h_ref[...], w_ref[...], NN).astype(BF16)
     for s in range(2):
-        v = v_all[s * BLK : (s + 1) * BLK]
-        v_ref[s] = v
-        cum = cum_ref[s]
-        last = cum[BLK - 1 : BLK, :]
-        k_dec = (k_ref[s].astype(F32) * jnp.exp(last - cum)).astype(BF16)
-        delta_ref[s, 0] = dot(v, k_dec, TN).astype(BF16)
+        v_ref[s] = v_all[s * BLK : (s + 1) * BLK]
+        for j in range(pair):
+            v = v_all[s * BLK : (s + 1) * BLK, j * DV : (j + 1) * DV]
+            k_dec = k_dec_ref[s, :, j * DK : (j + 1) * DK]
+            delta_ref[s, j] = dot(v, k_dec, TN).astype(BF16)
 
 
 def final_kernel(
@@ -173,29 +183,36 @@
             dg_ref[s, :, keys] = (dlog * slope).astype(BF16)
 
 
-def local(hidden_in, query_act, key_act, gate_act, decay_bias, value_weight, out_grad):
+def over_sp(value):
+    return lax.all_to_all(value, "sp", split_axis=0, concat_axis=0, tiled=True)
+
+
+def arranged(hidden_in, query_act, key_act, gate_act, decay_bias, value_weight, out_grad):
     positions, sequences, width = hidden_in.shape
     blocks = lax.axis_size("sp")
+    group = lax.axis_size("dp")
     weight = lax.all_gather(value_weight, "dp", axis=0, tiled=True)
     items = sequences * HEADS
     pair = 2
     steps = HEADS // pair
+    values = HEADS * DV
+    rows = sequences * positions
 
     q = jnp.transpose(query_act, (1, 0, 2))
-    k = jnp.transpose(key_act, (1, 0, 2))
     g = jnp.transpose(gate_act, (1, 0, 2))
     do = jnp.transpose(out_grad, (1, 0, 2))
-    flat = jnp.transpose(hidden_in, (1, 0, 2)).reshape(sequences * positions, width)
     bias = decay_bias.reshape(1, HEADS * DK)
 
     key_spec = pl.BlockSpec((2, BLK, pair * DK), lambda i: (0, 0, i))
     val_spec = pl.BlockSpec((2, BLK, pair * DV), lambda i: (0, 0, i))
     bias_spec = pl.BlockSpec((1, pair * DK), lambda i: (0, i))
     state_spec = pl.BlockSpec((2, pair, DV, DK), lambda i: (0, i, 0, 0))
+    score_spec = pl.BlockSpec((2, pair, BLK, BLK), lambda i: (0, i, 0, 0))
     key_shape = (sequences, positions, HEADS * DK)
-    val_shape = (sequences, positions, HEADS * DV)
+    val_shape = (sequences, positions, values)
     state_shape = (sequences, HEADS, DV, DK)
     mm = 2 * BLK * DK * DV * items
+    big = 2 * rows * width * values
 
     delta, cum = pl.pallas_call(
         functools.partial(decay_kernel, pair),
@@ -214,75 +231,96 @@
         name="decay",
     )(q, g, bias, do)
 
-    rx = lax.all_to_all(
-        delta.reshape(items, DV + EXTRA, DK), "sp", split_axis=0, concat_axis=0, tiled=True
-    )
-    dv_intra = pl.pallas_call(
+    rx = over_sp(delta.reshape(items, DV + EXTRA, DK))
+
+    k = jnp.transpose(key_act, (1, 0, 2))
+    scores, k_dec = pl.pallas_call(
         functools.partial(intra_kernel, pair),
         grid=(steps,),
-        in_specs=[key_spec, key_spec, key_spec, val_spec],
-        out_specs=val_spec,
-        out_shape=jax.ShapeDtypeStruct(val_shape, F32),
+        in_specs=[key_spec, key_spec, key_spec],
+        out_specs=[score_spec, key_spec],
+        out_shape=[
+            jax.ShapeDtypeStruct((sequences, HEADS, BLK, BLK), BF16),
+            jax.ShapeDtypeStruct(key_shape, BF16),
+        ],
         compiler_params=params(),
         cost_estimate=cost(3 * mm, 5 << 20),
         name="intra",
-    )(q, k, cum, do)
-
-    tails = lax.slice_in_dim(rx, DV, DV + EXTRA, axis=1)
+    )(q, k, cum)
+    turned = jnp.transpose(hidden_in, (2, 1, 0)).reshape(width, rows)
+    flat = jnp.transpose(hidden_in, (1, 0, 2)).reshape(rows, width)
+
+    cut = 4
+    band = DV // cut
 
     def scan(arrived, reverse):
         return pl.pallas_call(
             functools.partial(scan_kernel, blocks, reverse),
+            grid=(cut,),
+            in_specs=[
+                pl.BlockSpec((blocks, band, DK), lambda i: (0, i, 0)),
+                pl.BlockSpec((blocks, EXTRA, DK), lambda i: (0, DV // EXTRA, 0)),
+            ],
+            out_specs=pl.BlockSpec((blocks, band, DK), lambda i: (0, i, 0)),
             out_shape=jax.ShapeDtypeStruct((blocks, DV, DK), BF16),
+            compiler_params=params(),
             cost_estimate=cost(mm, 3 << 20),
             name="scan",
-        )(arrived, tails)
-
-    dstate = lax.all_to_all(scan(rx, True), "sp", split_axis=0, concat_axis=0, tiled=True)
-    dstate = dstate.reshape(state_shape)
-
-    dv = pl.pallas_call(
+        )(arrived, rx)
+
+    dstate = over_sp(scan(rx, True)).reshape(state_shape)
+    dstate, flat, turned = lax.optimization_barrier((dstate, flat, turned))
+
+    dv, partial = pl.pallas_call(
         functools.partial(value_grad_kernel, pair),
         grid=(steps,),
-        in_specs=[key_spec, key_spec, state_spec, val_spec],
-        out_specs=val_spec,
-        out_shape=jax.ShapeDtypeStruct(val_shape, BF16),
-        compiler_params=params(),
-        cost_estimate=cost(mm, 5 << 20),
+        in_specs=[
+            score_spec,
+            val_spec,
+            key_spec,
+            state_spec,
+            pl.BlockSpec((width, rows), lambda i: (0, 0)),
+        ],
+        out_specs=[
+            val_spec,
+            pl.BlockSpec(
+                (group, blocks // steps, width // group, values // blocks),
+                lambda i: (0, i, 0, 0),
+            ),
+        ],
+        out_shape=[
+            jax.ShapeDtypeStruct(val_shape, BF16),
+            jax.ShapeDtypeStruct((group, blocks, width // group, values // blocks), BF16),
+        ],
+        compiler_params=params(),
+        cost_estimate=cost(big + 2 * mm, 14 << 20),
         name="value_grad",
-    )(k, cum, dstate, dv_intra)
-    flat_dv = dv.reshape(sequences * positions, HEADS * DV)
-
-    partial = dot(flat, flat_dv, TN).astype(BF16)
+    )(scores, do, k_dec, dstate, turned)
+    flat_dv = dv.reshape(rows, values)
+
+    partial = partial.reshape(group * blocks, width // group, values // blocks)
     partial = lax.psum_scatter(partial, "dp", scatter_dimension=0, tiled=True)
 
     v, vdelta = pl.pallas_call(
-        project_kernel,
-        grid=(HEADS,),
+        functools.partial(project_kernel, pair),
+        grid=(steps,),
         in_specs=[
-            pl.BlockSpec((sequences * positions, width), lambda i: (0, 0)),
-            pl.BlockSpec((width, DV), lambda i: (0, i)),
-            pl.BlockSpec((2, BLK, DK), lambda i: (0, 0, i)),
-            pl.BlockSpec((2, BLK, DK), lambda i: (0, 0, i)),
-        ],
-        out_specs=[
-            pl.BlockSpec((2, BLK, DV), lambda i: (0, 0, i)),
-            pl.BlockSpec((2, 1, DV, DK), lambda i: (0, i, 0, 0)),
-        ],
+            pl.BlockSpec((rows, width), lambda i: (0, 0)),
+            pl.BlockSpec((width, pair * DV), lambda i: (0, i)),
+            key_spec,
+        ],
+        out_specs=[val_spec, state_spec],
         out_shape=[
             jax.ShapeDtypeStruct(val_shape, BF16),
             jax.ShapeDtypeStruct(state_shape, BF16),
         ],
         compiler_params=params(),
-        cost_estimate=cost(2 * 256 * width * HEADS * DV + mm, 12 << 20),
+        cost_estimate=cost(big + mm, 12 << 20),
         name="project",
-    )(flat, weight, k, cum)
-
-    vrx = lax.all_to_all(
-        vdelta.reshape(items, DV, DK), "sp", split_axis=0, concat_axis=0, tiled=True
-    )
-    state = lax.all_to_all(scan(vrx, False), "sp", split_axis=0, concat_axis=0, tiled=True)
-    state = state.reshape(state_shape)
+    )(flat, weight, k_dec)
+
+    vrx = over_sp(vdelta.reshape(items, DV, DK))
+    state = over_sp(scan(vrx, False)).reshape(state_shape)
 
     hidden_grad = dot(flat_dv, weight, NT).astype(BF16)
 
@@ -307,9 +345,7 @@
         name="final",
     )(q, k, g, bias, cum, do, v, state, dstate)
 
-    tiles = partial.reshape(partial.shape[0], blocks, -1).transpose(1, 0, 2)
-    tiles = lax.all_to_all(tiles, "sp", split_axis=0, concat_axis=0, tiled=True)
-    weight_grad = jnp.sum(tiles.astype(F32), axis=0)
+    weight_grad = jnp.sum(over_sp(partial).astype(F32), axis=0)
 
     def back(value):
         return jnp.transpose(value.reshape(sequences, positions, -1), (1, 0, 2))
@@ -319,7 +355,7 @@
 
 def solution(mesh):
     return jax.shard_map(
-        local,
+        arranged,
         mesh=mesh,
         in_specs=(
             P("sp", "dp", None),

time: 171 us -> 167 us (0.977)
  matrix products: 12.7 us -> 5.74 us
  waiting for transfers between devices: 8.47 us -> 5.11 us
  starting transfers between devices: 10.1 us -> 12.5 us
  local copies, waits for them, and re-layouts: 19.3 us -> 21.7 us
    dot_general x2 -> x1, matrix products: 12.7 us -> 5.74 us  [dot(): return lax.dot_general(a, b, dims, preferred_element_type=F32)]
    all_to_all x2, waiting for transfers between devices: 7.77 us -> 4.39 us  [over_sp(): return lax.all_to_all(value, 'sp', split_axis=0, concat_axis=0, tiled=True)]
    transpose x2 -> x3, local copies, waits for them, and re-layouts: 3.8 us -> 6.91 us  [the longest x1 3.11 us: arranged(): turned = jnp.transpose(hidden_in, (2, 1, 0)).reshape(width, rows)]
    all_to_all x2, starting transfers between devices: 10.1 us -> 12.4 us  [over_sp(): return lax.all_to_all(value, 'sp', split_axis=0, concat_axis=0, tiled=True)]
    unnamed x16 -> x14, local copies, waits for them, and re-layouts: 12.8 us -> 12.7 us
  transfers between devices with their start and end apart: 4 -> 4, of which waited for: 1 -> 1; matrix products, arithmetic and copies ran while one was open for 18% -> 16% of each run, Pallas kernels for 24% -> 25%
where the time goes in v1:
time: 167 us; the launch traced here: 166 us
  blocking collectives  64.2 us (38%)
  Pallas kernels  41.9 us (25%)
  local copies, waits for them, and re-layouts  21.7 us (13%)
  between operations  14.1 us (8%)
  starting transfers between devices  12.5 us (7%)
  matrix products  5.74 us (3%)
  waiting for transfers between devices  5.11 us (3%)
    all_to_all x3, blocking collectives, over_sp(): return lax.all_to_all(value, 'sp', split_axis=0, concat_axis=0, tiled=True)  64.2 us
    unnamed x14, local copies, waits for them, and re-layouts  12.7 us
    all_to_all x2, starting transfers between devices, over_sp(): return lax.all_to_all(value, 'sp', split_axis=0, concat_axis=0, tiled=True)  12.4 us
    pallas_call x1, Pallas kernels, arranged(): pl.pallas_call(functools.partial(final_kernel, pair), grid=(steps,), in_s...  9.87 us
    pallas_call x1, Pallas kernels, arranged(): pl.pallas_call(functools.partial(project_kernel, pair), grid=(steps,), in...  8.06 us
    pallas_call x1, Pallas kernels, arranged(): pl.pallas_call(functools.partial(value_grad_kernel, pair), grid=(steps,),...  7.87 us
    pallas_call x2, Pallas kernels, scan(): pl.pallas_call(functools.partial(scan_kernel, blocks, reverse), grid=(cut...  7.1 us
    dot_general x1, matrix products, dot(): return lax.dot_general(a, b, dims, preferred_element_type=F32)  5.74 us
  transfers between devices with their start and end apart: 4, of which 1 were waited for; matrix products, arithmetic and copies ran while one was open for 16% of the time, Pallas kernels for 25%

profile of v1, /device:TPU:8, one launch (start us, length us, event | category | flops | bytes accessed | tf_op | source)
XLA Modules:
  0.0 166.0 jit_solution(17352277739782051436)
XLA Ops:
  7.2 0.0 copy-start.2
  7.2 0.0 copy-start
  7.2 0.0 all-gather.2.cloned.1.call-start
  7.2 0.7 all-gather.2.cloned.1.call-update
  7.9 2.6 %copy.31 = bf16[128,2,2048]{2,0,1:T(8,128)(2,1)} copy(bf16[128,2,2048]{2,1,0:T(2,128)(2,1)} %param.13) | data formatting | bytes 2097152 | tf_op args[6]
  10.5 2.4 %copy_bitcast_fusion.3 = (bf16[2,128,1024]{2,1,0:T(8,128)(2,1)}, bf16[2,128,1024]{2,1,0:T(8,128)(2,1)}) fusion(bf16[128,2,1024]{2,1,0:T(2,128)(2,1)} %param.10, bf16[128,2,1024]{2,1,0:T(2,128)(2,1)} %param.8), kind=kLoop, calls=%fused_computation.5 | loop fusion | bytes 2097152 | tf_op jit(solution)/shard_map/transpose | solution.py:202
  12.9 4.9 %decay.1 = (bf16[2,8,272,128]{3,2,1,0:T(8,128)(2,1)}, f32[2,128,1024]{2,1,0:T(8,128)}) custom-call(bf16[2,128,1024]{2,1,0:T(8,128)(2,1)} %get-tuple-element.39.q_ref, bf16[2,128,1024]{2,1,0:T(8,128)(2,1)} %get-tuple-element.38.g_ref, f32[1,1024]{1,0:T(1,128)} %bitcast.54, bf16[2,128,2048]{2,1,0:T(8,128)(2,1)} %bitcast.33), custom_call_target="tpu_custom_call" | custom-call | flops 402653184 | bytes 5242880 | tf_op jit(solution)/shard_map/decay/pallas_call | solution.py:217
  17.8 25.0 %all_to_all.25.rx_ref.last_ref = bf16[16,272,128]{2,1,0:T(8,128)(2,1)} all-to-all(bf16[16,272,128]{2,1,0:T(8,128)(2,1)} %bitcast.46), channel_id=1, replica_groups=mesh['sp'=16,'dp'=8] {'sp'}, dimensions={0} | all-to-all | bytes 2228224 | tf_op jit(solution)/shard_map/all_to_all | solution.py:187
  42.8 3.5 %scan.2 = bf16[16,256,128]{2,1,0:T(8,128)(2,1)} custom-call(bf16[16,272,128]{2,1,0:T(8,128)(2,1)} %all_to_all.25.rx_ref.last_ref, bf16[16,272,128]{2,1,0:T(8,128)(2,1)} %all_to_all.25.rx_ref.last_ref), custom_call_target="tpu_custom_call" | custom-call | flops 134217728 | bytes 3145728 | tf_op jit(solution)/shard_map/scan/pallas_call | solution.py:257
  46.3 5.0 %all-to-all-start.1 = ((bf16[16,256,128]{2,1,0:T(8,128)(2,1)}), bf16[16,256,128]{2,1,0:T(8,128)(2,1)S(1)}, u32[]{:S(2)}, u32[]{:S(2)}) async-start(bf16[16,256,128]{2,1,0:T(8,128)(2,1)} %scan.2), calls=%async_computation.1 | async-start | bytes 2097152 | tf_op jit(solution)/shard_map/all_to_all | solution.py:187
  51.3 0.0 reduce-scatter.2.cloned.1.call-start
  51.3 0.0 copy-done.2
  51.3 0.9 copy.32
  52.3 0.0 copy-done
  52.3 1.3 copy.16
  53.6 3.1 %copy.17 = bf16[2048,2,128]{2,1,0:T(2,128)(2,1)S(1)} copy(bf16[2048,2,128]{0,1,2:T(2,128)(2,1)S(1)} %bitcast.41) | data formatting | bytes 2097152 | tf_op jit(solution)/shard_map/transpose | solution.py:250
  56.7 1.1 copy.29
  57.9 4.2 %intra.1 = (bf16[2,8,128,128]{3,2,1,0:T(8,128)(2,1)}, bf16[2,128,1024]{2,1,0:T(8,128)(2,1)}) custom-call(bf16[2,128,1024]{2,1,0:T(8,128)(2,1)} %get-tuple-element.39.q_ref, bf16[2,128,1024]{2,1,0:T(8,128)(2,1)} %bitcast.37, f32[2,128,1024]{2,1,0:T(8,128)} %get-tuple-element.19.cum_ref), custom_call_target="tpu_custom_call" | custom-call | flops 402653184 | bytes 5242880 | tf_op jit(solution)/shard_map/intra/pallas_call | solution.py:237
  62.1 4.4 %all-to-all-done.1 = bf16[16,256,128]{2,1,0:T(8,128)(2,1)S(1)} async-done(((bf16[16,256,128]{2,1,0:T(8,128)(2,1)}), bf16[16,256,128]{2,1,0:T(8,128)(2,1)S(1)}, u32[]{:S(2)}, u32[]{:S(2)}) %all-to-all-start.1) | async-done | bytes 1048608 | tf_op jit(solution)/shard_map/all_to_all | solution.py:187
  66.4 0.0 copy-start.1
  66.4 1.0 copy-done.1
  67.4 7.9 %value_grad.1 = (bf16[2,128,2048]{2,1,0:T(8,128)(2,1)}, bf16[8,16,256,128]{3,2,1,0:T(8,128)(2,1)}) custom-call(bf16[2,8,128,128]{3,2,1,0:T(8,128)(2,1)} %get-tuple-element.20.scores_ref, bf16[2,128,2048]{2,1,0:T(8,128)(2,1)} %bitcast.34, bf16[2,128,1024]{2,1,0:T(8,128)(2,1)} %get-tuple-element.21.k_dec_ref, bf16[2,8,256,128]{3,2,1,0:T(8,128)(2,1)} %bitcast.43, ...), custom_call_target="tpu_custom_call" | custom-call | flops 2415919104 | bytes 14680064 | tf_op jit(solution)/shard_map/value_grad/pallas_call | solution.py:274
  75.3 0.0 reduce-scatter.2.cloned.1.call-update
  75.3 0.0 copy-start.3
  75.3 0.0 all-gather.2.cloned.1.call-done.w_ref
  75.4 8.1 %project.1 = (bf16[2,128,2048]{2,1,0:T(8,128)(2,1)}, bf16[2,8,256,128]{3,2,1,0:T(8,128)(2,1)}) custom-call(bf16[256,2048]{1,0:T(8,128)(2,1)} %bitcast.39, bf16[2048,2048]{1,0:T(8,128)(2,1)} %all-gather.2.cloned.1.call-done.w_ref, bf16[2,128,1024]{2,1,0:T(8,128)(2,1)} %get-tuple-element.21.k_dec_ref), custom_call_target="tpu_custom_call" | custom-call | flops 2281701376 | bytes 12582912 | tf_op jit(solution)/shard_map/project/pallas_call | solution.py:304
  83.4 20.1 %all_to_all.26.rx_ref = bf16[16,256,128]{2,1,0:T(8,128)(2,1)} all-to-all(bf16[16,256,128]{2,1,0:T(8,128)(2,1)} %bitcast.49), channel_id=1, replica_groups=mesh['sp'=16,'dp'=8] {'sp'}, dimensions={0} | all-to-all | bytes 2097152 | tf_op jit(solution)/shard_map/all_to_all | solution.py:187
  103.5 3.6 %scan.3 = bf16[16,256,128]{2,1,0:T(8,128)(2,1)} custom-call(bf16[16,256,128]{2,1,0:T(8,128)(2,1)} %all_to_all.26.rx_ref, bf16[16,272,128]{2,1,0:T(8,128)(2,1)} %all_to_all.25.rx_ref.last_ref), custom_call_target="tpu_custom_call" | custom-call | flops 134217728 | bytes 3145728 | tf_op jit(solution)/shard_map/scan/pallas_call | solution.py:257
  107.1 19.1 %all_to_all.27 = bf16[16,256,128]{2,1,0:T(8,128)(2,1)} all-to-all(bf16[16,256,128]{2,1,0:T(8,128)(2,1)} %scan.3), channel_id=1, replica_groups=mesh['sp'=16,'dp'=8] {'sp'}, dimensions={0} | all-to-all | bytes 2097152 | tf_op jit(solution)/shard_map/all_to_all | solution.py:187
  126.2 0.0 reduce-scatter.2.cloned.1.call-done
  126.2 7.4 %all-to-all-start.4 = ((bf16[16,256,128]{2,1,0:T(8,128)(2,1)}), bf16[16,256,128]{2,1,0:T(8,128)(2,1)S(1)}, u32[]{:S(2)}, u32[]{:S(2)}) async-start(bf16[16,256,128]{2,1,0:T(8,128)(2,1)} %reduce-scatter.2.cloned.1.call-done), calls=%async_computation.5 | async-start | bytes 2097152 | tf_op jit(solution)/shard_map/all_to_all | solution.py:187
  133.6 0.0 copy-done.3
  133.6 5.7 %convolution_convert_fusion = bf16[256,2048]{1,0:T(8,128)(2,1)S(1)} fusion(bf16[256,2048]{1,0:T(8,128)(2,1)S(1)} %bitcast.56, bf16[2048,2048]{1,0:T(8,128)(2,1)} %all-gather.2.cloned.1.call-done.w_ref), kind=kOutput, calls=%fused_computation | convolution fusion | flops 2148007936 | bytes 10485760 | tf_op jit(solution)/shard_map/dot_general | solution.py:26
  139.3 2.0 %copy.30 = bf16[2,128,2048]{2,0,1:T(2,128)(2,1)} copy(bf16[2,128,2048]{2,1,0:T(8,128)(2,1)S(1)} %bitcast.50) | data formatting | bytes 2097152 | tf_op jit(solution)/shard_map/reshape | solution.py:351
  141.4 9.9 %final.1 = (bf16[2,128,1024]{2,1,0:T(8,128)(2,1)}, bf16[2,128,1024]{2,1,0:T(8,128)(2,1)}, bf16[2,128,1024]{2,1,0:T(8,128)(2,1)}) custom-call(bf16[2,128,1024]{2,1,0:T(8,128)(2,1)} %get-tuple-element.39.q_ref, bf16[2,128,1024]{2,1,0:T(8,128)(2,1)} %bitcast.38, bf16[2,128,1024]{2,1,0:T(8,128)(2,1)} %get-tuple-element.38.g_ref, f32[1,1024]{1,0:T(1,128)} %bitcast.55, ...), custom_call_target="tpu_custom_call" | custom-call | flops 805306368 | bytes 10485760 | tf_op jit(solution)/shard_map/final/pallas_call | solution.py:327
  151.3 2.4 %copy.19 = bf16[128,2,1024]{2,1,0:T(2,128)(2,1)} copy(bf16[128,2,1024]{2,0,1:T(8,128)(2,1)} %bitcast.53) | data formatting | bytes 1048576
  153.6 2.4 %copy.20 = bf16[128,2,1024]{2,1,0:T(2,128)(2,1)} copy(bf16[128,2,1024]{2,0,1:T(8,128)(2,1)} %bitcast.52) | data formatting | bytes 1048576
  156.0 2.4 %copy.21 = bf16[128,2,1024]{2,1,0:T(2,128)(2,1)} copy(bf16[128,2,1024]{2,0,1:T(8,128)(2,1)} %bitcast.51) | data formatting | bytes 1048576
  158.4 0.0 all-to-all-done.4
  158.4 0.8 convert_reduce_fusion
Async XLA Ops:
  7.2 44.2 %copy-start.2 = (bf16[128,2,1024]{2,1,0:T(2,128)(2,1)S(1)}, bf16[128,2,1024]{2,1,0:T(2,128)(2,1)}, u32[]{:S(2)}) copy-start(bf16[128,2,1024]{2,1,0:T(2,128)(2,1)} %param.9) | copy-start | bytes 1572868
  7.2 45.1 %copy-start = (bf16[128,2,2048]{2,1,0:T(2,128)(2,1)S(1)}, bf16[128,2,2048]{2,1,0:T(2,128)(2,1)}, u32[]{:S(2)}) copy-start(bf16[128,2,2048]{2,1,0:T(2,128)(2,1)} %param.7) | copy-start | bytes 3145732
  7.2 68.2 %all-gather.2.cloned.1.call-start = ((), (), s32[]{:S(2)}) async-start(), calls=%async_computation.6 | async-start | bytes 9437184 | tf_op jit(solution)/shard_map/all_gather | solution.py:194
  46.3 20.1 %all-to-all-start.1 = ((bf16[16,256,128]{2,1,0:T(8,128)(2,1)}), bf16[16,256,128]{2,1,0:T(8,128)(2,1)S(1)}, u32[]{:S(2)}, u32[]{:S(2)}) async-start(bf16[16,256,128]{2,1,0:T(8,128)(2,1)} %scan.2), calls=%async_computation.1 | async-start | bytes 2097152 | tf_op jit(solution)/shard_map/all_to_all | solution.py:187
  51.3 74.9 %reduce-scatter.2.cloned.1.call-start = ((), (), s32[]{:S(2)}) async-start(), calls=%async_computation.7 | async-start | bytes 9437184 | tf_op jit(solution)/shard_map/reduce_scatter | solution.py:302
  66.4 1.0 copy-start.1
  75.3 58.3 %copy-start.3 = (bf16[2,128,2048]{2,1,0:T(8,128)(2,1)S(1)}, bf16[2,128,2048]{2,1,0:T(8,128)(2,1)}, u32[]{:S(2)}) copy-start(bf16[2,128,2048]{2,1,0:T(8,128)(2,1)} %get-tuple-element.25) | copy-start | bytes 3145732
  126.2 32.2 %all-to-all-start.4 = ((bf16[16,256,128]{2,1,0:T(8,128)(2,1)}), bf16[16,256,128]{2,1,0:T(8,128)(2,1)S(1)}, u32[]{:S(2)}, u32[]{:S(2)}) async-start(bf16[16,256,128]{2,1,0:T(8,128)(2,1)} %reduce-scatter.2.cloned.1.call-done), calls=%async_computation.5 | async-start | bytes 2097152 | tf_op jit(solution)/shard_map/all_to_all | solution.py:187
Sparse Core Ops, SparseCore 0:
  9.7 51.8 all-gather.1
  75.4 50.6 reduce-scatter.1

commit v2 on v1

v2 whole, which is shorter than its diff:
```python
import functools

import jax
import jax.numpy as jnp
from jax import lax
from jax.experimental import pallas as pl
from jax.experimental.pallas import tpu as pltpu
from jax.sharding import PartitionSpec as P

HEADS = 8
DK = 128
DV = 256
BLK = 128
SEQS = 2
ROWS = SEQS * BLK
EXTRA = 16
SOFTNESS = 16.0
SCALE = DK**-0.5
PAIR = 4
STEPS = HEADS // PAIR
F32 = jnp.float32
BF16 = jnp.bfloat16

NN = (((1,), (0,)), ((), ()))
NT = (((1,), (1,)), ((), ()))
TN = (((0,), (0,)), ((), ()))


def dot(a, b, dims):
    return lax.dot_general(a, b, dims, preferred_element_type=F32)


def split2(x):
    hi = x.astype(BF16)
    lo = (x - hi.astype(F32)).astype(BF16)
    return hi, lo


def iota_pair(shape):
    return (
        lax.broadcasted_iota(jnp.int32, shape, 0),
        lax.broadcasted_iota(jnp.int32, shape, 1),
    )


def causal():
    row, col = iota_pair((ROWS, ROWS))
    return (row >= col) & (((row - col) & 1) == 0)


def first_rows(width):
    return (lax.broadcasted_iota(jnp.int32, (ROWS, width), 0) & 1) == 0


def halves(x, first):
    zero = jnp.zeros_like(x)
    return jnp.concatenate([jnp.where(first, x, zero), jnp.where(first, zero, x)], axis=1)


def chosen(x, first):
    return jnp.where(first, x[:, :DK], x[:, DK:])


def last_of(cum, first):
    return jnp.where(first, cum[ROWS - 2 : ROWS - 1], cum[ROWS - 1 : ROWS])


def native(ref, cols):
    return ref[:, :, cols].reshape(ROWS, cols.stop - cols.start)


def head_slices(j):
    return slice(j * DK, (j + 1) * DK), slice(j * DV, (j + 1) * DV)


def cost(flops, moved):
    return pl.CostEstimate(flops=flops, bytes_accessed=moved, transcendentals=0)


def params():
    return pltpu.CompilerParams(dimension_semantics=("arbitrary",))


def decay_kernel(q_ref, g_ref, bias_ref, do_ref, delta_ref, cum_ref, q_dec_ref):
    lower = causal().astype(BF16)
    first = first_rows(DK)
    for j in range(PAIR):
        keys, vals = head_slices(j)
        x = native(g_ref, keys).astype(F32) + bias_ref[:, keys]
        log_decay = (jnp.minimum(x, 0.0) - jnp.log(1.0 + jnp.exp(-jnp.abs(x)))) / SOFTNESS
        sums = dot(lower, jnp.concatenate(split2(log_decay), axis=1), NN)
        cum = sums[:, :DK] + sums[:, DK:]
        cum_ref[:, keys] = cum
        q_dec = (native(q_ref, keys).astype(F32) * SCALE * jnp.exp(cum)).astype(BF16)
        q_dec_ref[:, keys] = q_dec
        delta = dot(native(do_ref, vals), halves(q_dec, first), TN)
        for s in range(SEQS):
            delta_ref[s, j, :DV, :] = delta[:, s * DK : (s + 1) * DK].astype(BF16)
            last = cum[ROWS - SEQS + s : ROWS - SEQS + s + 1]
            one, two = split2(last)
            three = last - one.astype(F32) - two.astype(F32)
            rows = lax.broadcasted_iota(jnp.int32, (EXTRA, DK), 0)
            tail = jnp.where(
                rows == 0, one.astype(F32), jnp.where(rows == 1, two.astype(F32), three)
            )
            delta_ref[s, j, DV:, :] = tail.astype(BF16)


def intra_kernel(k_ref, cum_ref, q_dec_ref, scores_ref, k_dec_ref):
    keep = causal()
    first = first_rows(DK)
    for j in range(PAIR):
        keys, _ = head_slices(j)
        cum = cum_ref[:, keys]
        k = native(k_ref, keys).astype(F32)
        k_inv = (k * jnp.exp(-cum)).astype(BF16)
        scores = dot(q_dec_ref[:, keys], k_inv, NT)
        scores_ref[j] = jnp.where(keep, scores, 0.0).astype(BF16)
        k_dec_ref[:, keys] = (k * jnp.exp(last_of(cum, first) - cum)).astype(BF16)


def scan_kernel(blocks, reverse, rx_ref, last_ref, out_ref):
    state = jnp.zeros((DV, DK), F32)
    order = range(blocks - 1, -1, -1) if reverse else range(blocks)
    for b in order:
        out_ref[b] = state.astype(BF16)
        tail = last_ref[b, DV:, :].astype(F32)
        decay = jnp.exp(tail[0:1] + tail[1:2] + tail[2:3])
        state = state * decay + rx_ref[b, :DV, :].astype(F32)


def value_grad_kernel(
    scores_ref, do_ref, k_dec_ref, dstate_ref, h_ref, dv_ref, part_ref
):
    first = first_rows(DK)
    heads = []
    for j in range(PAIR):
        keys, vals = head_slices(j)
        intra = dot(scores_ref[j], native(do_ref, vals), TN)
        dstate = jnp.concatenate([dstate_ref[0, j], dstate_ref[1, j]], axis=1)
        inter = dot(halves(k_dec_ref[:, keys], first), dstate, NT)
        dv = (intra + inter).astype(BF16)
        dv_ref[:, vals] = dv
        heads.append(dv)
    dv_all = jnp.concatenate(heads, axis=1)
    group, tiles, height, span = part_ref.shape
    for m in range(group):
        hidden = native(h_ref, slice(m * height, (m + 1) * height))
        part = dot(hidden, dv_all, TN).astype(BF16)
        for t in range(tiles):
            part_ref[m, t] = part[:, t * span : (t + 1) * span]


def project_kernel(h_ref, w_ref, k_dec_ref, v_ref, delta_ref):
    first = first_rows(DK)
    hidden = native(h_ref, slice(0, h_ref.shape[2]))
    v_all = dot(hidden, w_ref[...], NN).astype(BF16)
    v_ref[...] = v_all
    for j in range(PAIR):
        keys, vals = head_slices(j)
        delta = dot(v_all[:, vals], halves(k_dec_ref[:, keys], first), TN)
        for s in range(SEQS):
            delta_ref[s, j] = delta[:, s * DK : (s + 1) * DK].astype(BF16)


def hidden_grad_kernel(dv_ref, w_ref, out_ref):
    grad = dot(dv_ref[...], w_ref[...], NT).astype(BF16)
    out_ref[...] = grad.reshape(out_ref.shape)


def final_kernel(
    k_ref,
    g_ref,
    bias_ref,
    cum_ref,
    q_dec_ref,
    do_ref,
    v_ref,
    state_ref,
    dstate_ref,
    dq_ref,
    dk_ref,
    dg_ref,
):
    keep = causal()
    first = first_rows(DK)
    row, col = iota_pair((ROWS, ROWS))
    same = ((row - col) & 1) == 0
    sums = jnp.concatenate(
        [(same & (col >= row)).astype(BF16), (same & (col < row)).astype(BF16)], axis=1
    )
    for j in range(PAIR):
        keys, vals = head_slices(j)
        cum = cum_ref[:, keys]
        last = last_of(cum, first)
        q_scale = SCALE * jnp.exp(cum)
        inv_scale = jnp.exp(-cum)
        dec_scale = jnp.exp(last - cum)
        k = native(k_ref, keys).astype(F32)
        q_dec = q_dec_ref[:, keys]
        k_inv = (k * inv_scale).astype(BF16)
        k_dec = (k * dec_scale).astype(BF16)
        do = native(do_ref, vals)
        v = v_ref[:, vals]
        state = jnp.concatenate([state_ref[0, j], state_ref[1, j]], axis=1)
        dstate = jnp.concatenate([dstate_ref[0, j], dstate_ref[1, j]], axis=1)
        dscores = jnp.where(keep, dot(do, v, NT), 0.0).astype(BF16)
        dq_dec = dot(dscores, k_inv, NN) + chosen(dot(do, state, NN), first)
        dk_inv = dot(dscores, q_dec, TN)
        dk_dec = chosen(dot(v, dstate, NN), first)
        dq_ref[:, :, keys] = (q_scale * dq_dec).astype(BF16).reshape(BLK, SEQS, DK)
        dk = (inv_scale * dk_inv + dec_scale * dk_dec).astype(BF16)
        dk_ref[:, :, keys] = dk.reshape(BLK, SEQS, DK)
        after = q_dec.astype(F32) * dq_dec - k_inv.astype(F32) * dk_inv
        before = k_dec.astype(F32) * dk_dec
        terms = jnp.concatenate([after, before], axis=0)
        dlog = dot(sums, jnp.concatenate(split2(terms), axis=1), NN)
        through = jnp.sum(state.astype(F32) * dstate.astype(F32), axis=0, keepdims=True)
        through = jnp.where(first, through[:, :DK], through[:, DK:])
        dlog = dlog[:, :DK] + dlog[:, DK:] + jnp.exp(last) * through
        x = native(g_ref, keys).astype(F32) + bias_ref[:, keys]
        slope = (1.0 / SOFTNESS) / (1.0 + jnp.exp(x))
        dg_ref[:, :, keys] = (dlog * slope).astype(BF16).reshape(BLK, SEQS, DK)


def over_sp(value):
    return lax.all_to_all(value, "sp", split_axis=0, concat_axis=0, tiled=True)


def shaped(shape, dtype=BF16):
    return jax.ShapeDtypeStruct(shape, dtype)


def arranged(hidden_in, query_act, key_act, gate_act, decay_bias, value_weight, out_grad):
    _, sequences, width = hidden_in.shape
    blocks = lax.axis_size("sp")
    group = lax.axis_size("dp")
    weight = lax.all_gather(value_weight, "dp", axis=0, tiled=True)
    items = sequences * HEADS
    values = HEADS * DV
    bias = decay_bias.reshape(1, HEADS * DK)

    raw_key = pl.BlockSpec((BLK, SEQS, PAIR * DK), lambda i: (0, 0, i))
    raw_val = pl.BlockSpec((BLK, SEQS, PAIR * DV), lambda i: (0, 0, i))
    bias_spec = pl.BlockSpec((1, PAIR * DK), lambda i: (0, i))
    key_spec = pl.BlockSpec((ROWS, PAIR * DK), lambda i: (0, i))
    val_spec = pl.BlockSpec((ROWS, PAIR * DV), lambda i: (0, i))
    state_spec = pl.BlockSpec((SEQS, PAIR, DV, DK), lambda i: (0, i, 0, 0))
    score_spec = pl.BlockSpec((PAIR, ROWS, ROWS), lambda i: (i, 0, 0))
    raw_key_shape = (BLK, SEQS, HEADS * DK)
    key_shape = (ROWS, HEADS * DK)
    val_shape = (ROWS, values)
    state_shape = (SEQS, HEADS, DV, DK)
    mm = 2 * BLK * DK * DV * items
    big = 2 * ROWS * width * values

    delta, cum, q_dec = pl.pallas_call(
        decay_kernel,
        grid=(STEPS,),
        in_specs=[raw_key, raw_key, bias_spec, raw_val],
        out_specs=[
            pl.BlockSpec((SEQS, PAIR, DV + EXTRA, DK), lambda i: (0, i, 0, 0)),
            key_spec,
            key_spec,
        ],
        out_shape=[
            shaped((SEQS, HEADS, DV + EXTRA, DK)),
            shaped(key_shape, F32),
            shaped(key_shape),
        ],
        compiler_params=params(),
        cost_estimate=cost(3 * mm, 5 << 20),
        name="decay",
    )(query_act, gate_act, bias, out_grad)

    rx = over_sp(delta.reshape(items, DV + EXTRA, DK))

    scores, k_dec = pl.pallas_call(
        intra_kernel,
        grid=(STEPS,),
        in_specs=[raw_key, key_spec, key_spec],
        out_specs=[score_spec, key_spec],
        out_shape=[shaped((HEADS, ROWS, ROWS)), shaped(key_shape)],
        compiler_params=params(),
        cost_estimate=cost(3 * mm, 5 << 20),
        name="intra",
    )(key_act, cum, q_dec)

    def scan(arrived, reverse):
        return pl.pallas_call(
            functools.partial(scan_kernel, blocks, reverse),
            out_shape=shaped((blocks, DV, DK)),
            compiler_params=pltpu.CompilerParams(vmem_limit_bytes=12 << 20),
            cost_estimate=cost(mm, 3 << 20),
            name="scan",
        )(arrived, rx)

    dstate = over_sp(scan(rx, True)).reshape(state_shape)

    dv, partial = pl.pallas_call(
        value_grad_kernel,
        grid=(STEPS,),
        in_specs=[
            score_spec,
            raw_val,
            key_spec,
            state_spec,
            pl.BlockSpec((BLK, SEQS, width), lambda i: (0, 0, 0)),
        ],
        out_specs=[
            val_spec,
            pl.BlockSpec(
                (group, blocks // STEPS, width // group, values // blocks),
                lambda i: (0, i, 0, 0),
            ),
        ],
        out_shape=[
            shaped(val_shape),
            shaped((group, blocks, width // group, values // blocks)),
        ],
        compiler_params=params(),
        cost_estimate=cost(big + 2 * mm, 14 << 20),
        name="value_grad",
    )(scores, out_grad, k_dec, dstate, hidden_in)

    partial = partial.reshape(group * blocks, width // group, values // blocks)
    partial = lax.psum_scatter(partial, "dp", scatter_dimension=0, tiled=True)

    v, vdelta = pl.pallas_call(
        project_kernel,
        grid=(STEPS,),
        in_specs=[
            pl.BlockSpec((BLK, SEQS, width), lambda i: (0, 0, 0)),
            pl.BlockSpec((width, PAIR * DV), lambda i: (0, i)),
            key_spec,
        ],
        out_specs=[val_spec, state_spec],
        out_shape=[shaped(val_shape), shaped(state_shape)],
        compiler_params=params(),
        cost_estimate=cost(big + mm, 12 << 20),
        name="project",
    )(hidden_in, weight, k_dec)

    vrx = over_sp(vdelta.reshape(items, DV, DK))
    state = over_sp(scan(vrx, False)).reshape(state_shape)

    hidden_grad = pl.pallas_call(
        hidden_grad_kernel,
        grid=(4,),
        in_specs=[
            pl.BlockSpec(val_shape, lambda i: (0, 0)),
            pl.BlockSpec((width // 4, values), lambda i: (i, 0)),
        ],
        out_specs=pl.BlockSpec((BLK, SEQS, width // 4), lambda i: (0, 0, i)),
        out_shape=shaped((BLK, SEQS, width)),
        compiler_params=params(),
        cost_estimate=cost(big, 10 << 20),
        name="hidden_grad",
    )(dv, weight)

    dq, dk, dg = pl.pallas_call(
        final_kernel,
        grid=(STEPS,),
        in_specs=[
            raw_key,
            raw_key,
            bias_spec,
            key_spec,
            key_spec,
            raw_val,
            val_spec,
            state_spec,
            state_spec,
        ],
        out_specs=[raw_key, raw_key, raw_key],
        out_shape=[shaped(raw_key_shape)] * 3,
        compiler_params=params(),
        cost_estimate=cost(6 * mm, 10 << 20),
        name="final",
    )(key_act, gate_act, bias, cum, q_dec, out_grad, v, state, dstate)

    weight_grad = jnp.sum(over_sp(partial).astype(F32), axis=0)
    return (hidden_grad, dq, dk, dg, weight_grad)


def solution(mesh):
    rows = P("sp", "dp", None)
    return jax.shard_map(
        arranged,
        mesh=mesh,
        in_specs=(rows, rows, rows, rows, P(), P("dp", None), rows),
        out_specs=(rows, rows, rows, rows, P("dp", "sp")),
        check_vma=False,
    )
```

time: 167 us -> 154 us (0.922)
  the two profiles are of different devices: /device:TPU:8 before, /device:TPU:3 now
where the time goes in v2:
time: 154 us
  blocking collectives  63.1 us (41%)
  Pallas kernels  41.5 us (27%)
  waiting for transfers between devices  22.8 us (15%)
  between operations  14.1 us (9%)
  starting transfers between devices  10.4 us (7%)
    all_to_all x3, blocking collectives, over_sp(): return lax.all_to_all(value, 'sp', split_axis=0, concat_axis=0, tiled=True)  63.1 us
    all_to_all x2, waiting for transfers between devices, over_sp(): return lax.all_to_all(value, 'sp', split_axis=0, concat_axis=0, tiled=True)  15.6 us
    all_to_all x2, starting transfers between devices, over_sp(): return lax.all_to_all(value, 'sp', split_axis=0, concat_axis=0, tiled=True)  10.4 us
    pallas_call x1, Pallas kernels, arranged(): pl.pallas_call(final_kernel, grid=(STEPS,), in_specs=[raw_key, raw_key, b...  8.82 us
    pallas_call x1, Pallas kernels, arranged(): pl.pallas_call(value_grad_kernel, grid=(STEPS,), in_specs=[score_spec, ra...  7.23 us
    pallas_call x1, Pallas kernels, arranged(): pl.pallas_call(hidden_grad_kernel, grid=(4,), in_specs=[pl.BlockSpec(val_...  6.68 us
    pallas_call x1, Pallas kernels, arranged(): pl.pallas_call(decay_kernel, grid=(STEPS,), in_specs=[raw_key, raw_key, b...  6.63 us
    pallas_call x1, Pallas kernels, arranged(): pl.pallas_call(project_kernel, grid=(STEPS,), in_specs=[pl.BlockSpec((BLK...  6.48 us
  transfers between devices with their start and end apart: 4, of which 3 were waited for; matrix products, arithmetic and copies ran while one was open for 0% of the time, Pallas kernels for 27%

profile of v2, /device:TPU:3, one launch (start us, length us, event | category | flops | bytes accessed | tf_op | source)
XLA Modules:
  0.0 153.7 jit_solution(11175163526220507117)
XLA Ops:
  7.2 0.0 all-gather.2.cloned.1.call-start
  7.2 0.7 all-gather.2.cloned.1.call-update
  7.9 6.6 %decay.1 = (bf16[2,8,272,128]{3,2,1,0:T(8,128)(2,1)}, f32[256,1024]{1,0:T(8,128)}, bf16[256,1024]{1,0:T(8,128)(2,1)}) custom-call(bf16[128,2,1024]{2,1,0:T(2,128)(2,1)} %q_ref.1, bf16[128,2,1024]{2,1,0:T(2,128)(2,1)} %g_ref.3, f32[1,1024]{1,0:T(1,128)} %bitcast.12, bf16[128,2,2048]{2,1,0:T(2,128)(2,1)} %do_ref.5), custom_call_target="tpu_custom_call" | custom-call | flops 402653184 | bytes 5242880 | tf_op jit(solution)/shard_map/decay/pallas_call | solution.py:257
  14.5 24.7 %all_to_all.25.rx_ref.last_ref = bf16[16,272,128]{2,1,0:T(8,128)(2,1)S(1)} all-to-all(bf16[16,272,128]{2,1,0:T(8,128)(2,1)} %bitcast.10), channel_id=1, replica_groups=mesh['sp'=16,'dp'=8] {'sp'}, dimensions={0} | all-to-all | bytes 2228224 | tf_op jit(solution)/shard_map/all_to_all | solution.py:227
  39.2 1.4 scan.2
  40.6 3.7 %all-to-all-start.1 = ((bf16[16,256,128]{2,1,0:T(8,128)(2,1)}), bf16[16,256,128]{2,1,0:T(8,128)(2,1)S(1)}, u32[]{:S(2)}, u32[]{:S(2)}) async-start(bf16[16,256,128]{2,1,0:T(8,128)(2,1)} %scan.2), calls=%async_computation.1 | async-start | bytes 2097152 | tf_op jit(solution)/shard_map/all_to_all | solution.py:227
  44.3 0.0 reduce-scatter.2.cloned.1.call-start
  44.3 4.1 %intra.1 = (bf16[8,256,256]{2,1,0:T(8,128)(2,1)}, bf16[256,1024]{1,0:T(8,128)(2,1)}) custom-call(bf16[128,2,1024]{2,1,0:T(2,128)(2,1)} %k_ref.3, f32[256,1024]{1,0:T(8,128)} %get-tuple-element.17.cum_ref, bf16[256,1024]{1,0:T(8,128)(2,1)} %get-tuple-element.18.q_dec_ref), custom_call_target="tpu_custom_call" | custom-call | flops 402653184 | bytes 5242880 | tf_op jit(solution)/shard_map/intra/pallas_call | solution.py:278
  48.4 11.1 %all-to-all-done.1 = bf16[16,256,128]{2,1,0:T(8,128)(2,1)S(1)} async-done(((bf16[16,256,128]{2,1,0:T(8,128)(2,1)}), bf16[16,256,128]{2,1,0:T(8,128)(2,1)S(1)}, u32[]{:S(2)}, u32[]{:S(2)}) %all-to-all-start.1) | async-done | bytes 1048608 | tf_op jit(solution)/shard_map/all_to_all | solution.py:227
  59.5 0.0 copy-start
  59.5 1.0 copy-done
  60.5 7.2 %value_grad.1 = (bf16[256,2048]{1,0:T(8,128)(2,1)}, bf16[8,16,256,128]{3,2,1,0:T(8,128)(2,1)}) custom-call(bf16[8,256,256]{2,1,0:T(8,128)(2,1)} %get-tuple-element.19.scores_ref, bf16[128,2,2048]{2,1,0:T(2,128)(2,1)} %do_ref.5, bf16[256,1024]{1,0:T(8,128)(2,1)} %get-tuple-element.20.k_dec_ref, bf16[2,8,256,128]{3,2,1,0:T(8,128)(2,1)} %bitcast.7, ...), custom_call_target="tpu_custom_call" | custom-call | flops 2415919104 | bytes 14680064 | tf_op jit(solution)/shard_map/value_grad/pallas_call | solution.py:300
  67.7 0.0 reduce-scatter.2.cloned.1.call-update
  67.7 0.0 all-gather.2.cloned.1.call-done.w_ref
  67.7 6.5 %project.1 = (bf16[256,2048]{1,0:T(8,128)(2,1)}, bf16[2,8,256,128]{3,2,1,0:T(8,128)(2,1)}) custom-call(bf16[128,2,2048]{2,1,0:T(2,128)(2,1)} %h_ref.3, bf16[2048,2048]{1,0:T(8,128)(2,1)} %all-gather.2.cloned.1.call-done.w_ref, bf16[256,1024]{1,0:T(8,128)(2,1)} %get-tuple-element.20.k_dec_ref), custom_call_target="tpu_custom_call" | custom-call | flops 2281701376 | bytes 12582912 | tf_op jit(solution)/shard_map/project/pallas_call | solution.py:329
  74.2 20.4 %all_to_all.26.rx_ref = bf16[16,256,128]{2,1,0:T(8,128)(2,1)S(1)} all-to-all(bf16[16,256,128]{2,1,0:T(8,128)(2,1)} %bitcast.11), channel_id=1, replica_groups=mesh['sp'=16,'dp'=8] {'sp'}, dimensions={0} | all-to-all | bytes 2097152 | tf_op jit(solution)/shard_map/all_to_all | solution.py:227
  94.6 0.3 scan.3
  94.9 18.0 %all_to_all.27 = bf16[16,256,128]{2,1,0:T(8,128)(2,1)} all-to-all(bf16[16,256,128]{2,1,0:T(8,128)(2,1)S(1)} %scan.3), channel_id=1, replica_groups=mesh['sp'=16,'dp'=8] {'sp'}, dimensions={0} | all-to-all | bytes 2097152 | tf_op jit(solution)/shard_map/all_to_all | solution.py:227
  112.9 6.4 %reduce-scatter.2.cloned.1.call-done = bf16[16,256,128]{2,1,0:T(8,128)(2,1)} async-done(((bf16[128,256,128]{2,1,0:T(8,128)(2,1)}), bf16[16,256,128]{2,1,0:T(8,128)(2,1)}) %reduce-scatter.2.cloned.1.call-update) | async-done | bytes 1048592 | tf_op jit(solution)/shard_map/reduce_scatter | solution.py:327
  119.3 6.7 %all-to-all-start.4 = ((bf16[16,256,128]{2,1,0:T(8,128)(2,1)}), bf16[16,256,128]{2,1,0:T(8,128)(2,1)S(1)}, u32[]{:S(2)}, u32[]{:S(2)}) async-start(bf16[16,256,128]{2,1,0:T(8,128)(2,1)} %reduce-scatter.2.cloned.1.call-done), calls=%async_computation.5 | async-start | bytes 2097152 | tf_op jit(solution)/shard_map/all_to_all | solution.py:227
  126.1 6.7 %hidden_grad.1 = bf16[128,2,2048]{2,1,0:T(2,128)(2,1)} custom-call(bf16[256,2048]{1,0:T(8,128)(2,1)} %get-tuple-element.22.dv_ref, bf16[2048,2048]{1,0:T(8,128)(2,1)} %all-gather.2.cloned.1.call-done.w_ref), custom_call_target="tpu_custom_call" | custom-call | flops 2147483648 | bytes 10485760 | tf_op jit(solution)/shard_map/hidden_grad/pallas_call | solution.py:347
  132.7 8.8 %final.1 = (bf16[128,2,1024]{2,1,0:T(2,128)(2,1)}, bf16[128,2,1024]{2,1,0:T(2,128)(2,1)}, bf16[128,2,1024]{2,1,0:T(2,128)(2,1)}) custom-call(bf16[128,2,1024]{2,1,0:T(2,128)(2,1)} %k_ref.3, bf16[128,2,1024]{2,1,0:T(2,128)(2,1)} %g_ref.3, f32[1,1024]{1,0:T(1,128)} %bitcast.13, f32[256,1024]{1,0:T(8,128)} %get-tuple-element.17.cum_ref, ...), custom_call_target="tpu_custom_call" | custom-call | flops 805306368 | bytes 10485760 | tf_op jit(solution)/shard_map/final/pallas_call | solution.py:361
  141.5 4.5 %all-to-all-done.4 = bf16[16,256,128]{2,1,0:T(8,128)(2,1)S(1)} async-done(((bf16[16,256,128]{2,1,0:T(8,128)(2,1)}), bf16[16,256,128]{2,1,0:T(8,128)(2,1)S(1)}, u32[]{:S(2)}, u32[]{:S(2)}) %all-to-all-start.4) | async-done | bytes 1048608 | tf_op jit(solution)/shard_map/all_to_all | solution.py:227
  146.1 0.8 convert_reduce_fusion
Async XLA Ops:
  7.2 60.6 %all-gather.2.cloned.1.call-start = ((), (), s32[]{:S(2)}) async-start(), calls=%async_computation.6 | async-start | bytes 9437184 | tf_op jit(solution)/shard_map/all_gather | solution.py:238
  40.6 18.9 %all-to-all-start.1 = ((bf16[16,256,128]{2,1,0:T(8,128)(2,1)}), bf16[16,256,128]{2,1,0:T(8,128)(2,1)S(1)}, u32[]{:S(2)}, u32[]{:S(2)}) async-start(bf16[16,256,128]{2,1,0:T(8,128)(2,1)} %scan.2), calls=%async_computation.1 | async-start | bytes 2097152 | tf_op jit(solution)/shard_map/all_to_all | solution.py:227
  44.3 75.1 %reduce-scatter.2.cloned.1.call-start = ((), (), s32[]{:S(2)}) async-start(), calls=%async_computation.7 | async-start | bytes 9437184 | tf_op jit(solution)/shard_map/reduce_scatter | solution.py:327
  59.5 1.0 copy-start
  119.3 26.7 %all-to-all-start.4 = ((bf16[16,256,128]{2,1,0:T(8,128)(2,1)}), bf16[16,256,128]{2,1,0:T(8,128)(2,1)S(1)}, u32[]{:S(2)}, u32[]{:S(2)}) async-start(bf16[16,256,128]{2,1,0:T(8,128)(2,1)} %reduce-scatter.2.cloned.1.call-done), calls=%async_computation.5 | async-start | bytes 2097152 | tf_op jit(solution)/shard_map/all_to_all | solution.py:227
Sparse Core Ops, SparseCore 0:
  9.7 51.5 all-gather.1
  67.8 51.4 reduce-scatter.1

commit v3 on v2

--- a/solution.py
+++ b/solution.py
@@ -19,6 +19,7 @@
 PAIR = 4
 STEPS = HEADS // PAIR
 F32 = jnp.float32
+STRIP = 16
 BF16 = jnp.bfloat16
 
 NN = (((1,), (0,)), ((), ()))
@@ -66,7 +67,19 @@
 
 
 def native(ref, cols):
+    if cols.stop - cols.start == DK:
+        parts = [
+            ref[i : i + STRIP, :, cols].reshape(SEQS * STRIP, DK)
+            for i in range(0, BLK, STRIP)
+        ]
+        return jnp.concatenate(parts, axis=0)
     return ref[:, :, cols].reshape(ROWS, cols.stop - cols.start)
+
+
+def put(ref, cols, x):
+    for i in range(0, BLK, STRIP):
+        part = x[SEQS * i : SEQS * (i + STRIP)]
+        ref[i : i + STRIP, :, cols] = part.reshape(STRIP, SEQS, DK)
 
 
 def head_slices(j):
@@ -208,9 +221,9 @@
         dq_dec = dot(dscores, k_inv, NN) + chosen(dot(do, state, NN), first)
         dk_inv = dot(dscores, q_dec, TN)
         dk_dec = chosen(dot(v, dstate, NN), first)
-        dq_ref[:, :, keys] = (q_scale * dq_dec).astype(BF16).reshape(BLK, SEQS, DK)
+        put(dq_ref, keys, (q_scale * dq_dec).astype(BF16))
         dk = (inv_scale * dk_inv + dec_scale * dk_dec).astype(BF16)
-        dk_ref[:, :, keys] = dk.reshape(BLK, SEQS, DK)
+        put(dk_ref, keys, dk)
         after = q_dec.astype(F32) * dq_dec - k_inv.astype(F32) * dk_inv
         before = k_dec.astype(F32) * dk_dec
         terms = jnp.concatenate([after, before], axis=0)
@@ -220,7 +233,7 @@
         dlog = dlog[:, :DK] + dlog[:, DK:] + jnp.exp(last) * through
         x = native(g_ref, keys).astype(F32) + bias_ref[:, keys]
         slope = (1.0 / SOFTNESS) / (1.0 + jnp.exp(x))
-        dg_ref[:, :, keys] = (dlog * slope).astype(BF16).reshape(BLK, SEQS, DK)
+        put(dg_ref, keys, (dlog * slope).astype(BF16))
 
 
 def over_sp(value):

time: 154 us -> 152 us (0.987)
  Pallas kernels: 41.5 us -> 36.5 us
  waiting for transfers between devices: 22.8 us -> 24.8 us
    all_to_all x2, waiting for transfers between devices: 15.6 us -> 18.3 us  [over_sp(): return lax.all_to_all(value, 'sp', split_axis=0, concat_axis=0, tiled=True)]
    pallas_call x1, Pallas kernels: 6.63 us -> 4.31 us  [arranged(): pl.pallas_call(decay_kernel, grid=(STEPS,), in_specs=[raw_key, raw_key, b...]
    pallas_call x1, Pallas kernels: 8.82 us -> 7.14 us  [arranged(): pl.pallas_call(final_kernel, grid=(STEPS,), in_specs=[raw_key, raw_key, b...]
  transfers between devices with their start and end apart: 4 -> 4, of which waited for: 3 -> 3; matrix products, arithmetic and copies ran while one was open for 0% -> 0% of each run, Pallas kernels for 27% -> 24%
where the time goes in v3:
time: 152 us; the launch traced here: 151 us
  blocking collectives  63.8 us (42%)
  Pallas kernels  36.5 us (24%)
  waiting for transfers between devices  24.8 us (16%)
  between operations  14.1 us (9%)
  starting transfers between devices  10.4 us (7%)
    all_to_all x3, blocking collectives, over_sp(): return lax.all_to_all(value, 'sp', split_axis=0, concat_axis=0, tiled=True)  63.8 us
    all_to_all x2, waiting for transfers between devices, over_sp(): return lax.all_to_all(value, 'sp', split_axis=0, concat_axis=0, tiled=True)  18.3 us
    all_to_all x2, starting transfers between devices, over_sp(): return lax.all_to_all(value, 'sp', split_axis=0, concat_axis=0, tiled=True)  10.4 us
    pallas_call x1, Pallas kernels, arranged(): pl.pallas_call(value_grad_kernel, grid=(STEPS,), in_specs=[score_spec, ra...  7.23 us
    pallas_call x1, Pallas kernels, arranged(): pl.pallas_call(final_kernel, grid=(STEPS,), in_specs=[raw_key, raw_key, b...  7.14 us
    pallas_call x1, Pallas kernels, arranged(): pl.pallas_call(hidden_grad_kernel, grid=(4,), in_specs=[pl.BlockSpec(val_...  6.68 us
    pallas_call x1, Pallas kernels, arranged(): pl.pallas_call(project_kernel, grid=(STEPS,), in_specs=[pl.BlockSpec((BLK...  6.47 us
    reduce_scatter x1, waiting for transfers between devices, arranged(): partial = lax.psum_scatter(partial, 'dp', scatter_dimension=0, tiled=True)  5.78 us
  transfers between devices with their start and end apart: 4, of which 3 were waited for; matrix products, arithmetic and copies ran while one was open for 0% of the time, Pallas kernels for 24%

profile of v3, /device:TPU:3, one launch (start us, length us, event | category | flops | bytes accessed | tf_op | source)
XLA Modules:
  0.0 151.4 jit_solution(15857370715283350001)
XLA Ops:
  7.2 0.0 all-gather.2.cloned.1.call-start
  7.2 0.7 all-gather.2.cloned.1.call-update
  7.9 4.3 %decay.1 = (bf16[2,8,272,128]{3,2,1,0:T(8,128)(2,1)}, f32[256,1024]{1,0:T(8,128)}, bf16[256,1024]{1,0:T(8,128)(2,1)}) custom-call(bf16[128,2,1024]{2,1,0:T(2,128)(2,1)} %q_ref.1, bf16[128,2,1024]{2,1,0:T(2,128)(2,1)} %g_ref.3, f32[1,1024]{1,0:T(1,128)} %bitcast.12, bf16[128,2,2048]{2,1,0:T(2,128)(2,1)} %do_ref.5), custom_call_target="tpu_custom_call" | custom-call | flops 402653184 | bytes 5242880 | tf_op jit(solution)/shard_map/decay/pallas_call | solution.py:270
  12.2 24.7 %all_to_all.25.rx_ref.last_ref = bf16[16,272,128]{2,1,0:T(8,128)(2,1)S(1)} all-to-all(bf16[16,272,128]{2,1,0:T(8,128)(2,1)} %bitcast.10), channel_id=1, replica_groups=mesh['sp'=16,'dp'=8] {'sp'}, dimensions={0} | all-to-all | bytes 2228224 | tf_op jit(solution)/shard_map/all_to_all | solution.py:240
  36.9 1.4 scan.2
  38.3 3.7 %all-to-all-start.1 = ((bf16[16,256,128]{2,1,0:T(8,128)(2,1)}), bf16[16,256,128]{2,1,0:T(8,128)(2,1)S(1)}, u32[]{:S(2)}, u32[]{:S(2)}) async-start(bf16[16,256,128]{2,1,0:T(8,128)(2,1)} %scan.2), calls=%async_computation.1 | async-start | bytes 2097152 | tf_op jit(solution)/shard_map/all_to_all | solution.py:240
  42.0 0.0 reduce-scatter.2.cloned.1.call-start
  42.0 3.0 %intra.1 = (bf16[8,256,256]{2,1,0:T(8,128)(2,1)}, bf16[256,1024]{1,0:T(8,128)(2,1)}) custom-call(bf16[128,2,1024]{2,1,0:T(2,128)(2,1)} %k_ref.3, f32[256,1024]{1,0:T(8,128)} %get-tuple-element.17.cum_ref, bf16[256,1024]{1,0:T(8,128)(2,1)} %get-tuple-element.18.q_dec_ref), custom_call_target="tpu_custom_call" | custom-call | flops 402653184 | bytes 5242880 | tf_op jit(solution)/shard_map/intra/pallas_call | solution.py:291
  45.0 12.1 %all-to-all-done.1 = bf16[16,256,128]{2,1,0:T(8,128)(2,1)S(1)} async-done(((bf16[16,256,128]{2,1,0:T(8,128)(2,1)}), bf16[16,256,128]{2,1,0:T(8,128)(2,1)S(1)}, u32[]{:S(2)}, u32[]{:S(2)}) %all-to-all-start.1) | async-done | bytes 1048608 | tf_op jit(solution)/shard_map/all_to_all | solution.py:240
  57.2 0.0 copy-start
  57.2 1.0 copy-done
  58.1 7.2 %value_grad.1 = (bf16[256,2048]{1,0:T(8,128)(2,1)}, bf16[8,16,256,128]{3,2,1,0:T(8,128)(2,1)}) custom-call(bf16[8,256,256]{2,1,0:T(8,128)(2,1)} %get-tuple-element.19.scores_ref, bf16[128,2,2048]{2,1,0:T(2,128)(2,1)} %do_ref.5, bf16[256,1024]{1,0:T(8,128)(2,1)} %get-tuple-element.20.k_dec_ref, bf16[2,8,256,128]{3,2,1,0:T(8,128)(2,1)} %bitcast.7, ...), custom_call_target="tpu_custom_call" | custom-call | flops 2415919104 | bytes 14680064 | tf_op jit(solution)/shard_map/value_grad/pallas_call | solution.py:313
  65.4 0.0 reduce-scatter.2.cloned.1.call-update
  65.4 0.0 all-gather.2.cloned.1.call-done.w_ref
  65.4 6.5 %project.1 = (bf16[256,2048]{1,0:T(8,128)(2,1)}, bf16[2,8,256,128]{3,2,1,0:T(8,128)(2,1)}) custom-call(bf16[128,2,2048]{2,1,0:T(2,128)(2,1)} %h_ref.3, bf16[2048,2048]{1,0:T(8,128)(2,1)} %all-gather.2.cloned.1.call-done.w_ref, bf16[256,1024]{1,0:T(8,128)(2,1)} %get-tuple-element.20.k_dec_ref), custom_call_target="tpu_custom_call" | custom-call | flops 2281701376 | bytes 12582912 | tf_op jit(solution)/shard_map/project/pallas_call | solution.py:342
  71.9 20.5 %all_to_all.26.rx_ref = bf16[16,256,128]{2,1,0:T(8,128)(2,1)S(1)} all-to-all(bf16[16,256,128]{2,1,0:T(8,128)(2,1)} %bitcast.11), channel_id=1, replica_groups=mesh['sp'=16,'dp'=8] {'sp'}, dimensions={0} | all-to-all | bytes 2097152 | tf_op jit(solution)/shard_map/all_to_all | solution.py:240
  92.4 0.3 scan.3
  92.7 18.5 %all_to_all.27 = bf16[16,256,128]{2,1,0:T(8,128)(2,1)} all-to-all(bf16[16,256,128]{2,1,0:T(8,128)(2,1)S(1)} %scan.3), channel_id=1, replica_groups=mesh['sp'=16,'dp'=8] {'sp'}, dimensions={0} | all-to-all | bytes 2097152 | tf_op jit(solution)/shard_map/all_to_all | solution.py:240
  111.2 5.8 %reduce-scatter.2.cloned.1.call-done = bf16[16,256,128]{2,1,0:T(8,128)(2,1)} async-done(((bf16[128,256,128]{2,1,0:T(8,128)(2,1)}), bf16[16,256,128]{2,1,0:T(8,128)(2,1)}) %reduce-scatter.2.cloned.1.call-update) | async-done | bytes 1048592 | tf_op jit(solution)/shard_map/reduce_scatter | solution.py:340
  117.0 6.7 %all-to-all-start.4 = ((bf16[16,256,128]{2,1,0:T(8,128)(2,1)}), bf16[16,256,128]{2,1,0:T(8,128)(2,1)S(1)}, u32[]{:S(2)}, u32[]{:S(2)}) async-start(bf16[16,256,128]{2,1,0:T(8,128)(2,1)} %reduce-scatter.2.cloned.1.call-done), calls=%async_computation.5 | async-start | bytes 2097152 | tf_op jit(solution)/shard_map/all_to_all | solution.py:240
  123.7 6.7 %hidden_grad.1 = bf16[128,2,2048]{2,1,0:T(2,128)(2,1)} custom-call(bf16[256,2048]{1,0:T(8,128)(2,1)} %get-tuple-element.22.dv_ref, bf16[2048,2048]{1,0:T(8,128)(2,1)} %all-gather.2.cloned.1.call-done.w_ref), custom_call_target="tpu_custom_call" | custom-call | flops 2147483648 | bytes 10485760 | tf_op jit(solution)/shard_map/hidden_grad/pallas_call | solution.py:360
  130.4 7.1 %final.1 = (bf16[128,2,1024]{2,1,0:T(2,128)(2,1)}, bf16[128,2,1024]{2,1,0:T(2,128)(2,1)}, bf16[128,2,1024]{2,1,0:T(2,128)(2,1)}) custom-call(bf16[128,2,1024]{2,1,0:T(2,128)(2,1)} %k_ref.3, bf16[128,2,1024]{2,1,0:T(2,128)(2,1)} %g_ref.3, f32[1,1024]{1,0:T(1,128)} %bitcast.13, f32[256,1024]{1,0:T(8,128)} %get-tuple-element.17.cum_ref, ...), custom_call_target="tpu_custom_call" | custom-call | flops 805306368 | bytes 10485760 | tf_op jit(solution)/shard_map/final/pallas_call | solution.py:374
  137.6 6.2 %all-to-all-done.4 = bf16[16,256,128]{2,1,0:T(8,128)(2,1)S(1)} async-done(((bf16[16,256,128]{2,1,0:T(8,128)(2,1)}), bf16[16,256,128]{2,1,0:T(8,128)(2,1)S(1)}, u32[]{:S(2)}, u32[]{:S(2)}) %all-to-all-start.4) | async-done | bytes 1048608 | tf_op jit(solution)/shard_map/all_to_all | solution.py:240
  143.8 0.8 convert_reduce_fusion
Async XLA Ops:
  7.2 58.2 %all-gather.2.cloned.1.call-start = ((), (), s32[]{:S(2)}) async-start(), calls=%async_computation.6 | async-start | bytes 9437184 | tf_op jit(solution)/shard_map/all_gather | solution.py:251
  38.3 18.9 %all-to-all-start.1 = ((bf16[16,256,128]{2,1,0:T(8,128)(2,1)}), bf16[16,256,128]{2,1,0:T(8,128)(2,1)S(1)}, u32[]{:S(2)}, u32[]{:S(2)}) async-start(bf16[16,256,128]{2,1,0:T(8,128)(2,1)} %scan.2), calls=%async_computation.1 | async-start | bytes 2097152 | tf_op jit(solution)/shard_map/all_to_all | solution.py:240
  42.0 75.1 %reduce-scatter.2.cloned.1.call-start = ((), (), s32[]{:S(2)}) async-start(), calls=%async_computation.7 | async-start | bytes 9437184 | tf_op jit(solution)/shard_map/reduce_scatter | solution.py:340
  57.2 1.0 copy-start
  117.0 26.7 %all-to-all-start.4 = ((bf16[16,256,128]{2,1,0:T(8,128)(2,1)}), bf16[16,256,128]{2,1,0:T(8,128)(2,1)S(1)}, u32[]{:S(2)}, u32[]{:S(2)}) async-start(bf16[16,256,128]{2,1,0:T(8,128)(2,1)} %reduce-scatter.2.cloned.1.call-done), calls=%async_computation.5 | async-start | bytes 2097152 | tf_op jit(solution)/shard_map/all_to_all | solution.py:240
Sparse Core Ops, SparseCore 0:
  9.7 51.5 all-gather.1
  65.5 51.4 reduce-scatter.1

commit v4 on v3

--- a/solution.py
+++ b/solution.py
@@ -13,7 +13,7 @@
 BLK = 128
 SEQS = 2
 ROWS = SEQS * BLK
-EXTRA = 16
+EXTRA = 8
 SOFTNESS = 16.0
 SCALE = DK**-0.5
 PAIR = 4
@@ -94,18 +94,21 @@
     return pltpu.CompilerParams(dimension_semantics=("arbitrary",))
 
 
-def decay_kernel(q_ref, g_ref, bias_ref, do_ref, delta_ref, cum_ref, q_dec_ref):
+def decayed(q_ref, g_ref, bias_ref, keys, lower):
+    x = native(g_ref, keys).astype(F32) + bias_ref[:, keys]
+    log_decay = (jnp.minimum(x, 0.0) - jnp.log(1.0 + jnp.exp(-jnp.abs(x)))) / SOFTNESS
+    sums = dot(lower, jnp.concatenate(split2(log_decay), axis=1), NN)
+    cum = sums[:, :DK] + sums[:, DK:]
+    q_dec = (native(q_ref, keys).astype(F32) * SCALE * jnp.exp(cum)).astype(BF16)
+    return cum, q_dec
+
+
+def decay_kernel(q_ref, g_ref, bias_ref, do_ref, delta_ref):
     lower = causal().astype(BF16)
     first = first_rows(DK)
     for j in range(PAIR):
         keys, vals = head_slices(j)
-        x = native(g_ref, keys).astype(F32) + bias_ref[:, keys]
-        log_decay = (jnp.minimum(x, 0.0) - jnp.log(1.0 + jnp.exp(-jnp.abs(x)))) / SOFTNESS
-        sums = dot(lower, jnp.concatenate(split2(log_decay), axis=1), NN)
-        cum = sums[:, :DK] + sums[:, DK:]
-        cum_ref[:, keys] = cum
-        q_dec = (native(q_ref, keys).astype(F32) * SCALE * jnp.exp(cum)).astype(BF16)
-        q_dec_ref[:, keys] = q_dec
+        cum, q_dec = decayed(q_ref, g_ref, bias_ref, keys, lower)
         delta = dot(native(do_ref, vals), halves(q_dec, first), TN)
         for s in range(SEQS):
             delta_ref[s, j, :DV, :] = delta[:, s * DK : (s + 1) * DK].astype(BF16)
@@ -119,15 +122,20 @@
             delta_ref[s, j, DV:, :] = tail.astype(BF16)
 
 
-def intra_kernel(k_ref, cum_ref, q_dec_ref, scores_ref, k_dec_ref):
+def intra_kernel(
+    q_ref, k_ref, g_ref, bias_ref, cum_ref, q_dec_ref, scores_ref, k_dec_ref
+):
     keep = causal()
+    lower = keep.astype(BF16)
     first = first_rows(DK)
     for j in range(PAIR):
         keys, _ = head_slices(j)
-        cum = cum_ref[:, keys]
+        cum, q_dec = decayed(q_ref, g_ref, bias_ref, keys, lower)
+        cum_ref[:, keys] = cum
+        q_dec_ref[:, keys] = q_dec
         k = native(k_ref, keys).astype(F32)
         k_inv = (k * jnp.exp(-cum)).astype(BF16)
-        scores = dot(q_dec_ref[:, keys], k_inv, NT)
+        scores = dot(q_dec, k_inv, NT)
         scores_ref[j] = jnp.where(keep, scores, 0.0).astype(BF16)
         k_dec_ref[:, keys] = (k * jnp.exp(last_of(cum, first) - cum)).astype(BF16)
 
@@ -142,32 +150,76 @@
         state = state * decay + rx_ref[b, :DV, :].astype(F32)
 
 
-def value_grad_kernel(
-    scores_ref, do_ref, k_dec_ref, dstate_ref, h_ref, dv_ref, part_ref
-):
+def value_grad_kernel(scores_ref, do_ref, k_dec_ref, dstate_ref, dv_ref):
     first = first_rows(DK)
-    heads = []
     for j in range(PAIR):
         keys, vals = head_slices(j)
         intra = dot(scores_ref[j], native(do_ref, vals), TN)
         dstate = jnp.concatenate([dstate_ref[0, j], dstate_ref[1, j]], axis=1)
         inter = dot(halves(k_dec_ref[:, keys], first), dstate, NT)
-        dv = (intra + inter).astype(BF16)
-        dv_ref[:, vals] = dv
-        heads.append(dv)
-    dv_all = jnp.concatenate(heads, axis=1)
-    group, tiles, height, span = part_ref.shape
-    for m in range(group):
-        hidden = native(h_ref, slice(m * height, (m + 1) * height))
-        part = dot(hidden, dv_all, TN).astype(BF16)
+        dv_ref[:, vals] = (intra + inter).astype(BF16)
+
+
+def pick_kernel(order_ref, h_ref, out_ref):
+    out_ref[...] = h_ref[...]
+
+
+def part_kernel(order_ref, h_ref, got_ref, dv_ref, dv_got_ref, top_ref, bottom_ref):
+    cols = slice(0, h_ref.shape[2])
+    part = dot(native(h_ref, cols), dv_ref[...], TN)
+    part = (part + dot(native(got_ref, cols), dv_got_ref[...], TN)).astype(BF16)
+    half = part.shape[0] // 2
+    top_ref[...] = part[:half]
+    bottom_ref[...] = part[half:]
+
+
+def rest_kernel(order_ref, h_ref, got_ref, dv_ref, dv_got_ref, *outs):
+    cols = slice(0, h_ref.shape[2])
+    part = dot(native(h_ref, cols), dv_ref[...], TN)
+    part = (part + dot(native(got_ref, cols), dv_got_ref[...], TN)).astype(BF16)
+    half = part.shape[0] // 2
+    for p in range(3):
+
+        @pl.when(pl.program_id(0) == p)
+        def _():
+            outs[2 * p][...] = part[:half]
+            outs[2 * p + 1][...] = part[half:]
+
+
+def join_kernel(top_refs, bottom_refs, out_ref):
+    tiles, _, span = out_ref.shape
+    half = top_refs[0].shape[0]
+    for refs, start in ((top_refs, 0), (bottom_refs, half)):
+        total = refs[0][...].astype(F32) + refs[1][...].astype(F32)
+        total = (total + refs[2][...].astype(F32)).astype(BF16)
         for t in range(tiles):
-            part_ref[m, t] = part[:, t * span : (t + 1) * span]
-
-
-def project_kernel(h_ref, w_ref, k_dec_ref, v_ref, delta_ref):
+            out_ref[t, start : start + half] = total[:, t * span : (t + 1) * span]
+
+
+def join_parts(*refs):
+    join_kernel(refs[:3], refs[3:6], refs[6])
+
+
+def project_kernel(
+    order_ref, h_ref, near_ref, near_got_ref, far_ref, far_got_ref, k_dec_ref,
+    v_ref, delta_ref, held,
+):
     first = first_rows(DK)
-    hidden = native(h_ref, slice(0, h_ref.shape[2]))
-    v_all = dot(hidden, w_ref[...], NN).astype(BF16)
+    shard = far_ref.shape[0]
+
+    @pl.when(pl.program_id(0) == 0)
+    def _():
+        for p in range(held.shape[1] // shard):
+            start = pl.multiple_of(order_ref[p] * shard, shard)
+            cols = h_ref[:, :, pl.ds(start, shard)].reshape(ROWS, shard)
+            held[:, p * shard : (p + 1) * shard] = cols
+
+    v_all = jnp.zeros(v_ref.shape, F32)
+    start = 0
+    for ref in (near_ref, near_got_ref, far_ref, far_got_ref):
+        v_all += dot(held[:, start : start + ref.shape[0]], ref[...], NN)
+        start += ref.shape[0]
+    v_all = v_all.astype(BF16)
     v_ref[...] = v_all
     for j in range(PAIR):
         keys, vals = head_slices(j)
@@ -176,9 +228,19 @@
             delta_ref[s, j] = delta[:, s * DK : (s + 1) * DK].astype(BF16)
 
 
-def hidden_grad_kernel(dv_ref, w_ref, out_ref):
-    grad = dot(dv_ref[...], w_ref[...], NT).astype(BF16)
-    out_ref[...] = grad.reshape(out_ref.shape)
+def hidden_grad_kernel(
+    order_ref, dv_ref, near_ref, near_got_ref, far_ref, far_got_ref, out_ref
+):
+    p = pl.program_id(0)
+
+    def emit(ref):
+        grad = dot(dv_ref[...], ref[...], NT).astype(BF16)
+        out_ref[...] = grad.reshape(out_ref.shape)
+
+    pl.when(p < 3)(lambda: emit(near_ref))
+    pl.when((p >= 3) & (p < 6))(lambda: emit(near_got_ref))
+    pl.when(p == 6)(lambda: emit(far_ref))
+    pl.when(p == 7)(lambda: emit(far_got_ref))
 
 
 def final_kernel(
@@ -248,7 +310,32 @@
     _, sequences, width = hidden_in.shape
     blocks = lax.axis_size("sp")
     group = lax.axis_size("dp")
-    weight = lax.all_gather(value_weight, "dp", axis=0, tiled=True)
+    place = lax.axis_index("dp")
+    chip, core = place // 2, place % 2
+    chips = group // 2
+    shard = width // group
+    shift = jnp.array([0, -1, 1, 0, -1, 1, 2, 2, 2, 1, -1, 0, 2, 1, -1, 0], jnp.int32)
+    other = jnp.array([0, 0, 0, 1, 1, 1, 0, 1, 0, 0, 0, 0, 0, 0, 0, 0], jnp.int32)
+    twice = jnp.array([2] * 12 + [1] * 4, jnp.int32)
+    order = twice * ((chip + shift + chips) % chips) + (twice - 1) * ((core + other) % 2)
+    order = order.astype(jnp.int32)
+
+    def along(value, step):
+        pairs = [(d, (d + 2 * step) % group) for d in range(group)]
+        return lax.ppermute(value, "dp", pairs)
+
+    def swap(value):
+        return lax.ppermute(value, "dp", [(d, d ^ 1) for d in range(group)])
+
+    half = shard // 2
+    before = along(value_weight, 1)
+    after = along(value_weight, -1)
+    far_one = along(before[:half], 1)
+    far_two = along(after[half:], -1)
+    far = jnp.concatenate([far_one, far_two], axis=0)
+    near = jnp.concatenate([value_weight, before, after], axis=0)
+    near_got = swap(near)
+    far_got = swap(far)
     items = sequences * HEADS
     values = HEADS * DV
     bias = decay_bias.reshape(1, HEADS * DK)
@@ -267,37 +354,50 @@
     mm = 2 * BLK * DK * DV * items
     big = 2 * ROWS * width * values
 
-    delta, cum, q_dec = pl.pallas_call(
+    delta = pl.pallas_call(
         decay_kernel,
         grid=(STEPS,),
         in_specs=[raw_key, raw_key, bias_spec, raw_val],
-        out_specs=[
-            pl.BlockSpec((SEQS, PAIR, DV + EXTRA, DK), lambda i: (0, i, 0, 0)),
-            key_spec,
-            key_spec,
-        ],
+        out_specs=pl.BlockSpec((SEQS, PAIR, DV + EXTRA, DK), lambda i: (0, i, 0, 0)),
+        out_shape=shaped((SEQS, HEADS, DV + EXTRA, DK)),
+        compiler_params=params(),
+        cost_estimate=cost(3 * mm, 4 << 20),
+        name="decay",
+    )(query_act, gate_act, bias, out_grad)
+
+    rx = over_sp(delta.reshape(items, DV + EXTRA, DK))
+
+    cum, q_dec, scores, k_dec = pl.pallas_call(
+        intra_kernel,
+        grid=(STEPS,),
+        in_specs=[raw_key, raw_key, raw_key, bias_spec],
+        out_specs=[key_spec, key_spec, score_spec, key_spec],
         out_shape=[
-            shaped((SEQS, HEADS, DV + EXTRA, DK)),
             shaped(key_shape, F32),
             shaped(key_shape),
+            shaped((HEADS, ROWS, ROWS)),
+            shaped(key_shape),
         ],
-        compiler_params=params(),
-        cost_estimate=cost(3 * mm, 5 << 20),
-        name="decay",
-    )(query_act, gate_act, bias, out_grad)
-
-    rx = over_sp(delta.reshape(items, DV + EXTRA, DK))
-
-    scores, k_dec = pl.pallas_call(
-        intra_kernel,
-        grid=(STEPS,),
-        in_specs=[raw_key, key_spec, key_spec],
-        out_specs=[score_spec, key_spec],
-        out_shape=[shaped((HEADS, ROWS, ROWS)), shaped(key_shape)],
         compiler_params=params(),
         cost_estimate=cost(3 * mm, 5 << 20),
         name="intra",
-    )(key_act, cum, q_dec)
+    )(query_act, key_act, gate_act, bias)
+
+    raw = (BLK, SEQS, shard)
+    given = pl.pallas_call(
+        pick_kernel,
+        grid_spec=pltpu.PrefetchScalarGridSpec(
+            num_scalar_prefetch=1,
+            grid=(chips,),
+            in_specs=[pl.BlockSpec(raw, lambda i, o: (0, 0, 2 * i + o[3] % 2))],
+            out_specs=pl.BlockSpec(raw, lambda i, o: (0, 0, i)),
+        ),
+        out_shape=shaped((BLK, SEQS, width // 2)),
+        compiler_params=params(),
+        cost_estimate=cost(1 << 22, 1 << 20),
+        name="pick",
+    )(order, hidden_in)
+    got = swap(given)
 
     def scan(arrived, reverse):
         return pl.pallas_call(
@@ -308,68 +408,133 @@
             name="scan",
         )(arrived, rx)
 
-    dstate = over_sp(scan(rx, True)).reshape(state_shape)
-
-    dv, partial = pl.pallas_call(
+    dcarried = scan(rx, True)
+    dstate = over_sp(dcarried).reshape(state_shape)
+
+    dv = pl.pallas_call(
         value_grad_kernel,
         grid=(STEPS,),
-        in_specs=[
-            score_spec,
-            raw_val,
-            key_spec,
-            state_spec,
-            pl.BlockSpec((BLK, SEQS, width), lambda i: (0, 0, 0)),
-        ],
-        out_specs=[
-            val_spec,
-            pl.BlockSpec(
-                (group, blocks // STEPS, width // group, values // blocks),
-                lambda i: (0, i, 0, 0),
+        in_specs=[score_spec, raw_val, key_spec, state_spec],
+        out_specs=val_spec,
+        out_shape=shaped(val_shape),
+        compiler_params=params(),
+        cost_estimate=cost(3 * mm, 5 << 20),
+        name="value_grad",
+    )(scores, out_grad, k_dec, dstate)
+
+    dv_got = swap(dv)
+    turns = 2
+
+    def part():
+        raw = (BLK, SEQS, shard)
+        return pl.pallas_call(
+            part_kernel,
+            grid_spec=pltpu.PrefetchScalarGridSpec(
+                num_scalar_prefetch=1,
+                grid=(turns,),
+                in_specs=[
+                    pl.BlockSpec(raw, lambda i, o: (0, 0, o[8])),
+                    pl.BlockSpec(raw, lambda i, o: (0, 0, o[12])),
+                    pl.BlockSpec((ROWS, values // turns), lambda i, o: (0, i)),
+                    pl.BlockSpec((ROWS, values // turns), lambda i, o: (0, i)),
+                ],
+                out_specs=[pl.BlockSpec((half, values // turns), lambda i, o: (0, i))] * 2,
             ),
-        ],
-        out_shape=[
-            shaped(val_shape),
-            shaped((group, blocks, width // group, values // blocks)),
-        ],
-        compiler_params=params(),
-        cost_estimate=cost(big + 2 * mm, 14 << 20),
-        name="value_grad",
-    )(scores, out_grad, k_dec, dstate, hidden_in)
-
-    partial = partial.reshape(group * blocks, width // group, values // blocks)
-    partial = lax.psum_scatter(partial, "dp", scatter_dimension=0, tiled=True)
+            out_shape=[shaped((half, values))] * 2,
+            compiler_params=params(),
+            cost_estimate=cost(big // 4, 5 << 20),
+        )(order, hidden_in, got, dv, dv_got)
+
+    def rest():
+        raw = (BLK, SEQS, shard)
+        whole = pl.BlockSpec((ROWS, values), lambda i, o: (0, 0))
+        return pl.pallas_call(
+            rest_kernel,
+            grid_spec=pltpu.PrefetchScalarGridSpec(
+                num_scalar_prefetch=1,
+                grid=(3,),
+                in_specs=[
+                    pl.BlockSpec(raw, lambda i, o: (0, 0, o[9 + i])),
+                    pl.BlockSpec(raw, lambda i, o: (0, 0, o[13 + i])),
+                    whole,
+                    whole,
+                ],
+                out_specs=[pl.BlockSpec((half, values), lambda i, o: (0, 0))] * 6,
+            ),
+            out_shape=[shaped((half, values))] * 6,
+            compiler_params=params(),
+            cost_estimate=cost(3 * big // 4, 8 << 20),
+            name="part_rest",
+        )(order, hidden_in, got, dv, dv_got)
+
+    far_top, far_bottom = part()
+    from_before = along(far_top, 1)
+    from_after = along(far_bottom, -1)
+    next_top, next_bottom, last_top, last_bottom, own_top, own_bottom = rest()
+    ready_before = along(next_bottom, 1)
+    ready_after = along(last_top, -1)
+
+    def plus(one, two):
+        return (one.astype(F32) + two.astype(F32)).astype(BF16)
+
+    late_before = along(plus(next_top, from_before), 1)
+    late_after = along(plus(last_bottom, from_after), -1)
+    partial = pl.pallas_call(
+        join_parts,
+        out_shape=shaped((blocks, shard, values // blocks)),
+        compiler_params=pltpu.CompilerParams(vmem_limit_bytes=20 << 20),
+        cost_estimate=cost(1 << 22, 4 << 20),
+        name="join",
+    )(own_top, late_before, ready_after, own_bottom, ready_before, late_after)
 
     v, vdelta = pl.pallas_call(
         project_kernel,
-        grid=(STEPS,),
-        in_specs=[
-            pl.BlockSpec((BLK, SEQS, width), lambda i: (0, 0, 0)),
-            pl.BlockSpec((width, PAIR * DV), lambda i: (0, i)),
-            key_spec,
-        ],
-        out_specs=[val_spec, state_spec],
+        grid_spec=pltpu.PrefetchScalarGridSpec(
+            num_scalar_prefetch=1,
+            grid=(STEPS,),
+            in_specs=[
+                pl.BlockSpec((BLK, SEQS, width), lambda i, o: (0, 0, 0)),
+                pl.BlockSpec((3 * shard, PAIR * DV), lambda i, o: (0, i)),
+                pl.BlockSpec((3 * shard, PAIR * DV), lambda i, o: (0, i)),
+                pl.BlockSpec((shard, PAIR * DV), lambda i, o: (0, i)),
+                pl.BlockSpec((shard, PAIR * DV), lambda i, o: (0, i)),
+                pl.BlockSpec((ROWS, PAIR * DK), lambda i, o: (0, i)),
+            ],
+            out_specs=[
+                pl.BlockSpec((ROWS, PAIR * DV), lambda i, o: (0, i)),
+                pl.BlockSpec((SEQS, PAIR, DV, DK), lambda i, o: (0, i, 0, 0)),
+            ],
+            scratch_shapes=[pltpu.VMEM((ROWS, width), BF16)],
+        ),
         out_shape=[shaped(val_shape), shaped(state_shape)],
         compiler_params=params(),
         cost_estimate=cost(big + mm, 12 << 20),
         name="project",
-    )(hidden_in, weight, k_dec)
+    )(order, hidden_in, near, near_got, far, far_got, k_dec)
 
     vrx = over_sp(vdelta.reshape(items, DV, DK))
     state = over_sp(scan(vrx, False)).reshape(state_shape)
 
+    block = (shard, values)
     hidden_grad = pl.pallas_call(
         hidden_grad_kernel,
-        grid=(4,),
-        in_specs=[
-            pl.BlockSpec(val_shape, lambda i: (0, 0)),
-            pl.BlockSpec((width // 4, values), lambda i: (i, 0)),
-        ],
-        out_specs=pl.BlockSpec((BLK, SEQS, width // 4), lambda i: (0, 0, i)),
+        grid_spec=pltpu.PrefetchScalarGridSpec(
+            num_scalar_prefetch=1,
+            grid=(group,),
+            in_specs=[
+                pl.BlockSpec(val_shape, lambda i, o: (0, 0)),
+                pl.BlockSpec(block, lambda i, o: (jnp.minimum(i, 2), 0)),
+                pl.BlockSpec(block, lambda i, o: (jnp.clip(i - 3, 0, 2), 0)),
+                pl.BlockSpec(block, lambda i, o: (0, 0)),
+                pl.BlockSpec(block, lambda i, o: (0, 0)),
+            ],
+            out_specs=pl.BlockSpec((BLK, SEQS, shard), lambda i, o: (0, 0, o[i])),
+        ),
         out_shape=shaped((BLK, SEQS, width)),
         compiler_params=params(),
         cost_estimate=cost(big, 10 << 20),
         name="hidden_grad",
-    )(dv, weight)
+    )(order, dv, near, near_got, far, far_got)
 
     dq, dk, dg = pl.pallas_call(
         final_kernel,

time: 152 us -> 187 us (1.23)
  the two profiles are of different devices: /device:TPU:3 before, /device:TPU:8 now
where the time goes in v4:
time: 187 us; the launch traced here: 184 us
  waiting for transfers between devices  62.9 us (34%)
  Pallas kernels  56.3 us (30%)
  starting transfers between devices  48.7 us (26%)
  local copies, waits for them, and re-layouts  10 us (5%)
  other arithmetic  4.77 us (3%)
    all_to_all x5, waiting for transfers between devices, over_sp(): return lax.all_to_all(value, 'sp', split_axis=0, concat_axis=0, tiled=True)  32.3 us
    all_to_all x5, starting transfers between devices, over_sp(): return lax.all_to_all(value, 'sp', split_axis=0, concat_axis=0, tiled=True)  32.3 us
    ppermute x10, waiting for transfers between devices, along(): return lax.ppermute(value, 'dp', pairs)  30.7 us
    ppermute x10, starting transfers between devices, along(): return lax.ppermute(value, 'dp', pairs)  16.3 us
    pallas_call x1, Pallas kernels, arranged(): pl.pallas_call(hidden_grad_kernel, grid_spec=pltpu.PrefetchScalarGridSpec...  9.68 us
    pallas_call x1, Pallas kernels, arranged(): pl.pallas_call(project_kernel, grid_spec=pltpu.PrefetchScalarGridSpec(num...  8.1 us
    pallas_call x1, Pallas kernels, arranged(): pl.pallas_call(final_kernel, grid=(STEPS,), in_specs=[raw_key, raw_key, b...  7.13 us
    pallas_call x1, Pallas kernels, rest(): pl.pallas_call(rest_kernel, grid_spec=pltpu.PrefetchScalarGridSpec(num_sc...  6.75 us
  transfers between devices with their start and end apart: 19, of which 10 were waited for; matrix products, arithmetic and copies ran while one was open for 7% of the time, Pallas kernels for 27%

profile of v4, /device:TPU:8, one launch (start us, length us, event | category | flops | bytes accessed | tf_op | source)
XLA Modules:
  0.0 183.6 jit_solution(9568488518190527200)
XLA Ops:
  0.6 1.6 collective-permute-start
  2.2 1.7 collective-permute-start.1
  3.9 3.9 %decay.1 = bf16[2,8,264,128]{3,2,1,0:T(8,128)(2,1)} custom-call(bf16[128,2,1024]{2,1,0:T(2,128)(2,1)} %q_ref.3, bf16[128,2,1024]{2,1,0:T(2,128)(2,1)} %g_ref.5, f32[1,1024]{1,0:T(1,128)} %bitcast.10, bf16[128,2,2048]{2,1,0:T(2,128)(2,1)} %do_ref.5), custom_call_target="tpu_custom_call" | custom-call | flops 402653184 | bytes 4194304 | tf_op jit(solution)/shard_map/decay/pallas_call | solution.py:357
  7.9 8.4 %all-to-all-start = ((bf16[16,264,128]{2,1,0:T(8,128)(2,1)}), bf16[16,264,128]{2,1,0:T(8,128)(2,1)S(1)}, u32[]{:S(2)}, u32[]{:S(2)}) async-start(bf16[16,264,128]{2,1,0:T(8,128)(2,1)} %bitcast.7), calls=%async_computation | async-start | bytes 2162688 | tf_op jit(solution)/shard_map/all_to_all | solution.py:302
  16.3 2.3 %constant_dynamic-update-slice_fusion.2 = bf16[768,2048]{1,0:T(8,128)(2,1)} fusion(bf16[256,2048]{1,0:T(8,128)(2,1)} %param.15), kind=kLoop, calls=%fused_computation.5 | loop fusion | bytes 2097152
  18.6 8.4 %collective-permute-done = bf16[256,2048]{1,0:T(8,128)(2,1)S(1)} collective-permute-done((bf16[256,2048]{1,0:T(8,128)(2,1)}, bf16[256,2048]{1,0:T(8,128)(2,1)S(1)}, u32[]{:S(2)}, u32[]{:S(2)}) %collective-permute-start) | collective-permute-done | bytes 1048608 | tf_op jit(solution)/shard_map/ppermute | solution.py:325
  27.0 1.2 constant_dynamic-update-slice_fusion.1
  28.2 0.0 collective-permute-done.1
  28.2 1.1 constant_dynamic-update-slice_fusion.near_ref
  29.3 0.0 collective-permute-start.2
  29.3 2.6 %all-to-all-done.rx_ref.last_ref = bf16[16,264,128]{2,1,0:T(8,128)(2,1)S(1)} async-done(((bf16[16,264,128]{2,1,0:T(8,128)(2,1)}), bf16[16,264,128]{2,1,0:T(8,128)(2,1)S(1)}, u32[]{:S(2)}, u32[]{:S(2)}) %all-to-all-start) | async-done | bytes 1081376 | tf_op jit(solution)/shard_map/all_to_all | solution.py:302
  31.8 1.4 scan.2
  33.2 5.8 %all-to-all-start.1 = ((bf16[16,256,128]{2,1,0:T(8,128)(2,1)}), bf16[16,256,128]{2,1,0:T(8,128)(2,1)S(1)}, u32[]{:S(2)}, u32[]{:S(2)}) async-start(bf16[16,256,128]{2,1,0:T(8,128)(2,1)} %scan.2), calls=%async_computation.1 | async-start | bytes 2097152 | tf_op jit(solution)/shard_map/all_to_all | solution.py:302
  39.1 4.3 %intra.1 = (f32[256,1024]{1,0:T(8,128)}, bf16[256,1024]{1,0:T(8,128)(2,1)}, bf16[8,256,256]{2,1,0:T(8,128)(2,1)}, bf16[256,1024]{1,0:T(8,128)(2,1)}) custom-call(bf16[128,2,1024]{2,1,0:T(2,128)(2,1)} %q_ref.3, bf16[128,2,1024]{2,1,0:T(2,128)(2,1)} %k_ref.3, bf16[128,2,1024]{2,1,0:T(2,128)(2,1)} %g_ref.5, f32[1,1024]{1,0:T(1,128)} %bitcast.11), custom_call_target="tpu_custom_call" | custom-call | flops 402653184 | bytes 5242880 | tf_op jit(solution)/shard_map/intra/pallas_call | solution.py:370
  43.4 12.2 %all-to-all-done.1 = bf16[16,256,128]{2,1,0:T(8,128)(2,1)S(1)} async-done(((bf16[16,256,128]{2,1,0:T(8,128)(2,1)}), bf16[16,256,128]{2,1,0:T(8,128)(2,1)S(1)}, u32[]{:S(2)}, u32[]{:S(2)}) %all-to-all-start.1) | async-done | bytes 1048608 | tf_op jit(solution)/shard_map/all_to_all | solution.py:302
  55.5 1.1 copy-done.2
  56.6 3.4 %value_grad.1.dv_ref = bf16[256,2048]{1,0:T(8,128)(2,1)} custom-call(bf16[8,256,256]{2,1,0:T(8,128)(2,1)} %get-tuple-element.22.scores_ref, bf16[128,2,2048]{2,1,0:T(2,128)(2,1)} %do_ref.5, bf16[256,1024]{1,0:T(8,128)(2,1)} %get-tuple-element.23.k_dec_ref, bf16[2,8,256,128]{3,2,1,0:T(8,128)(2,1)} %bitcast.5), custom_call_target="tpu_custom_call" | custom-call | flops 402653184 | bytes 5242880 | tf_op jit(solution)/shard_map/value_grad/pallas_call | solution.py:414
  60.0 0.0 collective-permute-start.7
  60.0 1.1 slice.8
  61.1 0.4 collective-permute-start.3
  61.5 0.8 slice.9
  62.3 2.9 %collective-permute-start.4 = (bf16[128,2048]{1,0:T(8,128)(2,1)}, bf16[128,2048]{1,0:T(8,128)(2,1)}, u32[]{:S(2)}, u32[]{:S(2)}) collective-permute-start(bf16[128,2048]{1,0:T(8,128)(2,1)} %slice.9), channel_id=1, source_target_pairs={{0,6},{1,7},{2,0},{3,1},{4,2},{5,3},{6,4},{7,5},{8,14},{9,15},{10,... | collective-permute-start | bytes 1572872 | tf_op jit(solution)/shard_map/ppermute | solution.py:325
  65.2 0.5 fusion.2.order_ref
  65.7 3.8 %pick.1 = bf16[128,2,1024]{2,1,0:T(2,128)(2,1)} custom-call(s32[16]{0:T(128)} %fusion.2.order_ref, bf16[128,2,2048]{2,1,0:T(2,128)(2,1)} %h_ref.7), custom_call_target="tpu_custom_call" | custom-call | flops 4194304 | bytes 1048576 | tf_op jit(solution)/shard_map/pick/pallas_call | solution.py:387
  69.6 0.0 collective-permute-start.6
  69.6 7.1 %collective-permute-done.3 = bf16[128,2048]{1,0:T(8,128)(2,1)S(1)} collective-permute-done((bf16[128,2048]{1,0:T(8,128)(2,1)S(1)}, bf16[128,2048]{1,0:T(8,128)(2,1)S(1)}, u32[]{:S(2)}, u32[]{:S(2)}) %collective-permute-start.3) | collective-permute-done | bytes 524320 | tf_op jit(solution)/shard_map/ppermute | solution.py:325
  76.7 0.4 collective-permute-done.4
  77.1 1.1 constant_dynamic-update-slice_fusion.3.far_ref
  78.2 0.0 copy-start.3
  78.2 0.1 collective-permute-start.5
  78.3 0.0 collective-permute-done.6.got_ref
  78.3 0.0 collective-permute-done.7.dv_got_ref
  78.3 3.8 %shard_map.137 = (bf16[128,2048]{1,0:T(8,128)(2,1)}, bf16[128,2048]{1,0:T(8,128)(2,1)}) custom-call(s32[16]{0:T(128)} %fusion.2.order_ref, bf16[128,2,2048]{2,1,0:T(2,128)(2,1)} %h_ref.7, bf16[128,2,1024]{2,1,0:T(2,128)(2,1)} %collective-permute-done.6.got_ref, bf16[256,2048]{1,0:T(8,128)(2,1)} %value_grad.1.dv_ref, ...), custom_call_target="tpu_custom_call" | custom-call | flops 536870912 | bytes 5242880 | tf_op jit(solution)/shard_map/pallas_call | solution.py:430
  82.1 1.0 collective-permute-start.8
  83.1 2.7 %collective-permute-start.12 = (bf16[128,2048]{1,0:T(8,128)(2,1)}, bf16[128,2048]{1,0:T(8,128)(2,1)}, u32[]{:S(2)}, u32[]{:S(2)}) collective-permute-start(bf16[128,2048]{1,0:T(8,128)(2,1)} %get-tuple-element.38), channel_id=1, source_target_pairs={{0,6},{1,7},{2,0},{3,1},{4,2},{5,3},{6,4},{7,5},{8,14},{9,15},{10,... | collective-permute-start | bytes 1572872 | tf_op jit(solution)/shard_map/ppermute | solution.py:325
  85.8 6.8 %part_rest.1 = (bf16[128,2048]{1,0:T(8,128)(2,1)}, bf16[128,2048]{1,0:T(8,128)(2,1)}, bf16[128,2048]{1,0:T(8,128)(2,1)}, bf16[128,2048]{1,0:T(8,128)(2,1)}, bf16...) custom-call(s32[16]{0:T(128)} %fusion.2.order_ref, bf16[128,2,2048]{2,1,0:T(2,128)(2,1)} %h_ref.7, ...), custom_call_target="tpu_custom_call" | custom-call | flops 1610612736 | bytes 8388608 | tf_op jit(solution)/shard_map/part_rest/pallas_call | solution.py:451
  92.6 2.0 %collective-permute-start.10 = (bf16[128,2048]{1,0:T(8,128)(2,1)}, bf16[128,2048]{1,0:T(8,128)(2,1)}, u32[]{:S(2)}, u32[]{:S(2)}) collective-permute-start(bf16[128,2048]{1,0:T(8,128)(2,1)} %get-tuple-element.34), channel_id=1, source_target_pairs={{0,6},{1,7},{2,0},{3,1},{4,2},{5,3},{6,4},{7,5},{8,14},{9,15},{10,... | collective-permute-start | bytes 1572872 | tf_op jit(solution)/shard_map/ppermute | solution.py:325
  94.5 4.1 %collective-permute-done.8 = bf16[128,2048]{1,0:T(8,128)(2,1)} collective-permute-done((bf16[128,2048]{1,0:T(8,128)(2,1)}, bf16[128,2048]{1,0:T(8,128)(2,1)}, u32[]{:S(2)}, u32[]{:S(2)}) %collective-permute-start.8) | collective-permute-done | bytes 524320 | tf_op jit(solution)/shard_map/ppermute | solution.py:325
  98.6 0.0 collective-permute-start.11
  98.6 2.1 %add_convert_fusion.1 = bf16[128,2048]{1,0:T(8,128)(2,1)} fusion(bf16[128,2048]{1,0:T(8,128)(2,1)} %collective-permute-done.8, bf16[128,2048]{1,0:T(8,128)(2,1)} %get-tuple-element.32), kind=kLoop, calls=%fused_computation.2 | loop fusion | flops 1048576 | bytes 1572864 | tf_op jit(solution)/shard_map/convert_element_type | solution.py:478
  100.7 0.0 collective-permute-done.5.far_got_ref
  100.7 0.7 collective-permute-start.9
  101.4 0.0 collective-permute-done.2.near_got_ref
  101.4 0.3 copy-done.5
  101.8 8.1 %project.1 = (bf16[256,2048]{1,0:T(8,128)(2,1)}, bf16[2,8,256,128]{3,2,1,0:T(8,128)(2,1)}) custom-call(s32[16]{0:T(128)} %fusion.2.order_ref, bf16[128,2,2048]{2,1,0:T(2,128)(2,1)} %h_ref.7, bf16[768,2048]{1,0:T(8,128)(2,1)} %constant_dynamic-update-slice_fusion.near_ref, bf16[768,2048]{1,0:T(8,128)(2,1)} %collective-permute-done.2.near_got_ref, ...), custom_call_target="tpu_custom_call" | custom-call | flops 2281701376 | bytes 12582912 | tf_op jit(solution)/shard_map/project/pallas_call | solution.py:490
  109.9 5.8 %all-to-all-start.2 = ((bf16[16,256,128]{2,1,0:T(8,128)(2,1)}), bf16[16,256,128]{2,1,0:T(8,128)(2,1)S(1)}, u32[]{:S(2)}, u32[]{:S(2)}) async-start(bf16[16,256,128]{2,1,0:T(8,128)(2,1)} %bitcast.9), calls=%async_computation.2 | async-start | bytes 2097152 | tf_op jit(solution)/shard_map/all_to_all | solution.py:302
  115.7 0.0 collective-permute-done.12
  115.7 1.3 add_convert_fusion
  117.0 3.3 %collective-permute-start.13 = (bf16[128,2048]{1,0:T(8,128)(2,1)S(1)}, bf16[128,2048]{1,0:T(8,128)(2,1)S(1)}, u32[]{:S(2)}, u32[]{:S(2)}) collective-permute-start(bf16[128,2048]{1,0:T(8,128)(2,1)S(1)} %add_convert_fusion), channel_id=1, source_target_pairs={{0,6},{1,7},{2,0},{3,1},{4,2},{5,3},{6,4},{7,5},{8,14},{9,15},{10,... | collective-permute-start | bytes 1572872 | tf_op jit(solution)/shard_map/ppermute | solution.py:325
  120.4 0.0 collective-permute-done.10.refs_2_
  120.4 0.0 collective-permute-done.11.refs_4_
  120.4 4.7 %collective-permute-done.9.refs_1_ = bf16[128,2048]{1,0:T(8,128)(2,1)} collective-permute-done((bf16[128,2048]{1,0:T(8,128)(2,1)}, bf16[128,2048]{1,0:T(8,128)(2,1)}, u32[]{:S(2)}, u32[]{:S(2)}) %collective-permute-start.9) | collective-permute-done | bytes 524320 | tf_op jit(solution)/shard_map/ppermute | solution.py:325
  125.1 5.9 %collective-permute-done.13.refs_5_ = bf16[128,2048]{1,0:T(8,128)(2,1)S(1)} collective-permute-done((bf16[128,2048]{1,0:T(8,128)(2,1)S(1)}, bf16[128,2048]{1,0:T(8,128)(2,1)S(1)}, u32[]{:S(2)}, u32[]{:S(2)}) %collective-permute-start.13) | collective-permute-done | bytes 524320 | tf_op jit(solution)/shard_map/ppermute | solution.py:325
  131.0 2.9 %join.1 = bf16[16,256,128]{2,1,0:T(8,128)(2,1)} custom-call(bf16[128,2048]{1,0:T(8,128)(2,1)S(1)} %copy-done, bf16[128,2048]{1,0:T(8,128)(2,1)} %collective-permute-done.9.refs_1_, bf16[128,2048]{1,0:T(8,128)(2,1)} %collective-permute-done.10.refs_2_, bf16[128,2048]{1,0:T(8,128)(2,1)S(1)} %copy-done.1, bf16[128,2048]{1,0:T(8,128)(2,1)} %collective-permute-done.11.refs_4_, ...), custom_call_target="tpu_custom_call" | custom-call | flops 4194304 | bytes 4194304 | tf_op jit(solution)/shard_map/join/pallas_call | solution.py:482
  133.9 0.0 all-to-all-done.2.rx_ref
  133.9 7.3 %all-to-all-start.4 = ((bf16[16,256,128]{2,1,0:T(8,128)(2,1)}), bf16[16,256,128]{2,1,0:T(8,128)(2,1)S(1)}, u32[]{:S(2)}, u32[]{:S(2)}) async-start(bf16[16,256,128]{2,1,0:T(8,128)(2,1)} %join.1), calls=%async_computation.4 | async-start | bytes 2097152 | tf_op jit(solution)/shard_map/all_to_all | solution.py:302
  141.2 1.3 scan.3
  142.5 13.5 %all-to-all-done.4 = bf16[16,256,128]{2,1,0:T(8,128)(2,1)S(1)} async-done(((bf16[16,256,128]{2,1,0:T(8,128)(2,1)}), bf16[16,256,128]{2,1,0:T(8,128)(2,1)S(1)}, u32[]{:S(2)}, u32[]{:S(2)}) %all-to-all-start.4) | async-done | bytes 1048608 | tf_op jit(solution)/shard_map/all_to_all | solution.py:302
  156.0 4.9 %all-to-all-start.3 = ((bf16[16,256,128]{2,1,0:T(8,128)(2,1)}), bf16[16,256,128]{2,1,0:T(8,128)(2,1)S(1)}, u32[]{:S(2)}, u32[]{:S(2)}) async-start(bf16[16,256,128]{2,1,0:T(8,128)(2,1)} %scan.3), calls=%async_computation.3 | async-start | bytes 2097152 | tf_op jit(solution)/shard_map/all_to_all | solution.py:302
  160.9 9.7 %hidden_grad.1 = bf16[128,2,2048]{2,1,0:T(2,128)(2,1)} custom-call(s32[16]{0:T(128)} %fusion.2.order_ref, bf16[256,2048]{1,0:T(8,128)(2,1)} %value_grad.1.dv_ref, bf16[768,2048]{1,0:T(8,128)(2,1)} %constant_dynamic-update-slice_fusion.near_ref, bf16[768,2048]{1,0:T(8,128)(2,1)} %collective-permute-done.2.near_got_ref, bf16[256,2048]{1,0:T(8,128)(2,1)} %copy-done.3, ...), custom_call_target="tpu_custom_call" | custom-call | flops 2147483648 | bytes 10485760 | tf_op jit(solution)/shard_map/hidden_grad/pallas_call | solution.py:519
  170.6 0.8 convert_reduce_fusion
  171.4 4.0 %all-to-all-done.3 = bf16[16,256,128]{2,1,0:T(8,128)(2,1)S(1)} async-done(((bf16[16,256,128]{2,1,0:T(8,128)(2,1)}), bf16[16,256,128]{2,1,0:T(8,128)(2,1)S(1)}, u32[]{:S(2)}, u32[]{:S(2)}) %all-to-all-start.3) | async-done | bytes 1048608 | tf_op jit(solution)/shard_map/all_to_all | solution.py:302
  175.4 1.0 copy-done.4
  176.4 7.1 %final.1 = (bf16[128,2,1024]{2,1,0:T(2,128)(2,1)}, bf16[128,2,1024]{2,1,0:T(2,128)(2,1)}, bf16[128,2,1024]{2,1,0:T(2,128)(2,1)}) custom-call(bf16[128,2,1024]{2,1,0:T(2,128)(2,1)} %k_ref.3, bf16[128,2,1024]{2,1,0:T(2,128)(2,1)} %g_ref.5, f32[1,1024]{1,0:T(1,128)} %bitcast.12, f32[256,1024]{1,0:T(8,128)} %get-tuple-element.24.cum_ref, ...), custom_call_target="tpu_custom_call" | custom-call | flops 805306368 | bytes 10485760 | tf_op jit(solution)/shard_map/final/pallas_call | solution.py:539
  (19 shorter events, 0.1 us)
Async XLA Ops:
  0.6 26.4 %collective-permute-start = (bf16[256,2048]{1,0:T(8,128)(2,1)}, bf16[256,2048]{1,0:T(8,128)(2,1)S(1)}, u32[]{:S(2)}, u32[]{:S(2)}) collective-permute-start(bf16[256,2048]{1,0:T(8,128)(2,1)} %param.15), channel_id=1, source_target_pairs={{0,2},{1,3},{2,4},{3,5},{4,6},{5,7},{6,0},{7,1},{8,10},{9,11},{10,... | collective-permute-start | bytes 3145736 | tf_op jit(solution)/shard_map/ppermute | solution.py:325
  2.2 26.0 %collective-permute-start.1 = (bf16[256,2048]{1,0:T(8,128)(2,1)}, bf16[256,2048]{1,0:T(8,128)(2,1)S(1)}, u32[]{:S(2)}, u32[]{:S(2)}) collective-permute-start(bf16[256,2048]{1,0:T(8,128)(2,1)} %param.15), channel_id=1, source_target_pairs={{0,6},{1,7},{2,0},{3,1},{4,2},{5,3},{6,4},{7,5},{8,14},{9,15},{10,... | collective-permute-start | bytes 3145736 | tf_op jit(solution)/shard_map/ppermute | solution.py:325
  7.9 24.0 %all-to-all-start = ((bf16[16,264,128]{2,1,0:T(8,128)(2,1)}), bf16[16,264,128]{2,1,0:T(8,128)(2,1)S(1)}, u32[]{:S(2)}, u32[]{:S(2)}) async-start(bf16[16,264,128]{2,1,0:T(8,128)(2,1)} %bitcast.7), calls=%async_computation | async-start | bytes 2162688 | tf_op jit(solution)/shard_map/all_to_all | solution.py:302
  27.0 6.2 %copy-start.6 = (bf16[256,2048]{1,0:T(8,128)(2,1)}, bf16[256,2048]{1,0:T(8,128)(2,1)S(1)}, u32[]{:S(2)}) copy-start(bf16[256,2048]{1,0:T(8,128)(2,1)S(1)} %collective-permute-done) | copy-start | bytes 3145732
  29.3 72.2 %collective-permute-start.2 = (bf16[768,2048]{1,0:T(8,128)(2,1)}, bf16[768,2048]{1,0:T(8,128)(2,1)}, u32[]{:S(2)}, u32[]{:S(2)}) collective-permute-start(bf16[768,2048]{1,0:T(8,128)(2,1)} %constant_dynamic-update-slice_fusion.near_ref), channel_id=1, source_target_pairs={{0,1},{1,0},{2,3},{3,2},{4,5},{5,4},{6,7},{7,6},{8,9},{9,8},{10,11... | collective-permute-start | bytes 9437192 | tf_op jit(solution)/shard_map/ppermute | solution.py:328
  33.2 22.3 %all-to-all-start.1 = ((bf16[16,256,128]{2,1,0:T(8,128)(2,1)}), bf16[16,256,128]{2,1,0:T(8,128)(2,1)S(1)}, u32[]{:S(2)}, u32[]{:S(2)}) async-start(bf16[16,256,128]{2,1,0:T(8,128)(2,1)} %scan.2), calls=%async_computation.1 | async-start | bytes 2097152 | tf_op jit(solution)/shard_map/all_to_all | solution.py:302
  55.5 1.1 copy-start.2
  56.6 8.6 %copy-start.7 = (s32[16]{0:T(128)S(1)}, s32[16]{0:T(128)}, u32[]{:S(2)}) copy-start(s32[16]{0:T(128)} %constant.66) | copy-start | bytes 196
  56.6 8.6 %copy-start.8 = (s32[16]{0:T(128)S(1)}, s32[16]{0:T(128)}, u32[]{:S(2)}) copy-start(s32[16]{0:T(128)} %constant.60.clone) | copy-start | bytes 196
  56.6 8.6 %copy-start.9 = (s32[16]{0:T(128)S(1)}, s32[16]{0:T(128)}, u32[]{:S(2)}) copy-start(s32[16]{0:T(128)} %constant.59.clone) | copy-start | bytes 196
  56.6 8.6 %copy-start.10 = (s32[16]{0:T(128)S(1)}, s32[16]{0:T(128)}, u32[]{:S(2)}) copy-start(s32[16]{0:T(128)} %constant.58.clone) | copy-start | bytes 196
  60.0 18.3 %collective-permute-start.7 = (bf16[256,2048]{1,0:T(8,128)(2,1)}, bf16[256,2048]{1,0:T(8,128)(2,1)}, u32[]{:S(2)}, u32[]{:S(2)}) collective-permute-start(bf16[256,2048]{1,0:T(8,128)(2,1)} %value_grad.1.dv_ref), channel_id=1, source_target_pairs={{0,1},{1,0},{2,3},{3,2},{4,5},{5,4},{6,7},{7,6},{8,9},{9,8},{10,11... | collective-permute-start | bytes 3145736 | tf_op jit(solution)/shard_map/ppermute | solution.py:328
  61.1 15.6 %collective-permute-start.3 = (bf16[128,2048]{1,0:T(8,128)(2,1)S(1)}, bf16[128,2048]{1,0:T(8,128)(2,1)S(1)}, u32[]{:S(2)}, u32[]{:S(2)}) collective-permute-start(bf16[128,2048]{1,0:T(8,128)(2,1)S(1)} %slice.8), channel_id=1, source_target_pairs={{0,2},{1,3},{2,4},{3,5},{4,6},{5,7},{6,0},{7,1},{8,10},{9,11},{10,... | collective-permute-start | bytes 1572872 | tf_op jit(solution)/shard_map/ppermute | solution.py:325
  62.3 14.8 %collective-permute-start.4 = (bf16[128,2048]{1,0:T(8,128)(2,1)}, bf16[128,2048]{1,0:T(8,128)(2,1)}, u32[]{:S(2)}, u32[]{:S(2)}) collective-permute-start(bf16[128,2048]{1,0:T(8,128)(2,1)} %slice.9), channel_id=1, source_target_pairs={{0,6},{1,7},{2,0},{3,1},{4,2},{5,3},{6,4},{7,5},{8,14},{9,15},{10,... | collective-permute-start | bytes 1572872 | tf_op jit(solution)/shard_map/ppermute | solution.py:325
  69.6 8.7 %collective-permute-start.6 = (bf16[128,2,1024]{2,1,0:T(2,128)(2,1)}, bf16[128,2,1024]{2,1,0:T(2,128)(2,1)}, u32[]{:S(2)}, u32[]{:S(2)}) collective-permute-start(bf16[128,2,1024]{2,1,0:T(2,128)(2,1)} %pick.1), channel_id=1, source_target_pairs={{0,1},{1,0},{2,3},{3,2},{4,5},{5,4},{6,7},{7,6},{8,9},{9,8},{10,11... | collective-permute-start | bytes 1572872 | tf_op jit(solution)/shard_map/ppermute | solution.py:328
  78.2 14.4 %copy-start.3 = (bf16[256,2048]{1,0:T(8,128)(2,1)}, bf16[256,2048]{1,0:T(8,128)(2,1)S(1)}, u32[]{:S(2)}) copy-start(bf16[256,2048]{1,0:T(8,128)(2,1)S(1)} %constant_dynamic-update-slice_fusion.3.far_ref) | copy-start | bytes 3145732
  78.2 22.6 %collective-permute-start.5 = (bf16[256,2048]{1,0:T(8,128)(2,1)S(1)}, bf16[256,2048]{1,0:T(8,128)(2,1)S(1)}, u32[]{:S(2)}, u32[]{:S(2)}) collective-permute-start(bf16[256,2048]{1,0:T(8,128)(2,1)S(1)} %constant_dynamic-update-slice_fusion.3.far_ref), channel_id=1, source_target_pairs={{0,1},{1,0},{2,3},{3,2},{4,5},{5,4},{6,7},{7,6},{8,9},{9,8},{10,11... | collective-permute-start | bytes 3145736 | tf_op jit(solution)/shard_map/ppermute | solution.py:328
  82.1 16.6 %collective-permute-start.8 = (bf16[128,2048]{1,0:T(8,128)(2,1)}, bf16[128,2048]{1,0:T(8,128)(2,1)}, u32[]{:S(2)}, u32[]{:S(2)}) collective-permute-start(bf16[128,2048]{1,0:T(8,128)(2,1)} %get-tuple-element.33), channel_id=1, source_target_pairs={{0,2},{1,3},{2,4},{3,5},{4,6},{5,7},{6,0},{7,1},{8,10},{9,11},{10,... | collective-permute-start | bytes 1572872 | tf_op jit(solution)/shard_map/ppermute | solution.py:325
  83.1 32.6 %collective-permute-start.12 = (bf16[128,2048]{1,0:T(8,128)(2,1)}, bf16[128,2048]{1,0:T(8,128)(2,1)}, u32[]{:S(2)}, u32[]{:S(2)}) collective-permute-start(bf16[128,2048]{1,0:T(8,128)(2,1)} %get-tuple-element.38), channel_id=1, source_target_pairs={{0,6},{1,7},{2,0},{3,1},{4,2},{5,3},{6,4},{7,5},{8,14},{9,15},{10,... | collective-permute-start | bytes 1572872 | tf_op jit(solution)/shard_map/ppermute | solution.py:325
  92.6 27.8 %collective-permute-start.10 = (bf16[128,2048]{1,0:T(8,128)(2,1)}, bf16[128,2048]{1,0:T(8,128)(2,1)}, u32[]{:S(2)}, u32[]{:S(2)}) collective-permute-start(bf16[128,2048]{1,0:T(8,128)(2,1)} %get-tuple-element.34), channel_id=1, source_target_pairs={{0,6},{1,7},{2,0},{3,1},{4,2},{5,3},{6,4},{7,5},{8,14},{9,15},{10,... | collective-permute-start | bytes 1572872 | tf_op jit(solution)/shard_map/ppermute | solution.py:325
  98.6 21.7 %collective-permute-start.11 = (bf16[128,2048]{1,0:T(8,128)(2,1)}, bf16[128,2048]{1,0:T(8,128)(2,1)}, u32[]{:S(2)}, u32[]{:S(2)}) collective-permute-start(bf16[128,2048]{1,0:T(8,128)(2,1)} %get-tuple-element.36), channel_id=1, source_target_pairs={{0,2},{1,3},{2,4},{3,5},{4,6},{5,7},{6,0},{7,1},{8,10},{9,11},{10,... | collective-permute-start | bytes 1572872 | tf_op jit(solution)/shard_map/ppermute | solution.py:325
  100.7 1.0 copy-start.5
  100.7 24.4 %collective-permute-start.9 = (bf16[128,2048]{1,0:T(8,128)(2,1)}, bf16[128,2048]{1,0:T(8,128)(2,1)}, u32[]{:S(2)}, u32[]{:S(2)}) collective-permute-start(bf16[128,2048]{1,0:T(8,128)(2,1)} %add_convert_fusion.1), channel_id=1, source_target_pairs={{0,2},{1,3},{2,4},{3,5},{4,6},{5,7},{6,0},{7,1},{8,10},{9,11},{10,... | collective-permute-start | bytes 1572872 | tf_op jit(solution)/shard_map/ppermute | solution.py:325
  109.9 21.2 %copy-start = (bf16[128,2048]{1,0:T(8,128)(2,1)S(1)}, bf16[128,2048]{1,0:T(8,128)(2,1)}, u32[]{:S(2)}) copy-start(bf16[128,2048]{1,0:T(8,128)(2,1)} %get-tuple-element.31.refs_0_) | copy-start | bytes 1572868
  109.9 21.2 %copy-start.1 = (bf16[128,2048]{1,0:T(8,128)(2,1)S(1)}, bf16[128,2048]{1,0:T(8,128)(2,1)}, u32[]{:S(2)}) copy-start(bf16[128,2048]{1,0:T(8,128)(2,1)} %get-tuple-element.35.refs_3_) | copy-start | bytes 1572868
  109.9 24.0 %all-to-all-start.2 = ((bf16[16,256,128]{2,1,0:T(8,128)(2,1)}), bf16[16,256,128]{2,1,0:T(8,128)(2,1)S(1)}, u32[]{:S(2)}, u32[]{:S(2)}) async-start(bf16[16,256,128]{2,1,0:T(8,128)(2,1)} %bitcast.9), calls=%async_computation.2 | async-start | bytes 2097152 | tf_op jit(solution)/shard_map/all_to_all | solution.py:302
  117.0 14.0 %collective-permute-start.13 = (bf16[128,2048]{1,0:T(8,128)(2,1)S(1)}, bf16[128,2048]{1,0:T(8,128)(2,1)S(1)}, u32[]{:S(2)}, u32[]{:S(2)}) collective-permute-start(bf16[128,2048]{1,0:T(8,128)(2,1)S(1)} %add_convert_fusion), channel_id=1, source_target_pairs={{0,6},{1,7},{2,0},{3,1},{4,2},{5,3},{6,4},{7,5},{8,14},{9,15},{10,... | collective-permute-start | bytes 1572872 | tf_op jit(solution)/shard_map/ppermute | solution.py:325
  133.9 22.1 %all-to-all-start.4 = ((bf16[16,256,128]{2,1,0:T(8,128)(2,1)}), bf16[16,256,128]{2,1,0:T(8,128)(2,1)S(1)}, u32[]{:S(2)}, u32[]{:S(2)}) async-start(bf16[16,256,128]{2,1,0:T(8,128)(2,1)} %join.1), calls=%async_computation.4 | async-start | bytes 2097152 | tf_op jit(solution)/shard_map/all_to_all | solution.py:302
  156.0 19.4 %all-to-all-start.3 = ((bf16[16,256,128]{2,1,0:T(8,128)(2,1)}), bf16[16,256,128]{2,1,0:T(8,128)(2,1)S(1)}, u32[]{:S(2)}, u32[]{:S(2)}) async-start(bf16[16,256,128]{2,1,0:T(8,128)(2,1)} %scan.3), calls=%async_computation.3 | async-start | bytes 2097152 | tf_op jit(solution)/shard_map/all_to_all | solution.py:302
  175.4 1.0 copy-start.4

commit v5 on v4

--- a/solution.py
+++ b/solution.py
@@ -160,10 +160,6 @@
         dv_ref[:, vals] = (intra + inter).astype(BF16)
 
 
-def pick_kernel(order_ref, h_ref, out_ref):
-    out_ref[...] = h_ref[...]
-
-
 def part_kernel(order_ref, h_ref, got_ref, dv_ref, dv_got_ref, top_ref, bottom_ref):
     cols = slice(0, h_ref.shape[2])
     part = dot(native(h_ref, cols), dv_ref[...], TN)
@@ -200,26 +196,30 @@
     join_kernel(refs[:3], refs[3:6], refs[6])
 
 
-def project_kernel(
-    order_ref, h_ref, near_ref, near_got_ref, far_ref, far_got_ref, k_dec_ref,
-    v_ref, delta_ref, held,
-):
-    first = first_rows(DK)
-    shard = far_ref.shape[0]
+def hold(order_ref, h_ref, held, base):
+    shard = h_ref.shape[2] // 8
 
     @pl.when(pl.program_id(0) == 0)
     def _():
         for p in range(held.shape[1] // shard):
-            start = pl.multiple_of(order_ref[p] * shard, shard)
+            start = pl.multiple_of(order_ref[base + p] * shard, shard)
             cols = h_ref[:, :, pl.ds(start, shard)].reshape(ROWS, shard)
             held[:, p * shard : (p + 1) * shard] = cols
 
-    v_all = jnp.zeros(v_ref.shape, F32)
-    start = 0
-    for ref in (near_ref, near_got_ref, far_ref, far_got_ref):
-        v_all += dot(held[:, start : start + ref.shape[0]], ref[...], NN)
-        start += ref.shape[0]
-    v_all = v_all.astype(BF16)
+
+def near_kernel(order_ref, h_ref, *refs):
+    *pieces, sum_ref, held = refs
+    hold(order_ref, h_ref, held, 0)
+    weight = jnp.concatenate([ref[...] for ref in pieces], axis=0)
+    sum_ref[...] = dot(held[...], weight, NN)
+
+
+def project_kernel(order_ref, h_ref, sum_ref, k_dec_ref, *refs):
+    *pieces, v_ref, delta_ref, held = refs
+    first = first_rows(DK)
+    hold(order_ref, h_ref, held, 6)
+    weight = jnp.concatenate([ref[...] for ref in pieces], axis=0)
+    v_all = (sum_ref[...] + dot(held[...], weight, NN)).astype(BF16)
     v_ref[...] = v_all
     for j in range(PAIR):
         keys, vals = head_slices(j)
@@ -228,19 +228,28 @@
             delta_ref[s, j] = delta[:, s * DK : (s + 1) * DK].astype(BF16)
 
 
-def hidden_grad_kernel(
-    order_ref, dv_ref, near_ref, near_got_ref, far_ref, far_got_ref, out_ref
-):
-    p = pl.program_id(0)
-
-    def emit(ref):
-        grad = dot(dv_ref[...], ref[...], NT).astype(BF16)
-        out_ref[...] = grad.reshape(out_ref.shape)
-
-    pl.when(p < 3)(lambda: emit(near_ref))
-    pl.when((p >= 3) & (p < 6))(lambda: emit(near_got_ref))
-    pl.when(p == 6)(lambda: emit(far_ref))
-    pl.when(p == 7)(lambda: emit(far_got_ref))
+def hidden_grad_kernel(order_ref, dv_ref, *refs):
+    *pieces, out_ref = refs
+    shard = out_ref.shape[2] // 2
+    core = order_ref[0] % 2
+
+    def emit(side, weight):
+        grad = dot(dv_ref[...], weight, NT).astype(BF16)
+        start = pl.multiple_of(side * shard, shard)
+        out_ref[:, :, pl.ds(start, shard)] = grad.reshape(BLK, SEQS, shard)
+
+    groups = (
+        ((0,), (5,)),
+        ((1, 2), (6, 7)),
+        ((3, 4), (8, 9)),
+        ((10, 11), (12, 13)),
+    )
+    for k, (mine, got) in enumerate(groups):
+
+        @pl.when(pl.program_id(0) == k)
+        def _():
+            emit(core, jnp.concatenate([pieces[n][...] for n in mine], axis=0))
+            emit(1 - core, jnp.concatenate([pieces[n][...] for n in got], axis=0))
 
 
 def final_kernel(
@@ -328,14 +337,19 @@
         return lax.ppermute(value, "dp", [(d, d ^ 1) for d in range(group)])
 
     half = shard // 2
-    before = along(value_weight, 1)
-    after = along(value_weight, -1)
-    far_one = along(before[:half], 1)
-    far_two = along(after[half:], -1)
-    far = jnp.concatenate([far_one, far_two], axis=0)
-    near = jnp.concatenate([value_weight, before, after], axis=0)
-    near_got = swap(near)
-    far_got = swap(far)
+    top, bottom = value_weight[:half], value_weight[half:]
+
+    before_top = along(top, 1)
+    after_bottom = along(bottom, -1)
+    before_bottom = along(bottom, 1)
+    after_top = along(top, -1)
+    far_one = along(before_top, 1)
+    far_two = along(after_bottom, -1)
+
+    near = [value_weight, before_top, before_bottom, after_top, after_bottom]
+    near += [swap(value) for value in near]
+    far = [far_one, far_two]
+    far += [swap(far_one), swap(far_two)]
     items = sequences * HEADS
     values = HEADS * DV
     bias = decay_bias.reshape(1, HEADS * DK)
@@ -383,21 +397,7 @@
         name="intra",
     )(query_act, key_act, gate_act, bias)
 
-    raw = (BLK, SEQS, shard)
-    given = pl.pallas_call(
-        pick_kernel,
-        grid_spec=pltpu.PrefetchScalarGridSpec(
-            num_scalar_prefetch=1,
-            grid=(chips,),
-            in_specs=[pl.BlockSpec(raw, lambda i, o: (0, 0, 2 * i + o[3] % 2))],
-            out_specs=pl.BlockSpec(raw, lambda i, o: (0, 0, i)),
-        ),
-        out_shape=shaped((BLK, SEQS, width // 2)),
-        compiler_params=params(),
-        cost_estimate=cost(1 << 22, 1 << 20),
-        name="pick",
-    )(order, hidden_in)
-    got = swap(given)
+    got = swap(hidden_in)
 
     def scan(arrived, reverse):
         return pl.pallas_call(
@@ -434,7 +434,7 @@
                 grid=(turns,),
                 in_specs=[
                     pl.BlockSpec(raw, lambda i, o: (0, 0, o[8])),
-                    pl.BlockSpec(raw, lambda i, o: (0, 0, o[12])),
+                    pl.BlockSpec(raw, lambda i, o: (0, 0, o[8])),
                     pl.BlockSpec((ROWS, values // turns), lambda i, o: (0, i)),
                     pl.BlockSpec((ROWS, values // turns), lambda i, o: (0, i)),
                 ],
@@ -455,7 +455,7 @@
                 grid=(3,),
                 in_specs=[
                     pl.BlockSpec(raw, lambda i, o: (0, 0, o[9 + i])),
-                    pl.BlockSpec(raw, lambda i, o: (0, 0, o[13 + i])),
+                    pl.BlockSpec(raw, lambda i, o: (0, 0, o[9 + i])),
                     whole,
                     whole,
                 ],
@@ -487,54 +487,68 @@
         name="join",
     )(own_top, late_before, ready_after, own_bottom, ready_before, late_after)
 
+    hidden_spec = pl.BlockSpec((BLK, SEQS, width), lambda i, o: (0, 0, 0))
+    wide = pl.BlockSpec((ROWS, PAIR * DV), lambda i, o: (0, i))
+    near_spec = pl.BlockSpec((shard, PAIR * DV), lambda i, o: (0, i))
+    far_spec = pl.BlockSpec((half, PAIR * DV), lambda i, o: (0, i))
+    near_sum = pl.pallas_call(
+        near_kernel,
+        grid_spec=pltpu.PrefetchScalarGridSpec(
+            num_scalar_prefetch=1,
+            grid=(STEPS,),
+            in_specs=[hidden_spec] + ([near_spec] + [far_spec] * 4) * 2,
+            out_specs=wide,
+            scratch_shapes=[pltpu.VMEM((ROWS, 6 * shard), BF16)],
+        ),
+        out_shape=shaped(val_shape, F32),
+        compiler_params=params(),
+        cost_estimate=cost(3 * big // 4, 10 << 20),
+        name="project_near",
+    )(order, hidden_in, *near)
+
     v, vdelta = pl.pallas_call(
         project_kernel,
         grid_spec=pltpu.PrefetchScalarGridSpec(
             num_scalar_prefetch=1,
             grid=(STEPS,),
             in_specs=[
-                pl.BlockSpec((BLK, SEQS, width), lambda i, o: (0, 0, 0)),
-                pl.BlockSpec((3 * shard, PAIR * DV), lambda i, o: (0, i)),
-                pl.BlockSpec((3 * shard, PAIR * DV), lambda i, o: (0, i)),
-                pl.BlockSpec((shard, PAIR * DV), lambda i, o: (0, i)),
-                pl.BlockSpec((shard, PAIR * DV), lambda i, o: (0, i)),
+                hidden_spec,
+                wide,
                 pl.BlockSpec((ROWS, PAIR * DK), lambda i, o: (0, i)),
-            ],
+            ]
+            + [far_spec] * 4,
             out_specs=[
-                pl.BlockSpec((ROWS, PAIR * DV), lambda i, o: (0, i)),
+                wide,
                 pl.BlockSpec((SEQS, PAIR, DV, DK), lambda i, o: (0, i, 0, 0)),
             ],
-            scratch_shapes=[pltpu.VMEM((ROWS, width), BF16)],
+            scratch_shapes=[pltpu.VMEM((ROWS, 2 * shard), BF16)],
         ),
         out_shape=[shaped(val_shape), shaped(state_shape)],
         compiler_params=params(),
-        cost_estimate=cost(big + mm, 12 << 20),
+        cost_estimate=cost(big // 4 + mm, 7 << 20),
         name="project",
-    )(order, hidden_in, near, near_got, far, far_got, k_dec)
+    )(order, hidden_in, near_sum, k_dec, *far)
 
     vrx = over_sp(vdelta.reshape(items, DV, DK))
     state = over_sp(scan(vrx, False)).reshape(state_shape)
 
-    block = (shard, values)
+    whole = pl.BlockSpec((shard, values), lambda i, o: (0, 0))
+    part_whole = pl.BlockSpec((half, values), lambda i, o: (0, 0))
     hidden_grad = pl.pallas_call(
         hidden_grad_kernel,
         grid_spec=pltpu.PrefetchScalarGridSpec(
             num_scalar_prefetch=1,
-            grid=(group,),
-            in_specs=[
-                pl.BlockSpec(val_shape, lambda i, o: (0, 0)),
-                pl.BlockSpec(block, lambda i, o: (jnp.minimum(i, 2), 0)),
-                pl.BlockSpec(block, lambda i, o: (jnp.clip(i - 3, 0, 2), 0)),
-                pl.BlockSpec(block, lambda i, o: (0, 0)),
-                pl.BlockSpec(block, lambda i, o: (0, 0)),
-            ],
-            out_specs=pl.BlockSpec((BLK, SEQS, shard), lambda i, o: (0, 0, o[i])),
+            grid=(chips,),
+            in_specs=[pl.BlockSpec(val_shape, lambda i, o: (0, 0))]
+            + ([whole] + [part_whole] * 4) * 2
+            + [part_whole] * 4,
+            out_specs=pl.BlockSpec((BLK, SEQS, 2 * shard), lambda i, o: (0, 0, o[15 - i])),
         ),
         out_shape=shaped((BLK, SEQS, width)),
         compiler_params=params(),
         cost_estimate=cost(big, 10 << 20),
         name="hidden_grad",
-    )(order, dv, near, near_got, far, far_got)
+    )(order, dv, *near, *far)
 
     dq, dk, dg = pl.pallas_call(
         final_kernel,

time: 187 us -> 172 us (0.920)
  local copies, waits for them, and re-layouts: 10 us -> 2.07 us
  waiting for transfers between devices: 62.9 us -> 56.6 us
  starting transfers between devices: 48.7 us -> 52.9 us
  Pallas kernels: 56.3 us -> 54.2 us
    all_to_all x5, waiting for transfers between devices: 32.3 us -> 22 us  [over_sp(): return lax.all_to_all(value, 'sp', split_axis=0, concat_axis=0, tiled=True)]
    unnamed x25 -> x20, local copies, waits for them, and re-layouts: 5.98 us -> 1.03 us
    ppermute x10 -> x12, waiting for transfers between devices: 30.7 us -> 34.6 us  [along(): return lax.ppermute(value, 'dp', pairs)]
    pallas_call x1, Pallas kernels: 3.83 us -> 6.74 us  [arranged(): pl.pallas_call(near_kernel, grid_spec=pltpu.PrefetchScalarGridSpec(num_sc...]
    pallas_call x1, Pallas kernels: 8.1 us -> 5.54 us  [arranged(): pl.pallas_call(project_kernel, grid_spec=pltpu.PrefetchScalarGridSpec(num...]
    concatenate x2 -> x0, local copies, waits for them, and re-layouts: 2.14 us -> none  [the longest x1 1.08 us: arranged(): far = jnp.concatenate([far_one, far_two], axis=0)]
    ppermute x10 -> x12, starting transfers between devices: 16.3 us -> 17.4 us  [along(): return lax.ppermute(value, 'dp', pairs)]
  transfers between devices with their start and end apart: 19 -> 26, of which waited for: 10 -> 8; matrix products, arithmetic and copies ran while one was open for 7% -> 2% of each run, Pallas kernels for 27% -> 29%
where the time goes in v5:
time: 172 us; the launch traced here: 170 us
  waiting for transfers between devices  56.6 us (33%)
  Pallas kernels  54.2 us (32%)
  starting transfers between devices  52.9 us (31%)
  other arithmetic  3.66 us (2%)
  local copies, waits for them, and re-layouts  2.07 us (1%)
    ppermute x12, waiting for transfers between devices, along(): return lax.ppermute(value, 'dp', pairs)  34.6 us
    all_to_all x5, starting transfers between devices, over_sp(): return lax.all_to_all(value, 'sp', split_axis=0, concat_axis=0, tiled=True)  33.6 us
    all_to_all x5, waiting for transfers between devices, over_sp(): return lax.all_to_all(value, 'sp', split_axis=0, concat_axis=0, tiled=True)  22 us
    ppermute x12, starting transfers between devices, along(): return lax.ppermute(value, 'dp', pairs)  17.4 us
    pallas_call x1, Pallas kernels, arranged(): pl.pallas_call(hidden_grad_kernel, grid_spec=pltpu.PrefetchScalarGridSpec...  8.48 us
    pallas_call x1, Pallas kernels, arranged(): pl.pallas_call(final_kernel, grid=(STEPS,), in_specs=[raw_key, raw_key, b...  7.14 us
    pallas_call x1, Pallas kernels, rest(): pl.pallas_call(rest_kernel, grid_spec=pltpu.PrefetchScalarGridSpec(num_sc...  6.78 us
    pallas_call x1, Pallas kernels, arranged(): pl.pallas_call(near_kernel, grid_spec=pltpu.PrefetchScalarGridSpec(num_sc...  6.74 us
  transfers between devices with their start and end apart: 26, of which 8 were waited for; matrix products, arithmetic and copies ran while one was open for 2% of the time, Pallas kernels for 29%

profile of v5, /device:TPU:8, one launch (start us, length us, event | category | flops | bytes accessed | tf_op | source)
XLA Modules:
  0.0 170.2 jit_solution(11023289831122092671)
XLA Ops:
  0.6 0.0 copy-start.3
  0.6 4.0 %decay.1 = bf16[2,8,264,128]{3,2,1,0:T(8,128)(2,1)} custom-call(bf16[128,2,1024]{2,1,0:T(2,128)(2,1)} %q_ref.3, bf16[128,2,1024]{2,1,0:T(2,128)(2,1)} %g_ref.5, f32[1,1024]{1,0:T(1,128)} %bitcast.10, bf16[128,2,2048]{2,1,0:T(2,128)(2,1)} %do_ref.5), custom_call_target="tpu_custom_call" | custom-call | flops 402653184 | bytes 4194304 | tf_op jit(solution)/shard_map/decay/pallas_call | solution.py:371
  4.7 8.4 %all-to-all-start = ((bf16[16,264,128]{2,1,0:T(8,128)(2,1)}), bf16[16,264,128]{2,1,0:T(8,128)(2,1)S(1)}, u32[]{:S(2)}, u32[]{:S(2)}) async-start(bf16[16,264,128]{2,1,0:T(8,128)(2,1)} %bitcast.7), calls=%async_computation | async-start | bytes 2162688 | tf_op jit(solution)/shard_map/all_to_all | solution.py:311
  13.1 0.1 collective-permute-start.4
  13.2 1.0 fusion.5
  14.2 1.5 collective-permute-start
  15.7 1.5 collective-permute-start.1
  17.2 1.7 %collective-permute-start.3 = (bf16[128,2048]{1,0:T(8,128)(2,1)}, bf16[128,2048]{1,0:T(8,128)(2,1)}, u32[]{:S(2)}, u32[]{:S(2)}) collective-permute-start(bf16[128,2048]{1,0:T(8,128)(2,1)} %get-tuple-element.39), channel_id=1, source_target_pairs={{0,6},{1,7},{2,0},{3,1},{4,2},{5,3},{6,4},{7,5},{8,14},{9,15},{10,... | collective-permute-start | bytes 1572872 | tf_op jit(solution)/shard_map/ppermute | solution.py:334
  18.9 0.5 collective-permute-start.2
  19.5 9.7 %all-to-all-done.rx_ref.last_ref = bf16[16,264,128]{2,1,0:T(8,128)(2,1)S(1)} async-done(((bf16[16,264,128]{2,1,0:T(8,128)(2,1)}), bf16[16,264,128]{2,1,0:T(8,128)(2,1)S(1)}, u32[]{:S(2)}, u32[]{:S(2)}) %all-to-all-start) | async-done | bytes 1081376 | tf_op jit(solution)/shard_map/all_to_all | solution.py:311
  29.2 1.3 scan.2
  30.5 5.5 %all-to-all-start.1 = ((bf16[16,256,128]{2,1,0:T(8,128)(2,1)}), bf16[16,256,128]{2,1,0:T(8,128)(2,1)S(1)}, u32[]{:S(2)}, u32[]{:S(2)}) async-start(bf16[16,256,128]{2,1,0:T(8,128)(2,1)} %scan.2), calls=%async_computation.1 | async-start | bytes 2097152 | tf_op jit(solution)/shard_map/all_to_all | solution.py:311
  36.0 0.0 collective-permute-done.refs_1_
  36.0 0.1 collective-permute-start.5
  36.1 5.2 %collective-permute-done.1.refs_2_ = bf16[128,2048]{1,0:T(8,128)(2,1)} collective-permute-done((bf16[128,2048]{1,0:T(8,128)(2,1)}, bf16[128,2048]{1,0:T(8,128)(2,1)}, u32[]{:S(2)}, u32[]{:S(2)}) %collective-permute-start.1) | collective-permute-done | bytes 524320 | tf_op jit(solution)/shard_map/ppermute | solution.py:334
  41.3 0.3 collective-permute-start.9
  41.6 3.0 %collective-permute-start.10 = (bf16[128,2048]{1,0:T(8,128)(2,1)}, bf16[128,2048]{1,0:T(8,128)(2,1)}, u32[]{:S(2)}, u32[]{:S(2)}) collective-permute-start(bf16[128,2048]{1,0:T(8,128)(2,1)} %collective-permute-done.3.refs_4_), channel_id=1, source_target_pairs={{0,6},{1,7},{2,0},{3,1},{4,2},{5,3},{6,4},{7,5},{8,14},{9,15},{10,... | collective-permute-start | bytes 1572872 | tf_op jit(solution)/shard_map/ppermute | solution.py:334
  44.5 0.0 collective-permute-done.2.refs_3_
  44.5 0.0 collective-permute-start.6
  44.5 0.0 collective-permute-done.4.refs_5_
  44.5 0.5 collective-permute-start.7
  45.0 0.1 collective-permute-start.8
  45.1 11.1 %collective-permute-done.9.refs_10_.refs_0_ = bf16[128,2048]{1,0:T(8,128)(2,1)} collective-permute-done((bf16[128,2048]{1,0:T(8,128)(2,1)}, bf16[128,2048]{1,0:T(8,128)(2,1)}, u32[]{:S(2)}, u32[]{:S(2)}) %collective-permute-start.9) | collective-permute-done | bytes 524320 | tf_op jit(solution)/shard_map/ppermute | solution.py:334
  56.3 0.0 collective-permute-start.11
  56.3 0.0 collective-permute-done.10.refs_11_.refs_1_
  56.3 0.5 collective-permute-start.12
  56.8 4.3 %intra.1 = (f32[256,1024]{1,0:T(8,128)}, bf16[256,1024]{1,0:T(8,128)(2,1)}, bf16[8,256,256]{2,1,0:T(8,128)(2,1)}, bf16[256,1024]{1,0:T(8,128)(2,1)}) custom-call(bf16[128,2,1024]{2,1,0:T(2,128)(2,1)} %q_ref.3, bf16[128,2,1024]{2,1,0:T(2,128)(2,1)} %k_ref.3, bf16[128,2,1024]{2,1,0:T(2,128)(2,1)} %g_ref.5, f32[1,1024]{1,0:T(1,128)} %bitcast.11), custom_call_target="tpu_custom_call" | custom-call | flops 402653184 | bytes 5242880 | tf_op jit(solution)/shard_map/intra/pallas_call | solution.py:384
  61.1 1.0 copy-done.4
  62.1 0.0 copy-start.9
  62.1 3.4 %value_grad.1.dv_ref = bf16[256,2048]{1,0:T(8,128)(2,1)} custom-call(bf16[8,256,256]{2,1,0:T(8,128)(2,1)} %get-tuple-element.22.scores_ref, bf16[128,2,2048]{2,1,0:T(2,128)(2,1)} %do_ref.5, bf16[256,1024]{1,0:T(8,128)(2,1)} %get-tuple-element.23.k_dec_ref, bf16[2,8,256,128]{3,2,1,0:T(8,128)(2,1)} %bitcast.5), custom_call_target="tpu_custom_call" | custom-call | flops 402653184 | bytes 5242880 | tf_op jit(solution)/shard_map/value_grad/pallas_call | solution.py:414
  65.5 0.0 collective-permute-done.6.refs_7_
  65.5 0.1 collective-permute-start.13
  65.6 0.5 collective-permute-start.14
  66.1 0.5 fusion.2.order_ref
  66.7 0.0 collective-permute-done.8.refs_9_
  66.7 6.7 %project_near.1.sum_ref = f32[256,2048]{1,0:T(8,128)} custom-call(s32[16]{0:T(128)} %fusion.2.order_ref, bf16[128,2,2048]{2,1,0:T(2,128)(2,1)} %h_ref.7, bf16[256,2048]{1,0:T(8,128)(2,1)} %refs_0_.3, bf16[128,2048]{1,0:T(8,128)(2,1)} %collective-permute-done.refs_1_, bf16[128,2048]{1,0:T(8,128)(2,1)} %collective-permute-done.1.refs_2_, ...), custom_call_target="tpu_custom_call" | custom-call | flops 1610612736 | bytes 10485760 | tf_op jit(solution)/shard_map/project_near/pallas_call | solution.py:494
  73.4 0.0 collective-permute-done.11.refs_12_.refs_2_
  73.4 5.5 %project.1 = (bf16[256,2048]{1,0:T(8,128)(2,1)}, bf16[2,8,256,128]{3,2,1,0:T(8,128)(2,1)}) custom-call(s32[16]{0:T(128)} %fusion.2.order_ref, bf16[128,2,2048]{2,1,0:T(2,128)(2,1)} %h_ref.7, f32[256,2048]{1,0:T(8,128)} %project_near.1.sum_ref, bf16[256,1024]{1,0:T(8,128)(2,1)} %get-tuple-element.23.k_dec_ref, ...), custom_call_target="tpu_custom_call" | custom-call | flops 671088640 | bytes 7340032 | tf_op jit(solution)/shard_map/project/pallas_call | solution.py:509
  79.0 7.2 %all-to-all-start.2 = ((bf16[16,256,128]{2,1,0:T(8,128)(2,1)}), bf16[16,256,128]{2,1,0:T(8,128)(2,1)S(1)}, u32[]{:S(2)}, u32[]{:S(2)}) async-start(bf16[16,256,128]{2,1,0:T(8,128)(2,1)} %bitcast.9), calls=%async_computation.2 | async-start | bytes 2097152 | tf_op jit(solution)/shard_map/all_to_all | solution.py:311
  86.2 0.0 collective-permute-done.14.dv_got_ref
  86.2 3.8 %shard_map.137 = (bf16[128,2048]{1,0:T(8,128)(2,1)}, bf16[128,2048]{1,0:T(8,128)(2,1)}) custom-call(s32[16]{0:T(128)} %fusion.2.order_ref, bf16[128,2,2048]{2,1,0:T(2,128)(2,1)} %h_ref.7, bf16[128,2,2048]{2,1,0:T(2,128)(2,1)} %collective-permute-done.13.got_ref, bf16[256,2048]{1,0:T(8,128)(2,1)} %value_grad.1.dv_ref, ...), custom_call_target="tpu_custom_call" | custom-call | flops 536870912 | bytes 5242880 | tf_op jit(solution)/shard_map/pallas_call | solution.py:430
  90.0 12.3 %all-to-all-done.2.rx_ref = bf16[16,256,128]{2,1,0:T(8,128)(2,1)S(1)} async-done(((bf16[16,256,128]{2,1,0:T(8,128)(2,1)}), bf16[16,256,128]{2,1,0:T(8,128)(2,1)S(1)}, u32[]{:S(2)}, u32[]{:S(2)}) %all-to-all-start.2) | async-done | bytes 1048608 | tf_op jit(solution)/shard_map/all_to_all | solution.py:311
  102.3 1.3 scan.3
  103.5 5.3 %all-to-all-start.3 = ((bf16[16,256,128]{2,1,0:T(8,128)(2,1)}), bf16[16,256,128]{2,1,0:T(8,128)(2,1)S(1)}, u32[]{:S(2)}, u32[]{:S(2)}) async-start(bf16[16,256,128]{2,1,0:T(8,128)(2,1)} %scan.3), calls=%async_computation.3 | async-start | bytes 2097152 | tf_op jit(solution)/shard_map/all_to_all | solution.py:311
  108.8 3.1 %collective-permute-start.19 = (bf16[128,2048]{1,0:T(8,128)(2,1)}, bf16[128,2048]{1,0:T(8,128)(2,1)S(1)}, u32[]{:S(2)}, u32[]{:S(2)}) collective-permute-start(bf16[128,2048]{1,0:T(8,128)(2,1)} %get-tuple-element.38), channel_id=1, source_target_pairs={{0,6},{1,7},{2,0},{3,1},{4,2},{5,3},{6,4},{7,5},{8,14},{9,15},{10,... | collective-permute-start | bytes 1572872 | tf_op jit(solution)/shard_map/ppermute | solution.py:334
  111.9 6.8 %part_rest.1 = (bf16[128,2048]{1,0:T(8,128)(2,1)}, bf16[128,2048]{1,0:T(8,128)(2,1)}, bf16[128,2048]{1,0:T(8,128)(2,1)}, bf16[128,2048]{1,0:T(8,128)(2,1)}, bf16...) custom-call(s32[16]{0:T(128)} %fusion.2.order_ref, bf16[128,2,2048]{2,1,0:T(2,128)(2,1)} %h_ref.7, ...), custom_call_target="tpu_custom_call" | custom-call | flops 1610612736 | bytes 8388608 | tf_op jit(solution)/shard_map/part_rest/pallas_call | solution.py:451
  118.7 0.1 collective-permute-start.17
  118.7 2.0 %collective-permute-start.18 = (bf16[128,2048]{1,0:T(8,128)(2,1)}, bf16[128,2048]{1,0:T(8,128)(2,1)S(1)}, u32[]{:S(2)}, u32[]{:S(2)}) collective-permute-start(bf16[128,2048]{1,0:T(8,128)(2,1)} %get-tuple-element.36), channel_id=1, source_target_pairs={{0,2},{1,3},{2,4},{3,5},{4,6},{5,7},{6,0},{7,1},{8,10},{9,11},{10,... | collective-permute-start | bytes 1572872 | tf_op jit(solution)/shard_map/ppermute | solution.py:334
  120.8 0.0 collective-permute-done.15
  120.8 1.2 add_convert_fusion.1
  121.9 0.1 collective-permute-start.16
  122.0 2.5 %collective-permute-done.19 = bf16[128,2048]{1,0:T(8,128)(2,1)S(1)} collective-permute-done((bf16[128,2048]{1,0:T(8,128)(2,1)}, bf16[128,2048]{1,0:T(8,128)(2,1)S(1)}, u32[]{:S(2)}, u32[]{:S(2)}) %collective-permute-start.19) | collective-permute-done | bytes 524320 | tf_op jit(solution)/shard_map/ppermute | solution.py:334
  124.5 1.2 add_convert_fusion
  125.7 3.7 %collective-permute-start.20 = (bf16[128,2048]{1,0:T(8,128)(2,1)S(1)}, bf16[128,2048]{1,0:T(8,128)(2,1)S(1)}, u32[]{:S(2)}, u32[]{:S(2)}) collective-permute-start(bf16[128,2048]{1,0:T(8,128)(2,1)S(1)} %add_convert_fusion), channel_id=1, source_target_pairs={{0,6},{1,7},{2,0},{3,1},{4,2},{5,3},{6,4},{7,5},{8,14},{9,15},{10,... | collective-permute-start | bytes 1572872 | tf_op jit(solution)/shard_map/ppermute | solution.py:334
  129.3 6.4 %collective-permute-done.17.refs_2_ = bf16[128,2048]{1,0:T(8,128)(2,1)S(1)} collective-permute-done((bf16[128,2048]{1,0:T(8,128)(2,1)}, bf16[128,2048]{1,0:T(8,128)(2,1)S(1)}, u32[]{:S(2)}, u32[]{:S(2)}) %collective-permute-start.17) | collective-permute-done | bytes 524320 | tf_op jit(solution)/shard_map/ppermute | solution.py:334
  135.7 0.0 collective-permute-done.18.refs_4_
  135.7 8.4 %collective-permute-done.16.refs_1_ = bf16[128,2048]{1,0:T(8,128)(2,1)S(1)} collective-permute-done((bf16[128,2048]{1,0:T(8,128)(2,1)S(1)}, bf16[128,2048]{1,0:T(8,128)(2,1)S(1)}, u32[]{:S(2)}, u32[]{:S(2)}) %collective-permute-start.16) | collective-permute-done | bytes 524320 | tf_op jit(solution)/shard_map/ppermute | solution.py:334
  144.1 0.9 collective-permute-done.20.refs_5_
  145.0 1.5 join.1
  146.5 0.0 all-to-all-done.3
  146.5 7.2 %all-to-all-start.4 = ((bf16[16,256,128]{2,1,0:T(8,128)(2,1)}), bf16[16,256,128]{2,1,0:T(8,128)(2,1)S(1)}, u32[]{:S(2)}, u32[]{:S(2)}) async-start(bf16[16,256,128]{2,1,0:T(8,128)(2,1)} %join.1), calls=%async_computation.4 | async-start | bytes 2097152 | tf_op jit(solution)/shard_map/all_to_all | solution.py:311
  153.7 8.5 %hidden_grad.1 = bf16[128,2,2048]{2,1,0:T(2,128)(2,1)} custom-call(s32[16]{0:T(128)} %fusion.2.order_ref, bf16[256,2048]{1,0:T(8,128)(2,1)} %value_grad.1.dv_ref, bf16[256,2048]{1,0:T(8,128)(2,1)} %refs_0_.3, bf16[128,2048]{1,0:T(8,128)(2,1)} %collective-permute-done.refs_1_, bf16[128,2048]{1,0:T(8,128)(2,1)} %collective-permute-done.1.refs_2_, ...), custom_call_target="tpu_custom_call" | custom-call | flops 2147483648 | bytes 10485760 | tf_op jit(solution)/shard_map/hidden_grad/pallas_call | solution.py:537
  162.2 7.1 %final.1 = (bf16[128,2,1024]{2,1,0:T(2,128)(2,1)}, bf16[128,2,1024]{2,1,0:T(2,128)(2,1)}, bf16[128,2,1024]{2,1,0:T(2,128)(2,1)}) custom-call(bf16[128,2,1024]{2,1,0:T(2,128)(2,1)} %k_ref.3, bf16[128,2,1024]{2,1,0:T(2,128)(2,1)} %g_ref.5, f32[1,1024]{1,0:T(1,128)} %bitcast.12, f32[256,1024]{1,0:T(8,128)} %get-tuple-element.24.cum_ref, ...), custom_call_target="tpu_custom_call" | custom-call | flops 805306368 | bytes 10485760 | tf_op jit(solution)/shard_map/final/pallas_call | solution.py:553
  169.4 0.8 convert_reduce_fusion
  (25 shorter events, 0.1 us)
Async XLA Ops:
  0.6 12.4 %copy-start.3 = (bf16[256,2048]{1,0:T(8,128)(2,1)S(1)}, bf16[256,2048]{1,0:T(8,128)(2,1)}, u32[]{:S(2)}) copy-start(bf16[256,2048]{1,0:T(8,128)(2,1)} %refs_0_.3) | copy-start | bytes 3145732
  4.7 24.5 %all-to-all-start = ((bf16[16,264,128]{2,1,0:T(8,128)(2,1)}), bf16[16,264,128]{2,1,0:T(8,128)(2,1)S(1)}, u32[]{:S(2)}, u32[]{:S(2)}) async-start(bf16[16,264,128]{2,1,0:T(8,128)(2,1)} %bitcast.7), calls=%async_computation | async-start | bytes 2162688 | tf_op jit(solution)/shard_map/all_to_all | solution.py:311
  13.1 31.5 %collective-permute-start.4 = (bf16[256,2048]{1,0:T(8,128)(2,1)S(1)}, bf16[256,2048]{1,0:T(8,128)(2,1)}, u32[]{:S(2)}, u32[]{:S(2)}) collective-permute-start(bf16[256,2048]{1,0:T(8,128)(2,1)S(1)} %copy-done.3), channel_id=1, source_target_pairs={{0,1},{1,0},{2,3},{3,2},{4,5},{5,4},{6,7},{7,6},{8,9},{9,8},{10,11... | collective-permute-start | bytes 3145736 | tf_op jit(solution)/shard_map/ppermute | solution.py:337
  14.2 21.8 %collective-permute-start = (bf16[128,2048]{1,0:T(8,128)(2,1)}, bf16[128,2048]{1,0:T(8,128)(2,1)}, u32[]{:S(2)}, u32[]{:S(2)}) collective-permute-start(bf16[128,2048]{1,0:T(8,128)(2,1)} %get-tuple-element.40), channel_id=1, source_target_pairs={{0,2},{1,3},{2,4},{3,5},{4,6},{5,7},{6,0},{7,1},{8,10},{9,11},{10,... | collective-permute-start | bytes 1572872 | tf_op jit(solution)/shard_map/ppermute | solution.py:334
  15.7 25.6 %collective-permute-start.1 = (bf16[128,2048]{1,0:T(8,128)(2,1)}, bf16[128,2048]{1,0:T(8,128)(2,1)}, u32[]{:S(2)}, u32[]{:S(2)}) collective-permute-start(bf16[128,2048]{1,0:T(8,128)(2,1)} %get-tuple-element.39), channel_id=1, source_target_pairs={{0,2},{1,3},{2,4},{3,5},{4,6},{5,7},{6,0},{7,1},{8,10},{9,11},{10,... | collective-permute-start | bytes 1572872 | tf_op jit(solution)/shard_map/ppermute | solution.py:334
  17.2 24.4 %collective-permute-start.3 = (bf16[128,2048]{1,0:T(8,128)(2,1)}, bf16[128,2048]{1,0:T(8,128)(2,1)}, u32[]{:S(2)}, u32[]{:S(2)}) collective-permute-start(bf16[128,2048]{1,0:T(8,128)(2,1)} %get-tuple-element.39), channel_id=1, source_target_pairs={{0,6},{1,7},{2,0},{3,1},{4,2},{5,3},{6,4},{7,5},{8,14},{9,15},{10,... | collective-permute-start | bytes 1572872 | tf_op jit(solution)/shard_map/ppermute | solution.py:334
  18.9 25.6 %collective-permute-start.2 = (bf16[128,2048]{1,0:T(8,128)(2,1)}, bf16[128,2048]{1,0:T(8,128)(2,1)}, u32[]{:S(2)}, u32[]{:S(2)}) collective-permute-start(bf16[128,2048]{1,0:T(8,128)(2,1)} %get-tuple-element.40), channel_id=1, source_target_pairs={{0,6},{1,7},{2,0},{3,1},{4,2},{5,3},{6,4},{7,5},{8,14},{9,15},{10,... | collective-permute-start | bytes 1572872 | tf_op jit(solution)/shard_map/ppermute | solution.py:334
  30.5 30.6 %all-to-all-start.1 = ((bf16[16,256,128]{2,1,0:T(8,128)(2,1)}), bf16[16,256,128]{2,1,0:T(8,128)(2,1)S(1)}, u32[]{:S(2)}, u32[]{:S(2)}) async-start(bf16[16,256,128]{2,1,0:T(8,128)(2,1)} %scan.2), calls=%async_computation.1 | async-start | bytes 2097152 | tf_op jit(solution)/shard_map/all_to_all | solution.py:311
  36.0 9.1 %collective-permute-start.5 = (bf16[128,2048]{1,0:T(8,128)(2,1)}, bf16[128,2048]{1,0:T(8,128)(2,1)}, u32[]{:S(2)}, u32[]{:S(2)}) collective-permute-start(bf16[128,2048]{1,0:T(8,128)(2,1)} %collective-permute-done.refs_1_), channel_id=1, source_target_pairs={{0,1},{1,0},{2,3},{3,2},{4,5},{5,4},{6,7},{7,6},{8,9},{9,8},{10,11... | collective-permute-start | bytes 1572872 | tf_op jit(solution)/shard_map/ppermute | solution.py:337
  41.3 15.0 %collective-permute-start.9 = (bf16[128,2048]{1,0:T(8,128)(2,1)}, bf16[128,2048]{1,0:T(8,128)(2,1)}, u32[]{:S(2)}, u32[]{:S(2)}) collective-permute-start(bf16[128,2048]{1,0:T(8,128)(2,1)} %collective-permute-done.refs_1_), channel_id=1, source_target_pairs={{0,2},{1,3},{2,4},{3,5},{4,6},{5,7},{6,0},{7,1},{8,10},{9,11},{10,... | collective-permute-start | bytes 1572872 | tf_op jit(solution)/shard_map/ppermute | solution.py:334
  41.6 14.7 %collective-permute-start.10 = (bf16[128,2048]{1,0:T(8,128)(2,1)}, bf16[128,2048]{1,0:T(8,128)(2,1)}, u32[]{:S(2)}, u32[]{:S(2)}) collective-permute-start(bf16[128,2048]{1,0:T(8,128)(2,1)} %collective-permute-done.3.refs_4_), channel_id=1, source_target_pairs={{0,6},{1,7},{2,0},{3,1},{4,2},{5,3},{6,4},{7,5},{8,14},{9,15},{10,... | collective-permute-start | bytes 1572872 | tf_op jit(solution)/shard_map/ppermute | solution.py:334
  44.5 21.0 %collective-permute-start.6 = (bf16[128,2048]{1,0:T(8,128)(2,1)}, bf16[128,2048]{1,0:T(8,128)(2,1)}, u32[]{:S(2)}, u32[]{:S(2)}) collective-permute-start(bf16[128,2048]{1,0:T(8,128)(2,1)} %collective-permute-done.1.refs_2_), channel_id=1, source_target_pairs={{0,1},{1,0},{2,3},{3,2},{4,5},{5,4},{6,7},{7,6},{8,9},{9,8},{10,11... | collective-permute-start | bytes 1572872 | tf_op jit(solution)/shard_map/ppermute | solution.py:337
  44.5 21.1 %collective-permute-start.7 = (bf16[128,2048]{1,0:T(8,128)(2,1)}, bf16[128,2048]{1,0:T(8,128)(2,1)}, u32[]{:S(2)}, u32[]{:S(2)}) collective-permute-start(bf16[128,2048]{1,0:T(8,128)(2,1)} %collective-permute-done.2.refs_3_), channel_id=1, source_target_pairs={{0,1},{1,0},{2,3},{3,2},{4,5},{5,4},{6,7},{7,6},{8,9},{9,8},{10,11... | collective-permute-start | bytes 1572872 | tf_op jit(solution)/shard_map/ppermute | solution.py:337
  45.0 21.6 %collective-permute-start.8 = (bf16[128,2048]{1,0:T(8,128)(2,1)}, bf16[128,2048]{1,0:T(8,128)(2,1)}, u32[]{:S(2)}, u32[]{:S(2)}) collective-permute-start(bf16[128,2048]{1,0:T(8,128)(2,1)} %collective-permute-done.3.refs_4_), channel_id=1, source_target_pairs={{0,1},{1,0},{2,3},{3,2},{4,5},{5,4},{6,7},{7,6},{8,9},{9,8},{10,11... | collective-permute-start | bytes 1572872 | tf_op jit(solution)/shard_map/ppermute | solution.py:337
  56.3 17.1 %collective-permute-start.11 = (bf16[128,2048]{1,0:T(8,128)(2,1)}, bf16[128,2048]{1,0:T(8,128)(2,1)}, u32[]{:S(2)}, u32[]{:S(2)}) collective-permute-start(bf16[128,2048]{1,0:T(8,128)(2,1)} %collective-permute-done.9.refs_10_.refs_0_), channel_id=1, source_target_pairs={{0,1},{1,0},{2,3},{3,2},{4,5},{5,4},{6,7},{7,6},{8,9},{9,8},{10,11... | collective-permute-start | bytes 1572872 | tf_op jit(solution)/shard_map/ppermute | solution.py:337
  56.3 17.1 %collective-permute-start.12 = (bf16[128,2048]{1,0:T(8,128)(2,1)}, bf16[128,2048]{1,0:T(8,128)(2,1)}, u32[]{:S(2)}, u32[]{:S(2)}) collective-permute-start(bf16[128,2048]{1,0:T(8,128)(2,1)} %collective-permute-done.10.refs_11_.refs_1_), channel_id=1, source_target_pairs={{0,1},{1,0},{2,3},{3,2},{4,5},{5,4},{6,7},{7,6},{8,9},{9,8},{10,11... | collective-permute-start | bytes 1572872 | tf_op jit(solution)/shard_map/ppermute | solution.py:337
  61.1 1.0 copy-start.4
  62.1 3.4 %copy-start.2 = (bf16[128,2,2048]{2,1,0:T(2,128)(2,1)S(1)}, bf16[128,2,2048]{2,1,0:T(2,128)(2,1)}, u32[]{:S(2)}) copy-start(bf16[128,2,2048]{2,1,0:T(2,128)(2,1)} %h_ref.7) | copy-start | bytes 3145732
  62.1 4.0 %copy-start.6 = (s32[16]{0:T(128)S(1)}, s32[16]{0:T(128)}, u32[]{:S(2)}) copy-start(s32[16]{0:T(128)} %constant.66) | copy-start | bytes 196
  62.1 4.0 %copy-start.7 = (s32[16]{0:T(128)S(1)}, s32[16]{0:T(128)}, u32[]{:S(2)}) copy-start(s32[16]{0:T(128)} %constant.59.clone) | copy-start | bytes 196
  62.1 4.0 %copy-start.8 = (s32[16]{0:T(128)S(1)}, s32[16]{0:T(128)}, u32[]{:S(2)}) copy-start(s32[16]{0:T(128)} %constant.60.clone) | copy-start | bytes 196
  62.1 4.0 %copy-start.9 = (s32[16]{0:T(128)S(1)}, s32[16]{0:T(128)}, u32[]{:S(2)}) copy-start(s32[16]{0:T(128)} %constant.58.clone) | copy-start | bytes 196
  65.5 20.7 %collective-permute-start.13 = (bf16[128,2,2048]{2,1,0:T(2,128)(2,1)S(1)}, bf16[128,2,2048]{2,1,0:T(2,128)(2,1)}, u32[]{:S(2)}, u32[]{:S(2)}) collective-permute-start(bf16[128,2,2048]{2,1,0:T(2,128)(2,1)S(1)} %copy-done.2), channel_id=1, source_target_pairs={{0,1},{1,0},{2,3},{3,2},{4,5},{5,4},{6,7},{7,6},{8,9},{9,8},{10,11... | collective-permute-start | bytes 3145736 | tf_op jit(solution)/shard_map/ppermute | solution.py:337
  65.6 20.6 %collective-permute-start.14 = (bf16[256,2048]{1,0:T(8,128)(2,1)}, bf16[256,2048]{1,0:T(8,128)(2,1)}, u32[]{:S(2)}, u32[]{:S(2)}) collective-permute-start(bf16[256,2048]{1,0:T(8,128)(2,1)} %value_grad.1.dv_ref), channel_id=1, source_target_pairs={{0,1},{1,0},{2,3},{3,2},{4,5},{5,4},{6,7},{7,6},{8,9},{9,8},{10,11... | collective-permute-start | bytes 3145736 | tf_op jit(solution)/shard_map/ppermute | solution.py:337
  79.0 23.3 %all-to-all-start.2 = ((bf16[16,256,128]{2,1,0:T(8,128)(2,1)}), bf16[16,256,128]{2,1,0:T(8,128)(2,1)S(1)}, u32[]{:S(2)}, u32[]{:S(2)}) async-start(bf16[16,256,128]{2,1,0:T(8,128)(2,1)} %bitcast.9), calls=%async_computation.2 | async-start | bytes 2097152 | tf_op jit(solution)/shard_map/all_to_all | solution.py:311
  90.0 30.8 %collective-permute-start.15 = (bf16[128,2048]{1,0:T(8,128)(2,1)}, bf16[128,2048]{1,0:T(8,128)(2,1)S(1)}, u32[]{:S(2)}, u32[]{:S(2)}) collective-permute-start(bf16[128,2048]{1,0:T(8,128)(2,1)} %get-tuple-element.33), channel_id=1, source_target_pairs={{0,2},{1,3},{2,4},{3,5},{4,6},{5,7},{6,0},{7,1},{8,10},{9,11},{10,... | collective-permute-start | bytes 1572872 | tf_op jit(solution)/shard_map/ppermute | solution.py:334
  103.5 43.0 %all-to-all-start.3 = ((bf16[16,256,128]{2,1,0:T(8,128)(2,1)}), bf16[16,256,128]{2,1,0:T(8,128)(2,1)S(1)}, u32[]{:S(2)}, u32[]{:S(2)}) async-start(bf16[16,256,128]{2,1,0:T(8,128)(2,1)} %scan.3), calls=%async_computation.3 | async-start | bytes 2097152 | tf_op jit(solution)/shard_map/all_to_all | solution.py:311
  108.8 15.7 %collective-permute-start.19 = (bf16[128,2048]{1,0:T(8,128)(2,1)}, bf16[128,2048]{1,0:T(8,128)(2,1)S(1)}, u32[]{:S(2)}, u32[]{:S(2)}) collective-permute-start(bf16[128,2048]{1,0:T(8,128)(2,1)} %get-tuple-element.38), channel_id=1, source_target_pairs={{0,6},{1,7},{2,0},{3,1},{4,2},{5,3},{6,4},{7,5},{8,14},{9,15},{10,... | collective-permute-start | bytes 1572872 | tf_op jit(solution)/shard_map/ppermute | solution.py:334
  118.7 26.4 %copy-start = (bf16[128,2048]{1,0:T(8,128)(2,1)S(1)}, bf16[128,2048]{1,0:T(8,128)(2,1)}, u32[]{:S(2)}) copy-start(bf16[128,2048]{1,0:T(8,128)(2,1)} %get-tuple-element.31.refs_0_) | copy-start | bytes 1572868
  118.7 26.4 %copy-start.1 = (bf16[128,2048]{1,0:T(8,128)(2,1)S(1)}, bf16[128,2048]{1,0:T(8,128)(2,1)}, u32[]{:S(2)}) copy-start(bf16[128,2048]{1,0:T(8,128)(2,1)} %get-tuple-element.35.refs_3_) | copy-start | bytes 1572868
  118.7 17.1 %collective-permute-start.17 = (bf16[128,2048]{1,0:T(8,128)(2,1)}, bf16[128,2048]{1,0:T(8,128)(2,1)S(1)}, u32[]{:S(2)}, u32[]{:S(2)}) collective-permute-start(bf16[128,2048]{1,0:T(8,128)(2,1)} %get-tuple-element.34), channel_id=1, source_target_pairs={{0,6},{1,7},{2,0},{3,1},{4,2},{5,3},{6,4},{7,5},{8,14},{9,15},{10,... | collective-permute-start | bytes 1572872 | tf_op jit(solution)/shard_map/ppermute | solution.py:334
  118.7 17.0 %collective-permute-start.18 = (bf16[128,2048]{1,0:T(8,128)(2,1)}, bf16[128,2048]{1,0:T(8,128)(2,1)S(1)}, u32[]{:S(2)}, u32[]{:S(2)}) collective-permute-start(bf16[128,2048]{1,0:T(8,128)(2,1)} %get-tuple-element.36), channel_id=1, source_target_pairs={{0,2},{1,3},{2,4},{3,5},{4,6},{5,7},{6,0},{7,1},{8,10},{9,11},{10,... | collective-permute-start | bytes 1572872 | tf_op jit(solution)/shard_map/ppermute | solution.py:334
  121.9 22.2 %collective-permute-start.16 = (bf16[128,2048]{1,0:T(8,128)(2,1)S(1)}, bf16[128,2048]{1,0:T(8,128)(2,1)S(1)}, u32[]{:S(2)}, u32[]{:S(2)}) collective-permute-start(bf16[128,2048]{1,0:T(8,128)(2,1)S(1)} %add_convert_fusion.1), channel_id=1, source_target_pairs={{0,2},{1,3},{2,4},{3,5},{4,6},{5,7},{6,0},{7,1},{8,10},{9,11},{10,... | collective-permute-start | bytes 1572872 | tf_op jit(solution)/shard_map/ppermute | solution.py:334
  125.7 19.3 %collective-permute-start.20 = (bf16[128,2048]{1,0:T(8,128)(2,1)S(1)}, bf16[128,2048]{1,0:T(8,128)(2,1)S(1)}, u32[]{:S(2)}, u32[]{:S(2)}) collective-permute-start(bf16[128,2048]{1,0:T(8,128)(2,1)S(1)} %add_convert_fusion), channel_id=1, source_target_pairs={{0,6},{1,7},{2,0},{3,1},{4,2},{5,3},{6,4},{7,5},{8,14},{9,15},{10,... | collective-permute-start | bytes 1572872 | tf_op jit(solution)/shard_map/ppermute | solution.py:334
  146.5 15.7 %copy-start.5 = (bf16[16,256,128]{2,1,0:T(8,128)(2,1)}, bf16[16,256,128]{2,1,0:T(8,128)(2,1)S(1)}, u32[]{:S(2)}) copy-start(bf16[16,256,128]{2,1,0:T(8,128)(2,1)S(1)} %all-to-all-done.3) | copy-start | bytes 3145732
  146.5 22.9 %all-to-all-start.4 = ((bf16[16,256,128]{2,1,0:T(8,128)(2,1)}), bf16[16,256,128]{2,1,0:T(8,128)(2,1)S(1)}, u32[]{:S(2)}, u32[]{:S(2)}) async-start(bf16[16,256,128]{2,1,0:T(8,128)(2,1)} %join.1), calls=%async_computation.4 | async-start | bytes 2097152 | tf_op jit(solution)/shard_map/all_to_all | solution.py:311

commit v6 on v5

--- a/solution.py
+++ b/solution.py
@@ -180,6 +180,11 @@
         def _():
             outs[2 * p][...] = part[:half]
             outs[2 * p + 1][...] = part[half:]
+
+
+def plus_kernel(one_ref, two_ref, three_ref, four_ref, top_ref, bottom_ref):
+    top_ref[...] = (one_ref[...].astype(F32) + two_ref[...].astype(F32)).astype(BF16)
+    bottom_ref[...] = (three_ref[...].astype(F32) + four_ref[...].astype(F32)).astype(BF16)
 
 
 def join_kernel(top_refs, bottom_refs, out_ref):
@@ -474,11 +479,15 @@
     ready_before = along(next_bottom, 1)
     ready_after = along(last_top, -1)
 
-    def plus(one, two):
-        return (one.astype(F32) + two.astype(F32)).astype(BF16)
-
-    late_before = along(plus(next_top, from_before), 1)
-    late_after = along(plus(last_bottom, from_after), -1)
+    late_top, late_bottom = pl.pallas_call(
+        plus_kernel,
+        out_shape=[shaped((half, values))] * 2,
+        compiler_params=pltpu.CompilerParams(vmem_limit_bytes=12 << 20),
+        cost_estimate=cost(1 << 22, 3 << 20),
+        name="plus",
+    )(next_top, from_before, last_bottom, from_after)
+    late_before = along(late_top, 1)
+    late_after = along(late_bottom, -1)
     partial = pl.pallas_call(
         join_parts,
         out_shape=shaped((blocks, shard, values // blocks)),

time: 172 us -> 171 us (level)
  waiting for transfers between devices: 56.6 us -> 52.9 us
  local copies, waits for them, and re-layouts: 2.07 us -> 5.24 us
  other arithmetic: 3.66 us -> 1.32 us
  starting transfers between devices: 52.9 us -> 55.1 us
    all_to_all x5, waiting for transfers between devices: 22 us -> 9.37 us  [over_sp(): return lax.all_to_all(value, 'sp', split_axis=0, concat_axis=0, tiled=True)]
    ppermute x12, waiting for transfers between devices: 34.6 us -> 43.5 us  [along(): return lax.ppermute(value, 'dp', pairs)]
    unnamed x20 -> x28, local copies, waits for them, and re-layouts: 1.03 us -> 4.21 us
    all_to_all x5, starting transfers between devices: 33.6 us -> 36.1 us  [over_sp(): return lax.all_to_all(value, 'sp', split_axis=0, concat_axis=0, tiled=True)]
    convert_element_type x2 -> x0, other arithmetic: 2.33 us -> none  [plus(): return (one.astype(F32) + two.astype(F32)).astype(BF16)]
  transfers between devices with their start and end apart: 26 -> 26, of which waited for: 8 -> 7; matrix products, arithmetic and copies ran while one was open for 2% -> 1% of each run, Pallas kernels for 29% -> 30%
where the time goes in v6:
time: 171 us; the launch traced here: 170 us
  starting transfers between devices  55.1 us (32%)
  Pallas kernels  54.5 us (32%)
  waiting for transfers between devices  52.9 us (31%)
  local copies, waits for them, and re-layouts  5.24 us (3%)
    ppermute x12, waiting for transfers between devices, along(): return lax.ppermute(value, 'dp', pairs)  43.5 us
    all_to_all x5, starting transfers between devices, over_sp(): return lax.all_to_all(value, 'sp', split_axis=0, concat_axis=0, tiled=True)  36.1 us
    ppermute x12, starting transfers between devices, along(): return lax.ppermute(value, 'dp', pairs)  17.3 us
    all_to_all x5, waiting for transfers between devices, over_sp(): return lax.all_to_all(value, 'sp', split_axis=0, concat_axis=0, tiled=True)  9.37 us
    pallas_call x1, Pallas kernels, arranged(): pl.pallas_call(hidden_grad_kernel, grid_spec=pltpu.PrefetchScalarGridSpec...  8.48 us
    pallas_call x1, Pallas kernels, arranged(): pl.pallas_call(final_kernel, grid=(STEPS,), in_specs=[raw_key, raw_key, b...  7.14 us
    pallas_call x1, Pallas kernels, rest(): pl.pallas_call(rest_kernel, grid_spec=pltpu.PrefetchScalarGridSpec(num_sc...  6.8 us
    pallas_call x1, Pallas kernels, arranged(): pl.pallas_call(near_kernel, grid_spec=pltpu.PrefetchScalarGridSpec(num_sc...  6.7 us
  transfers between devices with their start and end apart: 26, of which 7 were waited for; matrix products, arithmetic and copies ran while one was open for 1% of the time, Pallas kernels for 30%

profile of v6, /device:TPU:8, one launch (start us, length us, event | category | flops | bytes accessed | tf_op | source)
XLA Modules:
  0.0 169.9 jit_solution(16327577757497633183)
XLA Ops:
  0.6 0.0 copy-start.5
  0.6 4.0 %decay.1 = bf16[2,8,264,128]{3,2,1,0:T(8,128)(2,1)} custom-call(bf16[128,2,1024]{2,1,0:T(2,128)(2,1)} %q_ref.3, bf16[128,2,1024]{2,1,0:T(2,128)(2,1)} %g_ref.5, f32[1,1024]{1,0:T(1,128)} %bitcast.10, bf16[128,2,2048]{2,1,0:T(2,128)(2,1)} %do_ref.5), custom_call_target="tpu_custom_call" | custom-call | flops 402653184 | bytes 4194304 | tf_op jit(solution)/shard_map/decay/pallas_call | solution.py:376
  4.7 8.4 %all-to-all-start = ((bf16[16,264,128]{2,1,0:T(8,128)(2,1)}), bf16[16,264,128]{2,1,0:T(8,128)(2,1)S(1)}, u32[]{:S(2)}, u32[]{:S(2)}) async-start(bf16[16,264,128]{2,1,0:T(8,128)(2,1)} %bitcast.7), calls=%async_computation | async-start | bytes 2162688 | tf_op jit(solution)/shard_map/all_to_all | solution.py:316
  13.1 0.1 collective-permute-start.4
  13.2 1.0 fusion.5
  14.2 1.5 collective-permute-start
  15.7 1.5 collective-permute-start.1
  17.2 1.7 %collective-permute-start.3 = (bf16[128,2048]{1,0:T(8,128)(2,1)}, bf16[128,2048]{1,0:T(8,128)(2,1)}, u32[]{:S(2)}, u32[]{:S(2)}) collective-permute-start(bf16[128,2048]{1,0:T(8,128)(2,1)} %get-tuple-element.43), channel_id=1, source_target_pairs={{0,6},{1,7},{2,0},{3,1},{4,2},{5,3},{6,4},{7,5},{8,14},{9,15},{10,... | collective-permute-start | bytes 1572872 | tf_op jit(solution)/shard_map/ppermute | solution.py:339
  18.9 0.5 collective-permute-start.2
  19.5 11.1 %collective-permute-done.refs_1_ = bf16[128,2048]{1,0:T(8,128)(2,1)} collective-permute-done((bf16[128,2048]{1,0:T(8,128)(2,1)}, bf16[128,2048]{1,0:T(8,128)(2,1)}, u32[]{:S(2)}, u32[]{:S(2)}) %collective-permute-start) | collective-permute-done | bytes 524320 | tf_op jit(solution)/shard_map/ppermute | solution.py:339
  30.5 1.3 scan.2
  31.8 7.4 %all-to-all-start.1 = ((bf16[16,256,128]{2,1,0:T(8,128)(2,1)}), bf16[16,256,128]{2,1,0:T(8,128)(2,1)S(1)}, u32[]{:S(2)}, u32[]{:S(2)}) async-start(bf16[16,256,128]{2,1,0:T(8,128)(2,1)} %scan.2), calls=%async_computation.1 | async-start | bytes 2097152 | tf_op jit(solution)/shard_map/all_to_all | solution.py:316
  39.2 2.1 %collective-permute-done.1.refs_2_ = bf16[128,2048]{1,0:T(8,128)(2,1)} collective-permute-done((bf16[128,2048]{1,0:T(8,128)(2,1)}, bf16[128,2048]{1,0:T(8,128)(2,1)}, u32[]{:S(2)}, u32[]{:S(2)}) %collective-permute-start.1) | collective-permute-done | bytes 524320 | tf_op jit(solution)/shard_map/ppermute | solution.py:339
  41.3 0.3 collective-permute-start.9
  41.6 3.0 %collective-permute-start.10 = (bf16[128,2048]{1,0:T(8,128)(2,1)}, bf16[128,2048]{1,0:T(8,128)(2,1)}, u32[]{:S(2)}, u32[]{:S(2)}) collective-permute-start(bf16[128,2048]{1,0:T(8,128)(2,1)} %collective-permute-done.3.refs_4_), channel_id=1, source_target_pairs={{0,6},{1,7},{2,0},{3,1},{4,2},{5,3},{6,4},{7,5},{8,14},{9,15},{10,... | collective-permute-start | bytes 1572872 | tf_op jit(solution)/shard_map/ppermute | solution.py:339
  44.5 0.0 collective-permute-done.4.refs_5_
  44.5 0.5 collective-permute-start.7
  45.0 0.1 collective-permute-start.8
  45.1 11.1 %collective-permute-done.9.refs_10_.refs_0_ = bf16[128,2048]{1,0:T(8,128)(2,1)} collective-permute-done((bf16[128,2048]{1,0:T(8,128)(2,1)}, bf16[128,2048]{1,0:T(8,128)(2,1)}, u32[]{:S(2)}, u32[]{:S(2)}) %collective-permute-start.9) | collective-permute-done | bytes 524320 | tf_op jit(solution)/shard_map/ppermute | solution.py:339
  56.3 0.0 collective-permute-start.11
  56.3 0.0 collective-permute-done.10.refs_11_.refs_1_
  56.3 0.5 collective-permute-start.12
  56.8 4.3 %intra.1 = (f32[256,1024]{1,0:T(8,128)}, bf16[256,1024]{1,0:T(8,128)(2,1)}, bf16[8,256,256]{2,1,0:T(8,128)(2,1)}, bf16[256,1024]{1,0:T(8,128)(2,1)}) custom-call(bf16[128,2,1024]{2,1,0:T(2,128)(2,1)} %q_ref.3, bf16[128,2,1024]{2,1,0:T(2,128)(2,1)} %k_ref.3, bf16[128,2,1024]{2,1,0:T(2,128)(2,1)} %g_ref.5, f32[1,1024]{1,0:T(1,128)} %bitcast.11), custom_call_target="tpu_custom_call" | custom-call | flops 402653184 | bytes 5242880 | tf_op jit(solution)/shard_map/intra/pallas_call | solution.py:389
  61.1 0.5 fusion.2.order_ref
  61.6 0.0 all-to-all-done.1
  61.6 1.0 copy-done.6
  62.6 3.4 %value_grad.1.dv_ref = bf16[256,2048]{1,0:T(8,128)(2,1)} custom-call(bf16[8,256,256]{2,1,0:T(8,128)(2,1)} %get-tuple-element.24.scores_ref, bf16[128,2,2048]{2,1,0:T(2,128)(2,1)} %do_ref.5, bf16[256,1024]{1,0:T(8,128)(2,1)} %get-tuple-element.25.k_dec_ref, bf16[2,8,256,128]{3,2,1,0:T(8,128)(2,1)} %bitcast.5), custom_call_target="tpu_custom_call" | custom-call | flops 402653184 | bytes 5242880 | tf_op jit(solution)/shard_map/value_grad/pallas_call | solution.py:419
  66.0 0.0 collective-permute-done.6.refs_7_
  66.0 0.1 collective-permute-start.13
  66.2 0.0 copy-start.8
  66.2 0.5 collective-permute-start.14
  66.6 0.3 copy-done.8
  67.0 0.8 copy-done.9
  67.7 6.7 %project_near.1.sum_ref = f32[256,2048]{1,0:T(8,128)} custom-call(s32[16]{0:T(128)} %fusion.2.order_ref, bf16[128,2,2048]{2,1,0:T(2,128)(2,1)} %h_ref.7, bf16[256,2048]{1,0:T(8,128)(2,1)} %refs_0_.3, bf16[128,2048]{1,0:T(8,128)(2,1)} %collective-permute-done.refs_1_, bf16[128,2048]{1,0:T(8,128)(2,1)} %collective-permute-done.1.refs_2_, ...), custom_call_target="tpu_custom_call" | custom-call | flops 1610612736 | bytes 10485760 | tf_op jit(solution)/shard_map/project_near/pallas_call | solution.py:503
  74.4 0.0 collective-permute-done.11.refs_12_.refs_2_
  74.4 0.0 collective-permute-done.12.refs_13_.refs_3_
  74.5 5.5 %project.1 = (bf16[256,2048]{1,0:T(8,128)(2,1)}, bf16[2,8,256,128]{3,2,1,0:T(8,128)(2,1)}) custom-call(s32[16]{0:T(128)} %fusion.2.order_ref, bf16[128,2,2048]{2,1,0:T(2,128)(2,1)} %h_ref.7, f32[256,2048]{1,0:T(8,128)} %project_near.1.sum_ref, bf16[256,1024]{1,0:T(8,128)(2,1)} %get-tuple-element.25.k_dec_ref, ...), custom_call_target="tpu_custom_call" | custom-call | flops 671088640 | bytes 7340032 | tf_op jit(solution)/shard_map/project/pallas_call | solution.py:518
  80.0 7.2 %all-to-all-start.2 = ((bf16[16,256,128]{2,1,0:T(8,128)(2,1)}), bf16[16,256,128]{2,1,0:T(8,128)(2,1)S(1)}, u32[]{:S(2)}, u32[]{:S(2)}) async-start(bf16[16,256,128]{2,1,0:T(8,128)(2,1)} %bitcast.9), calls=%async_computation.2 | async-start | bytes 2097152 | tf_op jit(solution)/shard_map/all_to_all | solution.py:316
  87.2 0.0 collective-permute-done.13.got_ref
  87.2 3.8 %shard_map.137 = (bf16[128,2048]{1,0:T(8,128)(2,1)}, bf16[128,2048]{1,0:T(8,128)(2,1)}) custom-call(s32[16]{0:T(128)} %fusion.2.order_ref, bf16[128,2,2048]{2,1,0:T(2,128)(2,1)} %h_ref.7, bf16[128,2,2048]{2,1,0:T(2,128)(2,1)} %collective-permute-done.13.got_ref, bf16[256,2048]{1,0:T(8,128)(2,1)} %value_grad.1.dv_ref, ...), custom_call_target="tpu_custom_call" | custom-call | flops 536870912 | bytes 5242880 | tf_op jit(solution)/shard_map/pallas_call | solution.py:435
  91.1 0.2 collective-permute-start.15
  91.3 3.0 %collective-permute-start.16 = (bf16[128,2048]{1,0:T(8,128)(2,1)}, bf16[128,2048]{1,0:T(8,128)(2,1)S(1)}, u32[]{:S(2)}, u32[]{:S(2)}) collective-permute-start(bf16[128,2048]{1,0:T(8,128)(2,1)} %get-tuple-element.37), channel_id=1, source_target_pairs={{0,6},{1,7},{2,0},{3,1},{4,2},{5,3},{6,4},{7,5},{8,14},{9,15},{10,... | collective-permute-start | bytes 1572872 | tf_op jit(solution)/shard_map/ppermute | solution.py:339
  94.3 9.4 %all-to-all-done.2.rx_ref = bf16[16,256,128]{2,1,0:T(8,128)(2,1)S(1)} async-done(((bf16[16,256,128]{2,1,0:T(8,128)(2,1)}), bf16[16,256,128]{2,1,0:T(8,128)(2,1)S(1)}, u32[]{:S(2)}, u32[]{:S(2)}) %all-to-all-start.2) | async-done | bytes 1048608 | tf_op jit(solution)/shard_map/all_to_all | solution.py:316
  103.7 1.3 scan.3
  104.9 5.8 %all-to-all-start.3 = ((bf16[16,256,128]{2,1,0:T(8,128)(2,1)}), bf16[16,256,128]{2,1,0:T(8,128)(2,1)S(1)}, u32[]{:S(2)}, u32[]{:S(2)}) async-start(bf16[16,256,128]{2,1,0:T(8,128)(2,1)} %scan.3), calls=%async_computation.3 | async-start | bytes 2097152 | tf_op jit(solution)/shard_map/all_to_all | solution.py:316
  110.8 6.8 %part_rest.1 = (bf16[128,2048]{1,0:T(8,128)(2,1)}, bf16[128,2048]{1,0:T(8,128)(2,1)}, bf16[128,2048]{1,0:T(8,128)(2,1)}, bf16[128,2048]{1,0:T(8,128)(2,1)}, bf16...) custom-call(s32[16]{0:T(128)} %fusion.2.order_ref, bf16[128,2,2048]{2,1,0:T(2,128)(2,1)} %h_ref.7, ...), custom_call_target="tpu_custom_call" | custom-call | flops 1610612736 | bytes 8388608 | tf_op jit(solution)/shard_map/part_rest/pallas_call | solution.py:456
  117.6 2.2 %collective-permute-start.18 = (bf16[128,2048]{1,0:T(8,128)(2,1)}, bf16[128,2048]{1,0:T(8,128)(2,1)S(1)}, u32[]{:S(2)}, u32[]{:S(2)}) collective-permute-start(bf16[128,2048]{1,0:T(8,128)(2,1)} %get-tuple-element.39), channel_id=1, source_target_pairs={{0,6},{1,7},{2,0},{3,1},{4,2},{5,3},{6,4},{7,5},{8,14},{9,15},{10,... | collective-permute-start | bytes 1572872 | tf_op jit(solution)/shard_map/ppermute | solution.py:339
  119.7 0.0 collective-permute-start.19
  119.7 0.0 copy-start
  119.8 1.0 copy-done
  120.8 1.0 copy-done.1
  121.8 0.2 plus.1
  122.1 0.1 collective-permute-start.17
  122.2 3.3 %collective-permute-start.20 = (bf16[128,2048]{1,0:T(8,128)(2,1)S(1)}, bf16[128,2048]{1,0:T(8,128)(2,1)S(1)}, u32[]{:S(2)}, u32[]{:S(2)}) collective-permute-start(bf16[128,2048]{1,0:T(8,128)(2,1)S(1)} %get-tuple-element.42), channel_id=1, source_target_pairs={{0,6},{1,7},{2,0},{3,1},{4,2},{5,3},{6,4},{7,5},{8,14},{9,15},{10,... | collective-permute-start | bytes 1572872 | tf_op jit(solution)/shard_map/ppermute | solution.py:339
  125.5 7.1 %collective-permute-done.18.refs_2_ = bf16[128,2048]{1,0:T(8,128)(2,1)S(1)} collective-permute-done((bf16[128,2048]{1,0:T(8,128)(2,1)}, bf16[128,2048]{1,0:T(8,128)(2,1)S(1)}, u32[]{:S(2)}, u32[]{:S(2)}) %collective-permute-start.18) | collective-permute-done | bytes 524320 | tf_op jit(solution)/shard_map/ppermute | solution.py:339
  132.6 3.4 %collective-permute-done.19.refs_4_ = bf16[128,2048]{1,0:T(8,128)(2,1)S(1)} collective-permute-done((bf16[128,2048]{1,0:T(8,128)(2,1)}, bf16[128,2048]{1,0:T(8,128)(2,1)S(1)}, u32[]{:S(2)}, u32[]{:S(2)}) %collective-permute-start.19) | collective-permute-done | bytes 524320 | tf_op jit(solution)/shard_map/ppermute | solution.py:339
  136.0 8.7 %collective-permute-done.17.refs_1_ = bf16[128,2048]{1,0:T(8,128)(2,1)S(1)} collective-permute-done((bf16[128,2048]{1,0:T(8,128)(2,1)S(1)}, bf16[128,2048]{1,0:T(8,128)(2,1)S(1)}, u32[]{:S(2)}, u32[]{:S(2)}) %collective-permute-start.17) | collective-permute-done | bytes 524320 | tf_op jit(solution)/shard_map/ppermute | solution.py:339
  144.7 0.0 collective-permute-done.20.refs_5_
  144.7 1.5 join.1
  146.2 0.0 all-to-all-done.3
  146.2 7.2 %all-to-all-start.4 = ((bf16[16,256,128]{2,1,0:T(8,128)(2,1)}), bf16[16,256,128]{2,1,0:T(8,128)(2,1)S(1)}, u32[]{:S(2)}, u32[]{:S(2)}) async-start(bf16[16,256,128]{2,1,0:T(8,128)(2,1)} %join.1), calls=%async_computation.4 | async-start | bytes 2097152 | tf_op jit(solution)/shard_map/all_to_all | solution.py:316
  153.4 8.5 %hidden_grad.1 = bf16[128,2,2048]{2,1,0:T(2,128)(2,1)} custom-call(s32[16]{0:T(128)} %fusion.2.order_ref, bf16[256,2048]{1,0:T(8,128)(2,1)} %value_grad.1.dv_ref, bf16[256,2048]{1,0:T(8,128)(2,1)} %refs_0_.3, bf16[128,2048]{1,0:T(8,128)(2,1)} %collective-permute-done.refs_1_, bf16[128,2048]{1,0:T(8,128)(2,1)} %collective-permute-done.1.refs_2_, ...), custom_call_target="tpu_custom_call" | custom-call | flops 2147483648 | bytes 10485760 | tf_op jit(solution)/shard_map/hidden_grad/pallas_call | solution.py:546
  161.9 7.1 %final.1 = (bf16[128,2,1024]{2,1,0:T(2,128)(2,1)}, bf16[128,2,1024]{2,1,0:T(2,128)(2,1)}, bf16[128,2,1024]{2,1,0:T(2,128)(2,1)}) custom-call(bf16[128,2,1024]{2,1,0:T(2,128)(2,1)} %k_ref.3, bf16[128,2,1024]{2,1,0:T(2,128)(2,1)} %g_ref.5, f32[1,1024]{1,0:T(1,128)} %bitcast.12, f32[256,1024]{1,0:T(8,128)} %get-tuple-element.26.cum_ref, ...), custom_call_target="tpu_custom_call" | custom-call | flops 805306368 | bytes 10485760 | tf_op jit(solution)/shard_map/final/pallas_call | solution.py:562
  169.1 0.8 convert_reduce_fusion
  (32 shorter events, 0.1 us)
Async XLA Ops:
  0.6 12.4 %copy-start.5 = (bf16[256,2048]{1,0:T(8,128)(2,1)S(1)}, bf16[256,2048]{1,0:T(8,128)(2,1)}, u32[]{:S(2)}) copy-start(bf16[256,2048]{1,0:T(8,128)(2,1)} %refs_0_.3) | copy-start | bytes 3145732
  4.7 25.9 %all-to-all-start = ((bf16[16,264,128]{2,1,0:T(8,128)(2,1)}), bf16[16,264,128]{2,1,0:T(8,128)(2,1)S(1)}, u32[]{:S(2)}, u32[]{:S(2)}) async-start(bf16[16,264,128]{2,1,0:T(8,128)(2,1)} %bitcast.7), calls=%async_computation | async-start | bytes 2162688 | tf_op jit(solution)/shard_map/all_to_all | solution.py:316
  13.1 31.5 %collective-permute-start.4 = (bf16[256,2048]{1,0:T(8,128)(2,1)S(1)}, bf16[256,2048]{1,0:T(8,128)(2,1)}, u32[]{:S(2)}, u32[]{:S(2)}) collective-permute-start(bf16[256,2048]{1,0:T(8,128)(2,1)S(1)} %copy-done.5), channel_id=1, source_target_pairs={{0,1},{1,0},{2,3},{3,2},{4,5},{5,4},{6,7},{7,6},{8,9},{9,8},{10,11... | collective-permute-start | bytes 3145736 | tf_op jit(solution)/shard_map/ppermute | solution.py:342
  14.2 16.3 %collective-permute-start = (bf16[128,2048]{1,0:T(8,128)(2,1)}, bf16[128,2048]{1,0:T(8,128)(2,1)}, u32[]{:S(2)}, u32[]{:S(2)}) collective-permute-start(bf16[128,2048]{1,0:T(8,128)(2,1)} %get-tuple-element.44), channel_id=1, source_target_pairs={{0,2},{1,3},{2,4},{3,5},{4,6},{5,7},{6,0},{7,1},{8,10},{9,11},{10,... | collective-permute-start | bytes 1572872 | tf_op jit(solution)/shard_map/ppermute | solution.py:339
  15.7 25.6 %collective-permute-start.1 = (bf16[128,2048]{1,0:T(8,128)(2,1)}, bf16[128,2048]{1,0:T(8,128)(2,1)}, u32[]{:S(2)}, u32[]{:S(2)}) collective-permute-start(bf16[128,2048]{1,0:T(8,128)(2,1)} %get-tuple-element.43), channel_id=1, source_target_pairs={{0,2},{1,3},{2,4},{3,5},{4,6},{5,7},{6,0},{7,1},{8,10},{9,11},{10,... | collective-permute-start | bytes 1572872 | tf_op jit(solution)/shard_map/ppermute | solution.py:339
  17.2 24.4 %collective-permute-start.3 = (bf16[128,2048]{1,0:T(8,128)(2,1)}, bf16[128,2048]{1,0:T(8,128)(2,1)}, u32[]{:S(2)}, u32[]{:S(2)}) collective-permute-start(bf16[128,2048]{1,0:T(8,128)(2,1)} %get-tuple-element.43), channel_id=1, source_target_pairs={{0,6},{1,7},{2,0},{3,1},{4,2},{5,3},{6,4},{7,5},{8,14},{9,15},{10,... | collective-permute-start | bytes 1572872 | tf_op jit(solution)/shard_map/ppermute | solution.py:339
  18.9 25.6 %collective-permute-start.2 = (bf16[128,2048]{1,0:T(8,128)(2,1)}, bf16[128,2048]{1,0:T(8,128)(2,1)}, u32[]{:S(2)}, u32[]{:S(2)}) collective-permute-start(bf16[128,2048]{1,0:T(8,128)(2,1)} %get-tuple-element.44), channel_id=1, source_target_pairs={{0,6},{1,7},{2,0},{3,1},{4,2},{5,3},{6,4},{7,5},{8,14},{9,15},{10,... | collective-permute-start | bytes 1572872 | tf_op jit(solution)/shard_map/ppermute | solution.py:339
  30.5 14.5 %collective-permute-start.5 = (bf16[128,2048]{1,0:T(8,128)(2,1)}, bf16[128,2048]{1,0:T(8,128)(2,1)}, u32[]{:S(2)}, u32[]{:S(2)}) collective-permute-start(bf16[128,2048]{1,0:T(8,128)(2,1)} %collective-permute-done.refs_1_), channel_id=1, source_target_pairs={{0,1},{1,0},{2,3},{3,2},{4,5},{5,4},{6,7},{7,6},{8,9},{9,8},{10,11... | collective-permute-start | bytes 1572872 | tf_op jit(solution)/shard_map/ppermute | solution.py:342
  31.8 29.3 %copy-start.10 = (s32[16]{0:T(128)S(1)}, s32[16]{0:T(128)}, u32[]{:S(2)}) copy-start(s32[16]{0:T(128)} %constant.66) | copy-start | bytes 196
  31.8 29.3 %copy-start.11 = (s32[16]{0:T(128)S(1)}, s32[16]{0:T(128)}, u32[]{:S(2)}) copy-start(s32[16]{0:T(128)} %constant.59.clone) | copy-start | bytes 196
  31.8 29.3 %copy-start.12 = (s32[16]{0:T(128)S(1)}, s32[16]{0:T(128)}, u32[]{:S(2)}) copy-start(s32[16]{0:T(128)} %constant.60.clone) | copy-start | bytes 196
  31.8 29.3 %copy-start.13 = (s32[16]{0:T(128)S(1)}, s32[16]{0:T(128)}, u32[]{:S(2)}) copy-start(s32[16]{0:T(128)} %constant.58.clone) | copy-start | bytes 196
  31.8 29.8 %all-to-all-start.1 = ((bf16[16,256,128]{2,1,0:T(8,128)(2,1)}), bf16[16,256,128]{2,1,0:T(8,128)(2,1)S(1)}, u32[]{:S(2)}, u32[]{:S(2)}) async-start(bf16[16,256,128]{2,1,0:T(8,128)(2,1)} %scan.2), calls=%async_computation.1 | async-start | bytes 2097152 | tf_op jit(solution)/shard_map/all_to_all | solution.py:316
  41.3 15.0 %collective-permute-start.9 = (bf16[128,2048]{1,0:T(8,128)(2,1)}, bf16[128,2048]{1,0:T(8,128)(2,1)}, u32[]{:S(2)}, u32[]{:S(2)}) collective-permute-start(bf16[128,2048]{1,0:T(8,128)(2,1)} %collective-permute-done.refs_1_), channel_id=1, source_target_pairs={{0,2},{1,3},{2,4},{3,5},{4,6},{5,7},{6,0},{7,1},{8,10},{9,11},{10,... | collective-permute-start | bytes 1572872 | tf_op jit(solution)/shard_map/ppermute | solution.py:339
  41.6 14.7 %collective-permute-start.10 = (bf16[128,2048]{1,0:T(8,128)(2,1)}, bf16[128,2048]{1,0:T(8,128)(2,1)}, u32[]{:S(2)}, u32[]{:S(2)}) collective-permute-start(bf16[128,2048]{1,0:T(8,128)(2,1)} %collective-permute-done.3.refs_4_), channel_id=1, source_target_pairs={{0,6},{1,7},{2,0},{3,1},{4,2},{5,3},{6,4},{7,5},{8,14},{9,15},{10,... | collective-permute-start | bytes 1572872 | tf_op jit(solution)/shard_map/ppermute | solution.py:339
  44.5 21.5 %collective-permute-start.6 = (bf16[128,2048]{1,0:T(8,128)(2,1)}, bf16[128,2048]{1,0:T(8,128)(2,1)}, u32[]{:S(2)}, u32[]{:S(2)}) collective-permute-start(bf16[128,2048]{1,0:T(8,128)(2,1)} %collective-permute-done.1.refs_2_), channel_id=1, source_target_pairs={{0,1},{1,0},{2,3},{3,2},{4,5},{5,4},{6,7},{7,6},{8,9},{9,8},{10,11... | collective-permute-start | bytes 1572872 | tf_op jit(solution)/shard_map/ppermute | solution.py:342
  44.5 21.6 %collective-permute-start.7 = (bf16[128,2048]{1,0:T(8,128)(2,1)}, bf16[128,2048]{1,0:T(8,128)(2,1)S(1)}, u32[]{:S(2)}, u32[]{:S(2)}) collective-permute-start(bf16[128,2048]{1,0:T(8,128)(2,1)} %collective-permute-done.2.refs_3_), channel_id=1, source_target_pairs={{0,1},{1,0},{2,3},{3,2},{4,5},{5,4},{6,7},{7,6},{8,9},{9,8},{10,11... | collective-permute-start | bytes 1572872 | tf_op jit(solution)/shard_map/ppermute | solution.py:342
  45.0 21.6 %collective-permute-start.8 = (bf16[128,2048]{1,0:T(8,128)(2,1)}, bf16[128,2048]{1,0:T(8,128)(2,1)S(1)}, u32[]{:S(2)}, u32[]{:S(2)}) collective-permute-start(bf16[128,2048]{1,0:T(8,128)(2,1)} %collective-permute-done.3.refs_4_), channel_id=1, source_target_pairs={{0,1},{1,0},{2,3},{3,2},{4,5},{5,4},{6,7},{7,6},{8,9},{9,8},{10,11... | collective-permute-start | bytes 1572872 | tf_op jit(solution)/shard_map/ppermute | solution.py:342
  56.3 18.2 %collective-permute-start.11 = (bf16[128,2048]{1,0:T(8,128)(2,1)}, bf16[128,2048]{1,0:T(8,128)(2,1)}, u32[]{:S(2)}, u32[]{:S(2)}) collective-permute-start(bf16[128,2048]{1,0:T(8,128)(2,1)} %collective-permute-done.9.refs_10_.refs_0_), channel_id=1, source_target_pairs={{0,1},{1,0},{2,3},{3,2},{4,5},{5,4},{6,7},{7,6},{8,9},{9,8},{10,11... | collective-permute-start | bytes 1572872 | tf_op jit(solution)/shard_map/ppermute | solution.py:342
  56.3 18.2 %collective-permute-start.12 = (bf16[128,2048]{1,0:T(8,128)(2,1)}, bf16[128,2048]{1,0:T(8,128)(2,1)}, u32[]{:S(2)}, u32[]{:S(2)}) collective-permute-start(bf16[128,2048]{1,0:T(8,128)(2,1)} %collective-permute-done.10.refs_11_.refs_1_), channel_id=1, source_target_pairs={{0,1},{1,0},{2,3},{3,2},{4,5},{5,4},{6,7},{7,6},{8,9},{9,8},{10,11... | collective-permute-start | bytes 1572872 | tf_op jit(solution)/shard_map/ppermute | solution.py:342
  61.6 1.0 copy-start.6
  62.6 3.4 %copy-start.4 = (bf16[128,2,2048]{2,1,0:T(2,128)(2,1)S(1)}, bf16[128,2,2048]{2,1,0:T(2,128)(2,1)}, u32[]{:S(2)}) copy-start(bf16[128,2,2048]{2,1,0:T(2,128)(2,1)} %h_ref.7) | copy-start | bytes 3145732
  66.0 21.2 %collective-permute-start.13 = (bf16[128,2,2048]{2,1,0:T(2,128)(2,1)S(1)}, bf16[128,2,2048]{2,1,0:T(2,128)(2,1)}, u32[]{:S(2)}, u32[]{:S(2)}) collective-permute-start(bf16[128,2,2048]{2,1,0:T(2,128)(2,1)S(1)} %copy-done.4), channel_id=1, source_target_pairs={{0,1},{1,0},{2,3},{3,2},{4,5},{5,4},{6,7},{7,6},{8,9},{9,8},{10,11... | collective-permute-start | bytes 3145736 | tf_op jit(solution)/shard_map/ppermute | solution.py:342
  66.2 0.8 copy-start.8
  66.2 21.1 %collective-permute-start.14 = (bf16[256,2048]{1,0:T(8,128)(2,1)}, bf16[256,2048]{1,0:T(8,128)(2,1)}, u32[]{:S(2)}, u32[]{:S(2)}) collective-permute-start(bf16[256,2048]{1,0:T(8,128)(2,1)} %value_grad.1.dv_ref), channel_id=1, source_target_pairs={{0,1},{1,0},{2,3},{3,2},{4,5},{5,4},{6,7},{7,6},{8,9},{9,8},{10,11... | collective-permute-start | bytes 3145736 | tf_op jit(solution)/shard_map/ppermute | solution.py:342
  66.9 0.8 copy-start.9
  80.0 23.7 %all-to-all-start.2 = ((bf16[16,256,128]{2,1,0:T(8,128)(2,1)}), bf16[16,256,128]{2,1,0:T(8,128)(2,1)S(1)}, u32[]{:S(2)}, u32[]{:S(2)}) async-start(bf16[16,256,128]{2,1,0:T(8,128)(2,1)} %bitcast.9), calls=%async_computation.2 | async-start | bytes 2097152 | tf_op jit(solution)/shard_map/all_to_all | solution.py:316
  91.1 28.7 %collective-permute-start.15 = (bf16[128,2048]{1,0:T(8,128)(2,1)}, bf16[128,2048]{1,0:T(8,128)(2,1)S(1)}, u32[]{:S(2)}, u32[]{:S(2)}) collective-permute-start(bf16[128,2048]{1,0:T(8,128)(2,1)} %get-tuple-element.35), channel_id=1, source_target_pairs={{0,2},{1,3},{2,4},{3,5},{4,6},{5,7},{6,0},{7,1},{8,10},{9,11},{10,... | collective-permute-start | bytes 1572872 | tf_op jit(solution)/shard_map/ppermute | solution.py:339
  91.3 28.4 %collective-permute-start.16 = (bf16[128,2048]{1,0:T(8,128)(2,1)}, bf16[128,2048]{1,0:T(8,128)(2,1)S(1)}, u32[]{:S(2)}, u32[]{:S(2)}) collective-permute-start(bf16[128,2048]{1,0:T(8,128)(2,1)} %get-tuple-element.37), channel_id=1, source_target_pairs={{0,6},{1,7},{2,0},{3,1},{4,2},{5,3},{6,4},{7,5},{8,14},{9,15},{10,... | collective-permute-start | bytes 1572872 | tf_op jit(solution)/shard_map/ppermute | solution.py:339
  104.9 41.3 %all-to-all-start.3 = ((bf16[16,256,128]{2,1,0:T(8,128)(2,1)}), bf16[16,256,128]{2,1,0:T(8,128)(2,1)S(1)}, u32[]{:S(2)}, u32[]{:S(2)}) async-start(bf16[16,256,128]{2,1,0:T(8,128)(2,1)} %scan.3), calls=%async_computation.3 | async-start | bytes 2097152 | tf_op jit(solution)/shard_map/all_to_all | solution.py:316
  117.6 15.0 %collective-permute-start.18 = (bf16[128,2048]{1,0:T(8,128)(2,1)}, bf16[128,2048]{1,0:T(8,128)(2,1)S(1)}, u32[]{:S(2)}, u32[]{:S(2)}) collective-permute-start(bf16[128,2048]{1,0:T(8,128)(2,1)} %get-tuple-element.39), channel_id=1, source_target_pairs={{0,6},{1,7},{2,0},{3,1},{4,2},{5,3},{6,4},{7,5},{8,14},{9,15},{10,... | collective-permute-start | bytes 1572872 | tf_op jit(solution)/shard_map/ppermute | solution.py:339
  119.7 16.2 %collective-permute-start.19 = (bf16[128,2048]{1,0:T(8,128)(2,1)}, bf16[128,2048]{1,0:T(8,128)(2,1)S(1)}, u32[]{:S(2)}, u32[]{:S(2)}) collective-permute-start(bf16[128,2048]{1,0:T(8,128)(2,1)} %get-tuple-element.41), channel_id=1, source_target_pairs={{0,2},{1,3},{2,4},{3,5},{4,6},{5,7},{6,0},{7,1},{8,10},{9,11},{10,... | collective-permute-start | bytes 1572872 | tf_op jit(solution)/shard_map/ppermute | solution.py:339
  119.7 1.0 copy-start
  120.8 1.0 copy-start.1
  121.8 22.8 %copy-start.2 = (bf16[128,2048]{1,0:T(8,128)(2,1)S(1)}, bf16[128,2048]{1,0:T(8,128)(2,1)}, u32[]{:S(2)}) copy-start(bf16[128,2048]{1,0:T(8,128)(2,1)} %get-tuple-element.33.refs_0_) | copy-start | bytes 1572868
  121.8 22.8 %copy-start.3 = (bf16[128,2048]{1,0:T(8,128)(2,1)S(1)}, bf16[128,2048]{1,0:T(8,128)(2,1)}, u32[]{:S(2)}) copy-start(bf16[128,2048]{1,0:T(8,128)(2,1)} %get-tuple-element.40.refs_3_) | copy-start | bytes 1572868
  122.1 22.6 %collective-permute-start.17 = (bf16[128,2048]{1,0:T(8,128)(2,1)S(1)}, bf16[128,2048]{1,0:T(8,128)(2,1)S(1)}, u32[]{:S(2)}, u32[]{:S(2)}) collective-permute-start(bf16[128,2048]{1,0:T(8,128)(2,1)S(1)} %get-tuple-element.38), channel_id=1, source_target_pairs={{0,2},{1,3},{2,4},{3,5},{4,6},{5,7},{6,0},{7,1},{8,10},{9,11},{10,... | collective-permute-start | bytes 1572872 | tf_op jit(solution)/shard_map/ppermute | solution.py:339
  122.2 22.5 %collective-permute-start.20 = (bf16[128,2048]{1,0:T(8,128)(2,1)S(1)}, bf16[128,2048]{1,0:T(8,128)(2,1)S(1)}, u32[]{:S(2)}, u32[]{:S(2)}) collective-permute-start(bf16[128,2048]{1,0:T(8,128)(2,1)S(1)} %get-tuple-element.42), channel_id=1, source_target_pairs={{0,6},{1,7},{2,0},{3,1},{4,2},{5,3},{6,4},{7,5},{8,14},{9,15},{10,... | collective-permute-start | bytes 1572872 | tf_op jit(solution)/shard_map/ppermute | solution.py:339
  146.2 15.7 %copy-start.7 = (bf16[16,256,128]{2,1,0:T(8,128)(2,1)}, bf16[16,256,128]{2,1,0:T(8,128)(2,1)S(1)}, u32[]{:S(2)}) copy-start(bf16[16,256,128]{2,1,0:T(8,128)(2,1)S(1)} %all-to-all-done.3) | copy-start | bytes 3145732
  146.2 22.9 %all-to-all-start.4 = ((bf16[16,256,128]{2,1,0:T(8,128)(2,1)}), bf16[16,256,128]{2,1,0:T(8,128)(2,1)S(1)}, u32[]{:S(2)}, u32[]{:S(2)}) async-start(bf16[16,256,128]{2,1,0:T(8,128)(2,1)} %join.1), calls=%async_computation.4 | async-start | bytes 2097152 | tf_op jit(solution)/shard_map/all_to_all | solution.py:316
